TPU v7x, 128 devices: a whole 4x4x4 slice. The times are simulated.
128 devices in a mesh: kv: 32 (over z, y, core), tp: 4 (over x).
Axes of the slice: x: 4, y: 4, z: 4, core: 2. Of those that a mesh axis runs over, the one named last changes fastest.
Arguments:
- query_rows: bfloat16 [65536, 1536], P('kv', 'tp'), may hold values from -6 to 6
- key_rows: bfloat16 [65536, 1536], P('kv', 'tp'), may hold values from -6 to 6
- value_rows: bfloat16 [65536, 1536], P('kv', 'tp'), may hold values from -6 to 6
- log_sums: float32 [12, 65536], P('tp', 'kv'), may hold values from 5.5 to 7.5
- cotangent: bfloat16 [65536, 1536], P('kv', 'tp'), may hold values from -24 to 24
- layer_input: bfloat16 [65536, 4096], P('kv', 'tp'), may hold values from -0.29882812 to 0.29882812
- chosen: int32 [12, 2048, 12], P('tp'), may hold values from -1 to 1983, as said below
Outputs:
- grad_queries: bfloat16 [65536, 1536], P('kv', 'tp')
- grad_keys: float32 [65536, 1536], P('kv', 'tp')
- grad_values: float32 [65536, 1536], P('kv', 'tp')
- grad_weight: float32 [4096, 1536], P(('tp', 'kv'))
Inputs may be any that keep to these rules, and one draw needn't show every extreme that they name: `chosen`: for query block i, write j = i // 64. Every entry other than -1 names a block below j * 64; the entries of a row are distinct, the -1 entries stand last, and a row has exactly min(12, 2 * min(j, 31)) entries other than -1. For one head, the rows with the same j name at most 2 distinct blocks of any one span; for j >= 1 the span j - 1 gives exactly 2 blocks, named by every such row.
All inputs are finite; a program needn't handle non-finite values.
Results may differ from a plain program's by a relative error of at most 0.007.
Values may be sent and summed in bfloat16 or wider, within the bound.
No kernel may reach another device: no remote copies, remote signals or barrier semaphores. Data moves between devices by JAX's collectives and lax.ppermute only.
A program may use at most 192 MiB of HBM per device.

v0:
```python
import jax
import jax.numpy as jnp
from jax import lax
from jax.sharding import PartitionSpec as P

HEAD_DIM = 128
KEY_BLOCK = 32
CAP = 2


def sent_together(arrays, axis, split_dim, concat_dim, along):
    widths = [a.shape[along] for a in arrays]
    both = jnp.concatenate(arrays, axis=along)
    result = lax.all_to_all(both, axis, split_axis=split_dim, concat_axis=concat_dim, tiled=True)
    return tuple(jnp.split(result, [sum(widths[:k]) for k in range(1, len(widths))], axis=along))


def cut_along(x, dim, size):
    before, after = (x.shape[:dim], x.shape[dim + 1 :])
    return jnp.moveaxis(x.reshape(*before, size, -1, *after), dim, 0)


def sum_at_owner(x, axis, dim):
    parts = cut_along(x, dim, lax.axis_size(axis))
    arrived = lax.all_to_all(parts, axis, split_axis=0, concat_axis=0, tiled=True)
    return arrived.astype(jnp.float32).sum(axis=0)


def head_terms(inputs):
    (
        query_portion,
        local_key,
        local_value,
        output_gradient,
        log_sum,
        far_keys,
        far_values,
        slot_hot,
        usable,
    ) = inputs
    blocks, block_size, head_size = query_portion.shape
    chosen_count = slot_hot.shape[1]
    scale_factor = head_size ** (-0.5)
    pick_low = slot_hot.astype(jnp.bfloat16)
    pick_full = slot_hot.astype(jnp.float32)
    nearby_keys = (
        jnp.einsum("bcs,skd->bckd", pick_low, far_keys, preferred_element_type=jnp.float32)
        .astype(jnp.bfloat16)
        .reshape(blocks, chosen_count * block_size, head_size)
    )
    nearby_values = (
        jnp.einsum("bcs,skd->bckd", pick_low, far_values, preferred_element_type=jnp.float32)
        .astype(jnp.bfloat16)
        .reshape(blocks, chosen_count * block_size, head_size)
    )
    keep_far = jnp.repeat(usable, block_size, axis=1)[:, None, :]
    lower_triangular = jnp.tril(jnp.ones((block_size, block_size), dtype=bool))[None]
    far_scores = (
        jnp.einsum("cjw,ctw->cjt", query_portion, nearby_keys, preferred_element_type=jnp.float32)
        * scale_factor
    )
    own_scores = (
        jnp.einsum("cjw,ctw->cjt", query_portion, local_key, preferred_element_type=jnp.float32)
        * scale_factor
    )
    remote_probabilities = jnp.where(keep_far, jnp.exp(far_scores - log_sum[:, :, None]), 0.0)
    local_probabilities = jnp.where(
        lower_triangular, jnp.exp(own_scores - log_sum[:, :, None]), 0.0
    )
    far_grads = jnp.einsum(
        "cjw,ctw->cjt", output_gradient, nearby_values, preferred_element_type=jnp.float32
    )
    local_gradients = jnp.einsum(
        "cjw,ctw->cjt", output_gradient, local_value, preferred_element_type=jnp.float32
    )
    row_dots = jnp.sum(remote_probabilities * far_grads, axis=2) + jnp.sum(
        local_probabilities * local_gradients, axis=2
    )
    remote_score_gradient = (remote_probabilities * (far_grads - row_dots[:, :, None])).astype(
        jnp.bfloat16
    )
    local_score_gradient = (local_probabilities * (local_gradients - row_dots[:, :, None])).astype(
        jnp.bfloat16
    )
    query_sum = jnp.einsum(
        "lzs,lsa->lza", remote_score_gradient, nearby_keys, preferred_element_type=jnp.float32
    )
    query_sum = query_sum + jnp.einsum(
        "lzs,lsa->lza", local_score_gradient, local_key, preferred_element_type=jnp.float32
    )
    query_gradient = (scale_factor * query_sum).astype(jnp.bfloat16)
    far_gkey = scale_factor * jnp.einsum(
        "slm,slc->smc", remote_score_gradient, query_portion, preferred_element_type=jnp.float32
    )
    far_gvalue = jnp.einsum(
        "slm,slc->smc",
        remote_probabilities.astype(jnp.bfloat16),
        output_gradient,
        preferred_element_type=jnp.float32,
    )
    own_gkey = scale_factor * jnp.einsum(
        "slm,slc->smc", local_score_gradient, query_portion, preferred_element_type=jnp.float32
    )
    own_gvalue = jnp.einsum(
        "slm,slc->smc",
        local_probabilities.astype(jnp.bfloat16),
        output_gradient,
        preferred_element_type=jnp.float32,
    )
    entry_shape = (blocks, chosen_count, block_size, head_size)
    back_keys = jnp.einsum(
        "bcs,bckd->skd", pick_full, far_gkey.reshape(entry_shape), precision=lax.Precision.HIGHEST
    )
    back_values = jnp.einsum(
        "bcs,bckd->skd", pick_full, far_gvalue.reshape(entry_shape), precision=lax.Precision.HIGHEST
    )
    return (query_gradient, own_gkey, own_gvalue, back_keys, back_values)


def local(query_rows, key_rows, value_rows, log_sums, cotangent, layer_input, chosen):
    kv_count = lax.axis_size("kv")
    kv_place = lax.axis_index("kv")
    local_heads = log_sums.shape[0]
    rows_here = query_rows.shape[0]
    block_size = KEY_BLOCK
    head_size = HEAD_DIM
    blocks = rows_here // block_size
    capacity = CAP
    chosen_count = chosen.shape[2]
    four_shape = (blocks, block_size, local_heads, head_size)
    query_four = query_rows.reshape(four_shape)
    key_four = key_rows.reshape(four_shape)
    value_four = value_rows.reshape(four_shape)
    grad_four = cotangent.reshape(four_shape)
    everyone = chosen.reshape(local_heads, kv_count, blocks, chosen_count)
    own_ids = kv_place * blocks + jnp.arange(blocks, dtype=jnp.int32)
    wanted = jnp.any(everyone[:, :, :, :, None] == own_ids, axis=(2, 3))
    rank_out = jnp.cumsum(wanted.astype(jnp.int32), axis=2) - 1
    slot_ids = jnp.arange(capacity, dtype=jnp.int32)
    slot_hit = wanted[:, :, None, :] & (rank_out[:, :, None, :] == slot_ids[:, None])
    outgoing = slot_hit.astype(jnp.bfloat16)
    send_keys = jnp.einsum(
        "hncb,bkhd->hnckd", outgoing, key_four, preferred_element_type=jnp.float32
    ).astype(jnp.bfloat16)
    send_values = jnp.einsum(
        "hncb,bkhd->hnckd", outgoing, value_four, preferred_element_type=jnp.float32
    ).astype(jnp.bfloat16)
    own_lists = lax.dynamic_slice_in_dim(chosen, kv_place * blocks, blocks, 1)
    usable = own_lists >= 0
    safe_ids = jnp.maximum(own_lists, 0)
    every_id = jnp.arange(kv_count * blocks, dtype=jnp.int32)
    requested = jnp.any(own_lists[:, :, :, None] == every_id, axis=(1, 2)).reshape(
        local_heads, kv_count, blocks
    )
    rank_in = (jnp.cumsum(requested.astype(jnp.int32), axis=2) - 1).reshape(
        local_heads, kv_count * blocks
    )
    rank_of = jnp.take_along_axis(rank_in, safe_ids.reshape(local_heads, -1), axis=1).reshape(
        own_lists.shape
    )
    position = safe_ids // blocks * capacity + rank_of
    slot_count = kv_count * capacity
    slot_hot = usable[:, :, :, None] & (
        position[:, :, :, None] == jnp.arange(slot_count, dtype=jnp.int32)
    )
    piled_along_leading = (
        jnp.moveaxis(query_four, 2, 0),
        jnp.moveaxis(key_four, 2, 0),
        jnp.moveaxis(value_four, 2, 0),
        jnp.moveaxis(grad_four, 2, 0),
        log_sums.reshape(local_heads, blocks, block_size),
    )
    far_shape = (local_heads, slot_count, block_size, head_size)
    back_shape = (local_heads, kv_count, capacity, block_size, head_size)
    pieces = []
    for head_pos in range(local_heads):
        fetched_keys, fetched_values = sent_together(
            (send_keys[head_pos : head_pos + 1], send_values[head_pos : head_pos + 1]),
            "kv",
            1,
            1,
            0,
        )
        head_inputs = tuple((member[head_pos] for member in piled_along_leading))
        result = head_terms(
            head_inputs
            + (
                fetched_keys.reshape(far_shape[1:]),
                fetched_values.reshape(far_shape[1:]),
                slot_hot[head_pos],
                usable[head_pos],
            )
        )
        home_pair = tuple(
            (
                part.astype(jnp.float32)
                for part in sent_together(
                    (
                        result[3].reshape((1,) + back_shape[1:]).astype(jnp.bfloat16),
                        result[4].reshape((1,) + back_shape[1:]).astype(jnp.bfloat16),
                    ),
                    "kv",
                    1,
                    1,
                    0,
                )
            )
        )
        pieces.append(result[:3] + home_pair)
    query_gradient = jnp.stack([piece[0] for piece in pieces])
    own_gkey = jnp.stack([piece[1] for piece in pieces])
    own_gvalue = jnp.stack([piece[2] for piece in pieces])
    home_keys = jnp.concatenate([piece[3] for piece in pieces], axis=0)
    home_values = jnp.concatenate([piece[4] for piece in pieces], axis=0)
    landing = slot_hit.astype(jnp.float32)
    far_key_grad = jnp.einsum(
        "hncb,hnckd->hbkd", landing, home_keys, precision=lax.Precision.HIGHEST
    )
    far_value_grad = jnp.einsum(
        "hncb,hnckd->hbkd", landing, home_values, precision=lax.Precision.HIGHEST
    )
    grad_keys = jnp.moveaxis(own_gkey + far_key_grad, 0, 2).reshape(
        rows_here, local_heads * head_size
    )
    grad_values = jnp.moveaxis(own_gvalue + far_value_grad, 0, 2).reshape(
        rows_here, local_heads * head_size
    )
    grad_queries = jnp.moveaxis(query_gradient, 0, 2).reshape(rows_here, local_heads * head_size)
    all_heads = lax.all_gather(grad_queries, "tp", axis=1, tiled=True)
    grad_weight = sum_at_owner(
        lax.dot_general(
            layer_input, all_heads, (((0,), (0,)), ((), ())), preferred_element_type=jnp.float32
        ).astype(jnp.bfloat16),
        "kv",
        0,
    )
    return (grad_queries, grad_keys, grad_values, grad_weight)


def solution(mesh):
    placed = (
        P("kv", "tp"),
        P("kv", "tp"),
        P("kv", "tp"),
        P("tp", "kv"),
        P("kv", "tp"),
        P("kv", "tp"),
        P("tp", None, None),
    )
    return jax.shard_map(
        local,
        mesh=mesh,
        in_specs=placed,
        out_specs=(P("kv", "tp"), P("kv", "tp"), P("kv", "tp"), P(("tp", "kv"), None)),
        check_vma=False,
    )
```

profile of v0, /device:TPU:0, one launch (start us, length us, event | category | flops | bytes accessed | tf_op | source)
XLA Modules:
  0.0 474.2 jit_solution(7196066404645238701)
XLA Ops:
  7.2 4.0 reshape.212
  11.8 13.0 %compare_reduce_fusion = pred[3,32,64]{2,1,0:T(8,128)(4,1)S(1)} fusion(s32[64]{0:T(128)S(1)} %iota_add_fusion, s32[3,32,64,12]{2,3,1,0:T(8,128)S(1)} %copy.256), kind=kLoop, calls=%fused_computation.1 | loop fusion | flops 9431040 | bytes 301312 | tf_op jit(solution)/shard_map/reduce_or | solution.py:137
  25.5 5.1 %reshape.213 = bf16[64,32,3,128]{3,2,1,0:T(4,128)(2,1)} reshape(bf16[2048,384]{1,0:T(8,128)(2,1)} %param.9) | data formatting | bytes 3145728 | tf_op jit(solution)/shard_map/reshape | solution.py:133
  30.6 2.2 convolution_convert_fusion.8
  32.8 2.2 convolution_convert_fusion.7
  38.1 8.7 %all-to-all-start.2 = ((bf16[2,32,2,32,128]{4,3,2,0,1:T(8,128)(2,1)}), bf16[2,32,2,32,128]{4,3,2,0,1:T(8,128)(2,1)}, u32[]{:S(2)}, u32[]{:S(2)}) async-start(bf16[2,32,2,32,128]{4,3,2,0,1:T(8,128)(2,1)} %copy.283), calls=%async_computation.2 | async-start | bytes 2097152 | tf_op jit(solution)/shard_map/all_to_all | solution.py:14
  46.9 3.4 fusion
  50.3 2.0 reshape.219
  52.4 2.8 copy_bitcast_fusion.3
  60.4 19.0 %gather_fusion = s32[2304]{0:T(1024)S(1)} fusion(s32[3,2048]{1,0:T(4,128)S(1)} %sub.121, s32[2304]{0:T(1024)S(1)} %reshape.239), kind=kCustom, calls=%fused_computation | custom fusion | bytes 36864 | tf_op jit(solution)/shard_map/jit(take_along_axis)/gather | solution.py:158
  82.1 5.1 %reshape.216 = bf16[64,32,3,128]{3,2,1,0:T(4,128)(2,1)} reshape(bf16[2048,384]{1,0:T(8,128)(2,1)} %param.7) | data formatting | bytes 3145728 | tf_op jit(solution)/shard_map/reshape | solution.py:131
  87.3 4.0 copy_bitcast_fusion.4
  98.4 3.0 multiply_reduce_fusion
  101.3 2.2 multiply_reduce_fusion.1
  105.0 7.8 %all-to-all-start.1 = ((bf16[2,32,2,32,128]{4,3,2,0,1:T(8,128)(2,1)}), bf16[2,32,2,32,128]{4,3,2,0,1:T(8,128)(2,1)}, u32[]{:S(2)}, u32[]{:S(2)}) async-start(bf16[2,32,2,32,128]{4,3,2,0,1:T(8,128)(2,1)} %copy.273), calls=%async_computation.1 | async-start | bytes 2097152 | tf_op jit(solution)/shard_map/all_to_all | solution.py:14
  118.6 13.1 %exponential_select_fusion = f32[64,384,32]{1,2,0:T(8,128)S(1)} fusion(bf16[64,384,128]{2,0,1:T(8,128)(2,1)S(1)} %bitcast.450, f32[64,32]{1,0:T(8,128)S(1)} %copy-done.45, pred[64,384]{1,0:T(8,128)(4,1)S(1)} %copy-done.48, bf16[3,64,32,128]{3,2,1,0:T(8,128)(2,1)S(1)} %get-tuple-element.51), kind=kOutput, calls=%fused_computation.75 | convolution fusion | flops 203685888 | bytes 10018816 | tf_op jit(solution)/shard_map/cjw,ctw->cjt/dot_general | solution.py:59
  131.7 13.0 %fusion.39 = (f32[64,32]{1,0:T(8,128)S(1)}, f32[64,384,32]{1,2,0:T(8,128)S(1)}) fusion(f32[64,384,32]{1,2,0:T(8,128)S(1)} %exponential_select_fusion, bf16[3,64,32,128]{3,2,1,0:T(8,128)(2,1)S(1)} %get-tuple-element.49, bf16[64,384,128]{2,0,1:T(8,128)(2,1)S(1)} %bitcast.447), kind=kOutput, calls=%fused_computation.59 | convolution fusion | flops 202897408 | bytes 13115392 | tf_op jit(solution)/shard_map/cjw,ctw->cjt/dot_general | solution.py:70
  147.4 7.4 %all-to-all-start = ((bf16[2,32,2,32,128]{4,3,2,0,1:T(8,128)(2,1)}), bf16[2,32,2,32,128]{4,3,2,0,1:T(8,128)(2,1)}, u32[]{:S(2)}, u32[]{:S(2)}) async-start(bf16[2,32,2,32,128]{4,3,2,0,1:T(8,128)(2,1)} %copy.259), calls=%async_computation | async-start | bytes 2097152 | tf_op jit(solution)/shard_map/all_to_all | solution.py:14
  156.2 4.5 convolution_convert_fusion.4
  162.5 9.2 %exponential_select_fusion.1 = f32[64,384,32]{1,2,0:T(8,128)S(1)} fusion(bf16[64,384,128]{2,0,1:T(8,128)(2,1)} %bitcast.454, f32[64,32]{1,0:T(8,128)S(1)} %copy-done.44, pred[64,384]{1,0:T(8,128)(4,1)S(1)} %copy-done.47, bf16[3,64,32,128]{3,2,1,0:T(8,128)(2,1)S(1)} %get-tuple-element.51), kind=kOutput, calls=%fused_computation.76 | convolution fusion | flops 203685888 | bytes 10018816 | tf_op jit(solution)/shard_map/cjw,ctw->cjt/dot_general | solution.py:59
  171.8 13.0 %fusion.42 = (f32[64,32]{1,0:T(8,128)S(1)}, f32[64,384,32]{1,2,0:T(8,128)S(1)}) fusion(f32[64,384,32]{1,2,0:T(8,128)S(1)} %exponential_select_fusion.1, bf16[3,64,32,128]{3,2,1,0:T(8,128)(2,1)S(1)} %get-tuple-element.49, bf16[64,384,128]{2,0,1:T(8,128)(2,1)S(1)} %bitcast.448), kind=kOutput, calls=%fused_computation.65 | convolution fusion | flops 202897408 | bytes 13115392 | tf_op jit(solution)/shard_map/cjw,ctw->cjt/dot_general | solution.py:70
  188.0 13.4 %fusion.25 = f32[64,32,128]{2,1,0:T(8,128)} fusion(bf16[64,32,384]{2,1,0:T(8,128)(2,1)S(1)} %copy-done.10, bf16[64,384,128]{2,0,1:T(8,128)(2,1)S(1)} %bitcast.453), kind=kOutput, calls=%fused_computation.32 | convolution fusion | flops 201326592 | bytes 8912896 | tf_op jit(solution)/shard_map/lzs,lsa->lza/dot_general | solution.py:85
  201.4 13.5 %fusion.29 = f32[64,32,128]{2,1,0:T(8,128)} fusion(bf16[64,32,384]{2,1,0:T(8,128)(2,1)S(1)} %fusion.44, bf16[64,384,128]{2,0,1:T(8,128)(2,1)S(1)} %bitcast.457), kind=kOutput, calls=%fused_computation.36 | convolution fusion | flops 201326592 | bytes 8912896 | tf_op jit(solution)/shard_map/lzs,lsa->lza/dot_general | solution.py:85
  219.8 12.8 %exponential_select_fusion.2 = f32[64,384,32]{1,2,0:T(8,128)S(1)} fusion(bf16[64,384,128]{2,0,1:T(8,128)(2,1)S(1)} %bitcast.458, f32[64,32]{1,0:T(8,128)S(1)} %copy-done.43, pred[64,384]{1,0:T(8,128)(4,1)S(1)} %copy-done.46, bf16[3,64,32,128]{3,2,1,0:T(8,128)(2,1)S(1)} %get-tuple-element.51), kind=kOutput, calls=%fused_computation.77 | convolution fusion | flops 203685888 | bytes 10018816 | tf_op jit(solution)/shard_map/cjw,ctw->cjt/dot_general | solution.py:59
  232.5 14.6 %fusion.45 = (f32[64,32]{1,0:T(8,128)S(1)}, f32[64,384,32]{1,2,0:T(8,128)}) fusion(f32[64,384,32]{1,2,0:T(8,128)S(1)} %exponential_select_fusion.2, bf16[3,64,32,128]{3,2,1,0:T(8,128)(2,1)S(1)} %get-tuple-element.49, bf16[64,384,128]{2,0,1:T(8,128)(2,1)S(1)} %bitcast.449), kind=kOutput, calls=%fused_computation.71 | convolution fusion | flops 202897408 | bytes 13115392 | tf_op jit(solution)/shard_map/cjw,ctw->cjt/dot_general | solution.py:70
  247.2 2.4 fusion.47
  249.6 12.6 %fusion.33 = f32[64,32,128]{2,1,0:T(8,128)S(1)} fusion(bf16[64,32,384]{2,1,0:T(8,128)(2,1)S(1)} %fusion.47, bf16[64,384,128]{2,0,1:T(8,128)(2,1)S(1)} %bitcast.459), kind=kOutput, calls=%fused_computation.40 | convolution fusion | flops 201326592 | bytes 8912896 | tf_op jit(solution)/shard_map/lzs,lsa->lza/dot_general | solution.py:85
  272.1 3.7 fusion.56
  275.9 12.3 %fusion.141 = bf16[1,32,2,32,128]{4,1,3,2,0:T(8,128)(2,1)S(1)} fusion(f32[64,12,32,128]{3,2,1,0:T(8,128)S(1)} %bitcast.445, pred[32,2,64,12,1]{2,3,1,0,4:T(8,128)(4,1)S(1)} %bitcast.480), kind=kOutput, calls=%fused_computation.153 | convolution fusion | flops 2416181248 | bytes 13156352 | tf_op jit(solution)/shard_map/bcs,bckd->skd/dot_general | solution.py:114
  290.0 12.5 %fusion.138 = bf16[1,32,2,32,128]{4,1,3,2,0:T(8,128)(2,1)S(1)} fusion(f32[64,12,32,128]{3,2,1,0:T(8,128)S(1)} %bitcast.442, pred[32,2,64,12,1]{2,3,1,0,4:T(8,128)(4,1)S(1)} %bitcast.481), kind=kOutput, calls=%fused_computation.152 | convolution fusion | flops 2416181248 | bytes 13156352 | tf_op jit(solution)/shard_map/bcs,bckd->skd/dot_general | solution.py:111
  304.0 7.6 %all-to-all-start.5 = ((bf16[2,32,2,32,128]{4,3,2,0,1:T(8,128)(2,1)}), bf16[2,32,2,32,128]{4,3,2,0,1:T(8,128)(2,1)}, u32[]{:S(2)}, u32[]{:S(2)}) async-start(bf16[2,32,2,32,128]{4,3,2,0,1:T(8,128)(2,1)} %copy.312), calls=%async_computation.5 | async-start | bytes 2097152 | tf_op jit(solution)/shard_map/all_to_all | solution.py:14
  311.6 3.7 fusion.55
  315.4 12.5 %fusion.135 = bf16[1,32,2,32,128]{4,1,3,2,0:T(8,128)(2,1)S(1)} fusion(f32[64,12,32,128]{3,2,1,0:T(8,128)S(1)} %bitcast.446, pred[32,2,64,12,1]{2,3,1,0,4:T(8,128)(4,1)S(1)} %bitcast.478), kind=kOutput, calls=%fused_computation.151 | convolution fusion | flops 2416181248 | bytes 13156352 | tf_op jit(solution)/shard_map/bcs,bckd->skd/dot_general | solution.py:114
  329.7 12.2 %fusion.132 = bf16[1,32,2,32,128]{4,1,3,2,0:T(8,128)(2,1)S(1)} fusion(f32[64,12,32,128]{3,2,1,0:T(8,128)S(1)} %bitcast.443, pred[32,2,64,12,1]{2,3,1,0,4:T(8,128)(4,1)S(1)} %bitcast.479), kind=kOutput, calls=%fused_computation.150 | convolution fusion | flops 2416181248 | bytes 13156352 | tf_op jit(solution)/shard_map/bcs,bckd->skd/dot_general | solution.py:111
  343.5 5.6 %broadcast_multiply_fusion.2 = f32[64,384,128]{2,1,0:T(8,128)} fusion(bf16[64,32,384]{2,1,0:T(8,128)(2,1)S(1)} %copy-done.15, bf16[3,64,32,128]{3,2,1,0:T(8,128)(2,1)S(1)} %get-tuple-element.51), kind=kOutput, calls=%fused_computation.31 | convolution fusion | flops 204472320 | bytes 14680064 | tf_op jit(solution)/shard_map/slm,slc->smc/dot_general | solution.py:92
  349.1 5.6 %fusion.54 = f32[64,384,128]{2,1,0:T(8,128)} fusion(bf16[3,64,32,128]{3,2,1,0:T(8,128)(2,1)S(1)} %get-tuple-element.49, f32[64,384,32]{1,2,0:T(8,128)S(1)} %copy-done.4), kind=kOutput, calls=%fused_computation.82 | convolution fusion | flops 201326592 | bytes 16252928 | tf_op jit(solution)/shard_map/slm,slc->smc/dot_general | solution.py:95
  354.6 7.4 %all-to-all-start.4 = ((bf16[2,32,2,32,128]{4,3,2,0,1:T(8,128)(2,1)}), bf16[2,32,2,32,128]{4,3,2,0,1:T(8,128)(2,1)}, u32[]{:S(2)}, u32[]{:S(2)}) async-start(bf16[2,32,2,32,128]{4,3,2,0,1:T(8,128)(2,1)} %copy.305), calls=%async_computation.4 | async-start | bytes 2097152 | tf_op jit(solution)/shard_map/all_to_all | solution.py:14
  362.1 16.8 %fusion.129 = bf16[1,32,2,32,128]{4,1,3,2,0:T(8,128)(2,1)S(1)} fusion(f32[64,12,32,128]{3,2,1,0:T(8,128)} %bitcast.444, pred[32,2,64,12,1]{2,3,1,0,4:T(8,128)(4,1)S(1)} %bitcast.476), kind=kOutput, calls=%fused_computation.149 | convolution fusion | flops 2416181248 | bytes 13156352 | tf_op jit(solution)/shard_map/bcs,bckd->skd/dot_general | solution.py:114
  378.9 12.1 %fusion.126 = bf16[1,32,2,32,128]{4,1,3,2,0:T(8,128)(2,1)S(1)} fusion(f32[64,12,32,128]{3,2,1,0:T(8,128)S(1)} %bitcast.441, pred[32,2,64,12,1]{2,3,1,0,4:T(8,128)(4,1)S(1)} %bitcast.477), kind=kOutput, calls=%fused_computation.148 | convolution fusion | flops 2416181248 | bytes 13156352 | tf_op jit(solution)/shard_map/bcs,bckd->skd/dot_general | solution.py:111
  392.6 7.4 %all-to-all-start.3 = ((bf16[2,32,2,32,128]{4,3,2,0,1:T(8,128)(2,1)}), bf16[2,32,2,32,128]{4,3,2,0,1:T(8,128)(2,1)}, u32[]{:S(2)}, u32[]{:S(2)}) async-start(bf16[2,32,2,32,128]{4,3,2,0,1:T(8,128)(2,1)} %copy.298), calls=%async_computation.3 | async-start | bytes 2097152 | tf_op jit(solution)/shard_map/all_to_all | solution.py:14
  400.1 11.4 %convolution_convert_fusion = bf16[1536,1024]{0,1:T(8,128)(2,1)} fusion(bf16[2048,1536]{1,0:T(8,128)(2,1)} %all-gather.2.cloned.1.call-done, bf16[2048,1024]{1,0:T(8,128)(2,1)} %param.12), kind=kOutput, calls=%fused_computation.44 | convolution fusion | flops 6444023808 | bytes 13631488 | tf_op jit(solution)/shard_map/dot_general | solution.py:231
  411.4 5.8 %all-to-all-done.3 = bf16[2,32,2,32,128]{4,3,2,0,1:T(8,128)(2,1)} async-done(((bf16[2,32,2,32,128]{4,3,2,0,1:T(8,128)(2,1)}), bf16[2,32,2,32,128]{4,3,2,0,1:T(8,128)(2,1)}, u32[]{:S(2)}, u32[]{:S(2)}) %all-to-all-start.3) | async-done | bytes 1048608 | tf_op jit(solution)/shard_map/all_to_all | solution.py:14
  417.2 4.8 %all-to-all-start.6 = ((bf16[32,32,1536]{2,1,0:T(8,128)(2,1)}), bf16[32,32,1536]{2,1,0:T(8,128)(2,1)}, u32[]{:S(2)}, u32[]{:S(2)}) async-start(bf16[32,32,1536]{2,1,0:T(8,128)(2,1)} %bitcast.469), calls=%async_computation.6 | async-start | bytes 6291456 | tf_op jit(solution)/shard_map/all_to_all | solution.py:25
  433.3 2.9 copy.315
  439.8 2.2 fusion.38
  442.1 2.9 copy.320
  447.0 17.1 %all-to-all-done.6 = bf16[32,32,1536]{2,1,0:T(8,128)(2,1)} async-done(((bf16[32,32,1536]{2,1,0:T(8,128)(2,1)}), bf16[32,32,1536]{2,1,0:T(8,128)(2,1)}, u32[]{:S(2)}, u32[]{:S(2)}) %all-to-all-start.6) | async-done | bytes 3145760 | tf_op jit(solution)/shard_map/all_to_all | solution.py:25
  464.1 3.0 convert_reduce_fusion
  (216 shorter events, 75.2 us)
Async XLA Ops:
  7.2 4.0 copy-start.41
  11.2 19.5 %copy-start.6 = (bf16[64,32,3,128]{3,2,1,0:T(4,128)(2,1)}, bf16[64,32,3,128]{3,2,1,0:T(4,128)(2,1)S(1)}, u32[]{:S(2)}) copy-start(bf16[64,32,3,128]{3,2,1,0:T(4,128)(2,1)S(1)} %reshape.212) | copy-start | bytes 4718596
  24.7 8.1 %copy-start.39 = (pred[3,32,64]{2,1,0:T(8,128)(4,1)}, pred[3,32,64]{2,1,0:T(8,128)(4,1)S(1)}, u32[]{:S(2)}) copy-start(pred[3,32,64]{2,1,0:T(8,128)(4,1)S(1)} %compare_reduce_fusion) | copy-start | bytes 18436
  25.5 7.3 %copy-start.36 = (s32[3,32,64]{2,1,0:T(8,128)}, s32[3,32,64]{2,1,0:T(8,128)S(1)}, u32[]{:S(2)}) copy-start(s32[3,32,64]{2,1,0:T(8,128)S(1)} %broadcast_add_fusion) | copy-start | bytes 73732
  30.6 2.2 copy-start.7
  36.6 13.7 %copy-start.38 = (bf16[2048,384]{1,0:T(8,128)(2,1)S(1)}, bf16[2048,384]{1,0:T(8,128)(2,1)}, u32[]{:S(2)}) copy-start(bf16[2048,384]{1,0:T(8,128)(2,1)} %param.11) | copy-start | bytes 4718596
  38.1 66.9 %all-to-all-start.2 = ((bf16[2,32,2,32,128]{4,3,2,0,1:T(8,128)(2,1)}), bf16[2,32,2,32,128]{4,3,2,0,1:T(8,128)(2,1)}, u32[]{:S(2)}, u32[]{:S(2)}) async-start(bf16[2,32,2,32,128]{4,3,2,0,1:T(8,128)(2,1)} %copy.283), calls=%async_computation.2 | async-start | bytes 2097152 | tf_op jit(solution)/shard_map/all_to_all | solution.py:14
  60.4 20.2 %copy-start.49 = (f32[3,2048]{1,0:T(4,128)S(1)}, f32[3,2048]{1,0:T(4,128)}, u32[]{:S(2)}) copy-start(f32[3,2048]{1,0:T(4,128)} %param.10) | copy-start | bytes 73732
  87.3 4.0 copy-start.34
  87.3 4.0 copy-start.35
  98.3 3.0 copy-start.8
  98.3 3.0 copy-start.23
  98.3 5.2 %copy-start.21 = (f32[64,32,32]{1,2,0:T(8,128)S(1)}, f32[64,32,32]{1,2,0:T(8,128)}, u32[]{:S(2)}) copy-start(f32[64,32,32]{1,2,0:T(8,128)} %fusion.147) | copy-start | bytes 786436
  98.3 5.2 %copy-start.42 = (f32[64,32]{1,0:T(8,128)S(1)}, f32[64,32]{1,0:T(8,128)}, u32[]{:S(2)}) copy-start(f32[64,32]{1,0:T(8,128)} %sub.123) | copy-start | bytes 24580
  105.0 42.4 %all-to-all-start.1 = ((bf16[2,32,2,32,128]{4,3,2,0,1:T(8,128)(2,1)}), bf16[2,32,2,32,128]{4,3,2,0,1:T(8,128)(2,1)}, u32[]{:S(2)}, u32[]{:S(2)}) async-start(bf16[2,32,2,32,128]{4,3,2,0,1:T(8,128)(2,1)} %copy.273), calls=%async_computation.1 | async-start | bytes 2097152 | tf_op jit(solution)/shard_map/all_to_all | solution.py:14
  115.9 2.7 copy-start.5
  115.9 2.7 copy-start.45
  116.0 2.7 copy-start.48
  131.7 14.2 %copy-start.1 = (f32[64,384,32]{1,2,0:T(8,128)}, f32[64,384,32]{1,2,0:T(8,128)S(1)}, u32[]{:S(2)}) copy-start(f32[64,384,32]{1,2,0:T(8,128)S(1)} %exponential_select_fusion) | copy-start | bytes 9437188
  131.7 13.1 %copy-start.16 = (f32[64,32,32]{1,2,0:T(8,128)S(1)}, f32[64,32,32]{1,2,0:T(8,128)}, u32[]{:S(2)}) copy-start(f32[64,32,32]{1,2,0:T(8,128)} %get-tuple-element.36) | copy-start | bytes 786436
  131.7 13.1 %copy-start.25 = (f32[64,32,32]{1,2,0:T(8,128)S(1)}, f32[64,32,32]{1,2,0:T(8,128)}, u32[]{:S(2)}) copy-start(f32[64,32,32]{1,2,0:T(8,128)} %fusion.145) | copy-start | bytes 786436
  147.4 67.4 %all-to-all-start = ((bf16[2,32,2,32,128]{4,3,2,0,1:T(8,128)(2,1)}), bf16[2,32,2,32,128]{4,3,2,0,1:T(8,128)(2,1)}, u32[]{:S(2)}, u32[]{:S(2)}) async-start(bf16[2,32,2,32,128]{4,3,2,0,1:T(8,128)(2,1)} %copy.259), calls=%async_computation | async-start | bytes 2097152 | tf_op jit(solution)/shard_map/all_to_all | solution.py:14
  154.9 245.2 %all-gather.2.cloned.1.call-start = ((), (), s32[]{:S(2)}) async-start(), calls=%async_computation.7 | async-start | bytes 7864320 | tf_op jit(solution)/shard_map/all_gather | solution.py:229
  162.5 25.4 %slice-start = ((s8[6291456]{0:T(1024)(128)(4,1)}), s8[4194304]{0:T(1024)(128)(4,1)S(1)}, s32[]{:S(2)}) async-start(s8[6291456]{0:T(1024)(128)(4,1)} %bitcast.451), calls=%async_computation.8 | async-start | bytes 8388608
  171.8 13.1 %copy-start.2 = (f32[64,384,32]{1,2,0:T(8,128)}, f32[64,384,32]{1,2,0:T(8,128)S(1)}, u32[]{:S(2)}) copy-start(f32[64,384,32]{1,2,0:T(8,128)S(1)} %exponential_select_fusion.1) | copy-start | bytes 9437188
  171.8 16.2 %slice-start.1 = ((s8[6291456]{0:T(1024)(128)(4,1)}), s8[2097152]{0:T(1024)(128)(4,1)S(1)}, s32[]{:S(2)}) async-start(s8[6291456]{0:T(1024)(128)(4,1)} %bitcast.451), calls=%async_computation.9 | async-start | bytes 4194304
  184.9 2.1 copy-start.24
  185.2 16.1 %copy-start.12 = (bf16[64,32,384]{2,1,0:T(8,128)(2,1)}, bf16[64,32,384]{2,1,0:T(8,128)(2,1)S(1)}, u32[]{:S(2)}) copy-start(bf16[64,32,384]{2,1,0:T(8,128)(2,1)S(1)} %fusion.44) | copy-start | bytes 4718596
  185.3 2.7 copy-start.10
  186.9 14.5 %slice-start.2 = ((s8[6291456]{0:T(1024)(128)(4,1)}), s8[4194304]{0:T(1024)(128)(4,1)S(1)}, s32[]{:S(2)}) async-start(s8[6291456]{0:T(1024)(128)(4,1)} %bitcast.455), calls=%async_computation.10 | async-start | bytes 8388608
  188.0 13.4 %slice-start.3 = ((s8[6291456]{0:T(1024)(128)(4,1)}), s8[2097152]{0:T(1024)(128)(4,1)S(1)}, s32[]{:S(2)}) async-start(s8[6291456]{0:T(1024)(128)(4,1)} %bitcast.455), calls=%async_computation.11 | async-start | bytes 4194304
  232.5 14.6 %copy-start.3 = (f32[64,384,32]{1,2,0:T(8,128)}, f32[64,384,32]{1,2,0:T(8,128)S(1)}, u32[]{:S(2)}) copy-start(f32[64,384,32]{1,2,0:T(8,128)S(1)} %exponential_select_fusion.2) | copy-start | bytes 9437188
  249.6 12.6 %copy-start.14 = (bf16[64,32,384]{2,1,0:T(8,128)(2,1)}, bf16[64,32,384]{2,1,0:T(8,128)(2,1)S(1)}, u32[]{:S(2)}) copy-start(bf16[64,32,384]{2,1,0:T(8,128)(2,1)S(1)} %fusion.47) | copy-start | bytes 4718596
  249.6 12.7 %copy-start.19 = (f32[64,32,32]{1,2,0:T(8,128)S(1)}, f32[64,32,32]{1,2,0:T(8,128)}, u32[]{:S(2)}) copy-start(f32[64,32,32]{1,2,0:T(8,128)} %get-tuple-element.44) | copy-start | bytes 786436
  249.6 12.7 %copy-start.22 = (f32[64,32,32]{1,2,0:T(8,128)S(1)}, f32[64,32,32]{1,2,0:T(8,128)}, u32[]{:S(2)}) copy-start(f32[64,32,32]{1,2,0:T(8,128)} %fusion.147) | copy-start | bytes 786436
  249.6 12.9 %copy-start.9 = (bf16[3,64,32,128]{3,2,1,0:T(8,128)(2,1)S(1)}, bf16[3,64,32,128]{3,2,1,0:T(8,128)(2,1)}, u32[]{:S(2)}) copy-start(bf16[3,64,32,128]{3,2,1,0:T(8,128)(2,1)} %get-tuple-element.50) | copy-start | bytes 4718596
  249.6 12.9 %copy-start.26 = (bf16[64,32,32]{1,2,0:T(8,128)(2,1)S(1)}, bf16[64,32,32]{1,2,0:T(8,128)(2,1)}, u32[]{:S(2)}) copy-start(bf16[64,32,32]{1,2,0:T(8,128)(2,1)} %multiply_convert_fusion) | copy-start | bytes 393220
  275.8 12.3 %copy-start.11 = (bf16[64,32,384]{2,1,0:T(8,128)(2,1)S(1)}, bf16[64,32,384]{2,1,0:T(8,128)(2,1)}, u32[]{:S(2)}) copy-start(bf16[64,32,384]{2,1,0:T(8,128)(2,1)} %fusion.41) | copy-start | bytes 4718596
  304.0 50.7 %all-to-all-start.5 = ((bf16[2,32,2,32,128]{4,3,2,0,1:T(8,128)(2,1)}), bf16[2,32,2,32,128]{4,3,2,0,1:T(8,128)(2,1)}, u32[]{:S(2)}, u32[]{:S(2)}) async-start(bf16[2,32,2,32,128]{4,3,2,0,1:T(8,128)(2,1)} %copy.312), calls=%async_computation.5 | async-start | bytes 2097152 | tf_op jit(solution)/shard_map/all_to_all | solution.py:14
  315.3 12.5 %copy-start.13 = (bf16[64,32,384]{2,1,0:T(8,128)(2,1)S(1)}, bf16[64,32,384]{2,1,0:T(8,128)(2,1)}, u32[]{:S(2)}) copy-start(bf16[64,32,384]{2,1,0:T(8,128)(2,1)} %copy-done.12) | copy-start | bytes 4718596
  343.5 5.6 %copy-start.4 = (f32[64,384,32]{1,2,0:T(8,128)S(1)}, f32[64,384,32]{1,2,0:T(8,128)}, u32[]{:S(2)}) copy-start(f32[64,384,32]{1,2,0:T(8,128)} %copy-done.3) | copy-start | bytes 9437188
  354.6 38.0 %all-to-all-start.4 = ((bf16[2,32,2,32,128]{4,3,2,0,1:T(8,128)(2,1)}), bf16[2,32,2,32,128]{4,3,2,0,1:T(8,128)(2,1)}, u32[]{:S(2)}, u32[]{:S(2)}) async-start(bf16[2,32,2,32,128]{4,3,2,0,1:T(8,128)(2,1)} %copy.305), calls=%async_computation.4 | async-start | bytes 2097152 | tf_op jit(solution)/shard_map/all_to_all | solution.py:14
  362.1 16.8 %copy-start = (f32[64,384,128]{2,1,0:T(8,128)S(1)}, f32[64,384,128]{2,1,0:T(8,128)}, u32[]{:S(2)}) copy-start(f32[64,384,128]{2,1,0:T(8,128)} %broadcast_multiply_fusion.2) | copy-start | bytes 37748740
  392.6 24.6 %all-to-all-start.3 = ((bf16[2,32,2,32,128]{4,3,2,0,1:T(8,128)(2,1)}), bf16[2,32,2,32,128]{4,3,2,0,1:T(8,128)(2,1)}, u32[]{:S(2)}, u32[]{:S(2)}) async-start(bf16[2,32,2,32,128]{4,3,2,0,1:T(8,128)(2,1)} %copy.298), calls=%async_computation.3 | async-start | bytes 2097152 | tf_op jit(solution)/shard_map/all_to_all | solution.py:14
  417.2 46.8 %all-to-all-start.6 = ((bf16[32,32,1536]{2,1,0:T(8,128)(2,1)}), bf16[32,32,1536]{2,1,0:T(8,128)(2,1)}, u32[]{:S(2)}, u32[]{:S(2)}) async-start(bf16[32,32,1536]{2,1,0:T(8,128)(2,1)} %bitcast.469), calls=%async_computation.6 | async-start | bytes 6291456 | tf_op jit(solution)/shard_map/all_to_all | solution.py:25
  422.1 2.0 copy-start.20
  427.4 3.3 copy-start.37
  427.4 3.3 copy-start.40
  (14 other events, 21.2 us)
Sparse Core Ops, SparseCore 0:
  267.9 66.9 all-gather.1
where the time goes:
time: 481 us; the launch traced here: 474 us
  matrix products  261 us (54%)
  local copies, waits for them, and re-layouts  88.4 us (18%)
  starting transfers between devices  51.4 us (11%)
  other arithmetic  34.9 us (7%)
  waiting for transfers between devices  23 us (5%)
  between operations  15.4 us (3%)
    all_to_all x6, starting transfers between devices, sent_together(): lax.all_to_all(both, axis, split_axis=split_dim, concat_axis=concat_dim,...  46.5 us
    dot_general x3, matrix products, head_terms(): jnp.einsum('bcs,bckd->skd', pick_full, far_gvalue.reshape(entry_shape), p...  41.5 us
    dot_general x3, matrix products, head_terms(): jnp.einsum('cjw,ctw->cjt', output_gradient, nearby_values, preferred_elem...  40.7 us
    dot_general x3, matrix products, head_terms(): jnp.einsum('lzs,lsa->lza', remote_score_gradient, nearby_keys, preferred_...  39.4 us
    dot_general x3, matrix products, head_terms(): jnp.einsum('bcs,bckd->skd', pick_full, far_gkey.reshape(entry_shape), pre...  36.8 us
    dot_general x3, matrix products, head_terms(): jnp.einsum('cjw,ctw->cjt', query_portion, nearby_keys, preferred_element_...  35 us
    gather x4, local copies, waits for them, and re-layouts, local(): jnp.take_along_axis(rank_in, safe_ids.reshape(local_heads, -1), axis=1)  19.2 us
    all_to_all x1, waiting for transfers between devices, sum_at_owner(): lax.all_to_all(parts, axis, split_axis=0, concat_axis=0, tiled=True)  17.1 us
  transfers between devices with their start and end apart: 8, of which 2 were waited for; matrix products, arithmetic and copies ran while one was open for 62% of the time, Pallas kernels for 0%

commit v1 on v0

v1 whole, which is shorter than its diff:
```python
import functools

import jax
import jax.numpy as jnp
from jax import lax
from jax.experimental import pallas as pl
from jax.experimental.pallas import tpu as pltpu
from jax.sharding import PartitionSpec as P

HEAD_DIM = 128
KEY_BLOCK = 32
CAP = 2
BIG = 1 << 20
LOG2E = 1.4426950408889634
NEG = -1.0e30
TQ = 512
KB = 256


def to_lanes(column):
    wide = jnp.broadcast_to(column.astype(jnp.float32), (128, 128))
    return wide.T[0:1, :].astype(jnp.int32)


def pack_kernel(me_ref, chosen_ref, k_ref, v_ref, *rest, heads, spans, blocks, picks):
    sends = rest[:heads]
    tab_ref, bias_ref, lo_s, hi_s, tab_v, tab_s, sem = rest[heads:]
    me = me_ref[0]
    lo_s[...] = jnp.full((128, 128), BIG, jnp.int32)
    hi_s[...] = jnp.full((128, 128), -1, jnp.int32)
    for h in range(heads):

        def one_span(n, carry, h=h):
            ids = chosen_ref[h, pl.ds(n * blocks, blocks), :]
            mine = (ids >> 6) == me
            lo_s[pl.ds(h * spans + n, 1), 0:picks] = jnp.min(
                jnp.where(mine, ids, BIG), axis=0, keepdims=True
            )
            hi_s[pl.ds(h * spans + n, 1), 0:picks] = jnp.max(
                jnp.where(mine, ids, -1), axis=0, keepdims=True
            )
            return carry

        lax.fori_loop(0, spans, one_span, 0, unroll=4)
    lo = to_lanes(jnp.min(lo_s[...], axis=1, keepdims=True))
    hi = to_lanes(jnp.max(hi_s[...], axis=1, keepdims=True))
    tab_v[...] = jnp.zeros((8, 128), jnp.int32)
    tab_v[0:1, :] = lo & (blocks - 1)
    tab_v[1:2, :] = jnp.where(hi >= 0, hi, 0) & (blocks - 1)
    tab_v[2:3, :] = (hi >= 0).astype(jnp.int32)
    tab_v[3:4, :] = (hi > lo).astype(jnp.int32)
    tab_ref[...] = tab_v[...]
    copy = pltpu.make_async_copy(tab_v, tab_s, sem)
    copy.start()
    slot = lax.broadcasted_iota(jnp.int32, (blocks, 128), 1)
    place = lax.broadcasted_iota(jnp.int32, (blocks, blocks * KEY_BLOCK), 1) // KEY_BLOCK
    row = lax.broadcasted_iota(jnp.int32, (blocks, blocks * KEY_BLOCK), 0)
    expand = (place == row).astype(jnp.bfloat16)
    for h in range(heads):
        ids = chosen_ref[h, pl.ds(me * blocks, blocks), :]
        cols = [jnp.broadcast_to(ids[:, c : c + 1], (blocks, 128)) for c in range(picks)]
        least = jnp.full((blocks, 128), BIG, jnp.int32)
        most = jnp.full((blocks, 128), -1, jnp.int32)
        for col in cols:
            hit = (col >> 6) == (slot >> 1)
            least = jnp.minimum(least, jnp.where(hit, col, BIG))
            most = jnp.maximum(most, jnp.where(hit, col, -1))
        least = jnp.min(least, axis=0, keepdims=True)
        most = jnp.max(most, axis=0, keepdims=True)
        name = jnp.where(
            (slot[0:1] & 1) == 0, least, jnp.where(most > least, most, -7)
        )
        named = cols[0] == name
        for col in cols[1:]:
            named = named | (col == name)
        flag = jnp.where(named, 1.0, 0.0).astype(jnp.float32)
        flag = jnp.concatenate([flag, jnp.zeros((128 - blocks, 128), jnp.float32)], axis=0).T
        hot = flag[0 : spans * CAP, 0:blocks].astype(jnp.bfloat16)
        full = jnp.dot(hot, expand, preferred_element_type=jnp.float32)
        bias_ref[h] = jnp.where(full > 0.5, 0.0, NEG)
    copy.wait()
    for h in range(heads):
        lanes = slice(h * HEAD_DIM, (h + 1) * HEAD_DIM)

        def fill(n, carry, h=h, lanes=lanes):
            for c in range(CAP):
                b = tab_s[c, h * spans + n]
                sends[h][n, 0, c] = k_ref[b, :, lanes]
                sends[h][n, 1, c] = v_ref[b, :, lanes]
            return carry

        lax.fori_loop(0, spans, fill, 0, unroll=4)


def attend_kernel(*refs, head, first, tiles, far):
    if first:
        q_ref, g_ref, ko_ref, vo_ref, lse_ref, bias_ref, kv_ref = refs[:7]
        rest = refs[7:]
    else:
        q_ref, g_ref, ko_ref, vo_ref, lse_ref, bias_ref, kv_ref = refs[:7]
        rest = refs[8:]
    gqf_ref, gq_ref, dko_ref, dvo_ref, back_ref = rest[:5]
    p_s, dp_s, ds_s, dk_s, dv_s, kt_s = rest[5:]
    step = pl.program_id(0)
    scale = HEAD_DIM**-0.5
    nkb = far // KB
    per = KB // (CAP * KEY_BLOCK)

    @pl.when(step == 0)
    def _():
        dk_s[...] = jnp.zeros_like(dk_s)
        dv_s[...] = jnp.zeros_like(dv_s)
        for i in range(nkb):
            keys = kv_ref[i * per : (i + 1) * per, 0].reshape(KB, HEAD_DIM)
            kt_s[:, i * KB : (i + 1) * KB] = keys.astype(jnp.float32).T.astype(jnp.bfloat16)

    q = q_ref[...]
    g = g_ref[...]
    lse = lse_ref[head : head + 1, :] * LOG2E
    nt = (((1,), (1,)), ((), ()))

    def ahead(i, dots):
        keys = kv_ref[pl.ds(i * per, per), 0].reshape(KB, HEAD_DIM)
        values = kv_ref[pl.ds(i * per, per), 1].reshape(KB, HEAD_DIM)
        s = lax.dot_general(keys, q, nt, preferred_element_type=jnp.float32)
        dp = lax.dot_general(values, g, nt, preferred_element_type=jnp.float32)
        shift = bias_ref[pl.ds(i * per * CAP, per * CAP), :] - lse
        s = (s * (scale * LOG2E)).reshape(per * CAP, KEY_BLOCK, TQ) + shift[:, None, :]
        p = jnp.exp2(s).reshape(KB, TQ)
        rows = pl.ds(pl.multiple_of(i * KB, KB), KB)
        p_s[rows, :] = p
        dp_s[rows, :] = dp
        dv_s[rows, :] += jnp.dot(
            p.astype(jnp.bfloat16), g, preferred_element_type=jnp.float32
        )
        return dots + (p * dp).reshape(KB // 8, 8, TQ).sum(axis=0)

    dots = lax.fori_loop(0, nkb, ahead, jnp.zeros((8, TQ), jnp.float32))
    dots = jnp.sum(dots, axis=0, keepdims=True)
    key_at = lax.broadcasted_iota(jnp.int32, (128, 128), 0)
    row_at = lax.broadcasted_iota(jnp.int32, (128, 128), 1)
    near = (key_at // KEY_BLOCK == row_at // KEY_BLOCK) & (key_at <= row_at)
    own = []
    own_dots = []
    for t in range(TQ // 128):
        cut = slice(t * 128, (t + 1) * 128)
        s = lax.dot_general(ko_ref[cut, :], q[cut], nt, preferred_element_type=jnp.float32)
        dp = lax.dot_general(vo_ref[cut, :], g[cut], nt, preferred_element_type=jnp.float32)
        p = jnp.exp2(jnp.where(near, s * (scale * LOG2E) - lse[:, cut], NEG))
        own.append((p, dp))
        own_dots.append(jnp.sum(p * dp, axis=0, keepdims=True))
        dvo_ref[cut, :] = jnp.dot(
            p.astype(jnp.bfloat16), g[cut], preferred_element_type=jnp.float32
        )
    dots = dots + jnp.concatenate(own_dots, axis=1)

    def behind(i, carry):
        rows = pl.ds(pl.multiple_of(i * KB, KB), KB)
        ds = (p_s[rows, :] * (dp_s[rows, :] - dots)).astype(jnp.bfloat16)
        ds_s[rows, :] = ds
        dk_s[rows, :] += jnp.dot(ds, q, preferred_element_type=jnp.float32)
        return carry

    lax.fori_loop(0, nkb, behind, 0)
    total = jnp.dot(kt_s[...], ds_s[...], preferred_element_type=jnp.float32)
    for t in range(TQ // 128):
        cut = slice(t * 128, (t + 1) * 128)
        p, dp = own[t]
        ds = (p * (dp - dots[:, cut])).astype(jnp.bfloat16)
        dko_ref[cut, :] = scale * jnp.dot(ds, q[cut], preferred_element_type=jnp.float32)
        kt = ko_ref[cut, :].astype(jnp.float32).T.astype(jnp.bfloat16)
        part = total[:, cut] + jnp.dot(kt, ds, preferred_element_type=jnp.float32)
        out = (scale * part).T.astype(jnp.bfloat16)
        gq_ref[cut, :] = out
        gqf_ref[cut, :] = out

    @pl.when(step == tiles - 1)
    def _():
        back_ref[:, 0] = (scale * dk_s[...]).astype(jnp.bfloat16).reshape(back_ref[:, 0].shape)
        back_ref[:, 1] = dv_s[...].astype(jnp.bfloat16).reshape(back_ref[:, 1].shape)


def land_kernel(me_ref, tab_ref, back_ref, dko_ref, dvo_ref, *rest, head, spans):
    gk_ref, gv_ref = rest[-2:]
    gk_ref[...] = dko_ref[...]
    gv_ref[...] = dvo_ref[...]
    me = me_ref[0]

    def one(n, carry):
        for c in range(CAP):
            at = head * spans + n

            @pl.when(tab_ref[2 + c, at] > 0)
            def _(c=c, at=at):
                rows = pl.ds(pl.multiple_of(tab_ref[c, at] * KEY_BLOCK, KEY_BLOCK), KEY_BLOCK)
                gk_ref[rows, :] += back_ref[n, 0, c].astype(jnp.float32)
                gv_ref[rows, :] += back_ref[n, 1, c].astype(jnp.float32)

        return carry

    lax.fori_loop(me + 1, spans, one, 0)


def pack(me, chosen, key_rows, value_rows, heads, spans, blocks):
    picks = chosen.shape[2]
    rows = key_rows.shape[0]
    shape = (spans, 2, CAP, KEY_BLOCK, HEAD_DIM)
    vmem = pl.BlockSpec(memory_space=pltpu.VMEM)
    return pl.pallas_call(
        functools.partial(pack_kernel, heads=heads, spans=spans, blocks=blocks, picks=picks),
        out_shape=[jax.ShapeDtypeStruct(shape, jnp.bfloat16)] * heads
        + [
            jax.ShapeDtypeStruct((8, 128), jnp.int32),
            jax.ShapeDtypeStruct((heads, spans * CAP, rows), jnp.float32),
        ],
        in_specs=[pl.BlockSpec(memory_space=pltpu.SMEM), vmem, vmem, vmem],
        out_specs=[vmem] * (heads + 2),
        scratch_shapes=[
            pltpu.VMEM((128, 128), jnp.int32),
            pltpu.VMEM((128, 128), jnp.int32),
            pltpu.VMEM((8, 128), jnp.int32),
            pltpu.SMEM((8, 128), jnp.int32),
            pltpu.SemaphoreType.DMA,
        ],
        compiler_params=pltpu.CompilerParams(vmem_limit_bytes=40 * 1024 * 1024),
        name="pack",
    )(
        me,
        chosen,
        key_rows.reshape(blocks, KEY_BLOCK, -1),
        value_rows.reshape(blocks, KEY_BLOCK, -1),
    )


def attend(head, q, g, k, v, lse, bias, far_kv, gq_full):
    rows, width = q.shape
    heads = lse.shape[0]
    tiles = rows // TQ
    spans = far_kv.shape[0]
    far = spans * CAP * KEY_BLOCK
    first = gq_full is None
    column = pl.BlockSpec((TQ, HEAD_DIM), lambda i: (i, head))
    alone = pl.BlockSpec((TQ, HEAD_DIM), lambda i: (i, 0))
    whole = pl.BlockSpec(far_kv.shape, lambda i: (0, 0, 0, 0, 0))
    in_specs = [
        column,
        column,
        column,
        column,
        pl.BlockSpec((heads, TQ), lambda i: (0, i)),
        pl.BlockSpec((None, spans * CAP, TQ), lambda i: (head, 0, i)),
        whole,
    ]
    args = [q, g, k, v, lse, bias, far_kv]
    aliases = {}
    if not first:
        in_specs.append(pl.BlockSpec(memory_space=pl.ANY))
        args.append(gq_full)
        aliases = {7: 0}
    flops = 10 * rows * far * HEAD_DIM
    return pl.pallas_call(
        functools.partial(attend_kernel, head=head, first=first, tiles=tiles, far=far),
        grid=(tiles,),
        in_specs=in_specs,
        out_specs=[column, alone, alone, alone, whole],
        out_shape=[
            jax.ShapeDtypeStruct((rows, width), jnp.bfloat16),
            jax.ShapeDtypeStruct((rows, HEAD_DIM), jnp.bfloat16),
            jax.ShapeDtypeStruct((rows, HEAD_DIM), jnp.float32),
            jax.ShapeDtypeStruct((rows, HEAD_DIM), jnp.float32),
            jax.ShapeDtypeStruct(far_kv.shape, jnp.bfloat16),
        ],
        scratch_shapes=[
            pltpu.VMEM((far, TQ), jnp.float32),
            pltpu.VMEM((far, TQ), jnp.float32),
            pltpu.VMEM((far, TQ), jnp.bfloat16),
            pltpu.VMEM((far, HEAD_DIM), jnp.float32),
            pltpu.VMEM((far, HEAD_DIM), jnp.float32),
            pltpu.VMEM((HEAD_DIM, far), jnp.bfloat16),
        ],
        input_output_aliases=aliases,
        cost_estimate=pl.CostEstimate(
            flops=flops, transcendentals=rows * far, bytes_accessed=8 * 1024 * 1024
        ),
        compiler_params=pltpu.CompilerParams(
            dimension_semantics=("arbitrary",), vmem_limit_bytes=40 * 1024 * 1024
        ),
        name=f"attend{head}",
    )(*args)


def land(head, me, tab, home, dko, dvo, full, rows, width):
    spans = home.shape[0]
    smem = pl.BlockSpec(memory_space=pltpu.SMEM)
    column = pl.BlockSpec((rows, HEAD_DIM), lambda i: (0, head))
    alone = pl.BlockSpec((rows, HEAD_DIM), lambda i: (0, 0))
    in_specs = [smem, smem, pl.BlockSpec(home.shape, lambda i: (0, 0, 0, 0, 0)), alone, alone]
    args = [me, tab, home, dko, dvo]
    aliases = {}
    if full is not None:
        in_specs += [pl.BlockSpec(memory_space=pl.ANY)] * 2
        args += list(full)
        aliases = {5: 0, 6: 1}
    return pl.pallas_call(
        functools.partial(land_kernel, head=head, spans=spans),
        grid=(1,),
        in_specs=in_specs,
        out_specs=[column, column],
        out_shape=[jax.ShapeDtypeStruct((rows, width), jnp.float32)] * 2,
        input_output_aliases=aliases,
        compiler_params=pltpu.CompilerParams(vmem_limit_bytes=40 * 1024 * 1024),
        name=f"land{head}",
    )(*args)


def exchange(x):
    return lax.all_to_all(x, "kv", split_axis=0, concat_axis=0, tiled=True)


def local(query_rows, key_rows, value_rows, log_sums, cotangent, layer_input, chosen):
    spans = lax.axis_size("kv")
    heads = log_sums.shape[0]
    rows, width = query_rows.shape
    blocks = rows // KEY_BLOCK
    me = lax.axis_index("kv").astype(jnp.int32).reshape(1)
    packed = pack(me, chosen, key_rows, value_rows, heads, spans, blocks)
    sends, tab, bias = packed[:heads], packed[heads], packed[heads + 1]
    fars = [exchange(s) for s in sends]
    gq_full = None
    full = None
    weights = []
    for h in range(heads):
        gq_full, gq, dko, dvo, back = attend(
            h, query_rows, cotangent, key_rows, value_rows, log_sums, bias, fars[h], gq_full
        )
        home = exchange(back)
        everyone = lax.all_gather(gq, "tp", axis=0)
        part = lax.dot_general(
            layer_input,
            everyone,
            (((0,), (1,)), ((), ())),
            preferred_element_type=jnp.float32,
        ).astype(jnp.bfloat16)
        mine = exchange(part.reshape(spans, -1, part.shape[1] * HEAD_DIM))
        weights.append(mine.astype(jnp.float32).sum(axis=0))
        full = land(h, me, tab, home, dko, dvo, full, rows, width)
    tp = lax.axis_size("tp")
    stacked = jnp.stack([w.reshape(-1, tp, HEAD_DIM) for w in weights], axis=2)
    grad_weight = stacked.reshape(stacked.shape[0], -1)
    return gq_full, full[0], full[1], grad_weight


def solution(mesh):
    placed = (
        P("kv", "tp"),
        P("kv", "tp"),
        P("kv", "tp"),
        P("tp", "kv"),
        P("kv", "tp"),
        P("kv", "tp"),
        P("tp", None, None),
    )
    return jax.shard_map(
        local,
        mesh=mesh,
        in_specs=placed,
        out_specs=(P("kv", "tp"), P("kv", "tp"), P("kv", "tp"), P(("tp", "kv"), None)),
        check_vma=False,
    )
```

time: 481 us -> 309 us (0.64)
  matrix products: 261 us -> 18.5 us
  Pallas kernels: 0 us -> 89.2 us
  blocking collectives: 0 us -> 88.9 us
  local copies, waits for them, and re-layouts: 88.4 us -> 44.8 us
  other arithmetic: 34.9 us -> 4.33 us
  starting transfers between devices: 51.4 us -> 25.6 us
    dot_general x47 -> x3, matrix products: 261 us -> 18.5 us  [local(): lax.dot_general(layer_input, everyone, (((0,), (1,)), ((), ())), preferre...]
    pallas_call x0 -> x7, Pallas kernels: none -> 89.2 us  [the longest x3 75.9 us: attend(): pl.pallas_call(functools.partial(attend_kernel, head=head, first=first, t...]
    all_to_all x0 -> x4, blocking collectives: none -> 88.9 us  [exchange(): return lax.all_to_all(x, 'kv', split_axis=0, concat_axis=0, tiled=True)]
    all_to_all x7 -> x5, starting transfers between devices: 51.4 us -> 25.5 us  [exchange(): return lax.all_to_all(x, 'kv', split_axis=0, concat_axis=0, tiled=True)]
    gather x4 -> x0, local copies, waits for them, and re-layouts: 19.2 us -> none  [local(): jnp.take_along_axis(rank_in, safe_ids.reshape(local_heads, -1), axis=1)]
    unnamed x117 -> x75, local copies, waits for them, and re-layouts: 11.6 us -> 29.9 us
    reduce_or x2 -> x0, other arithmetic: 16.3 us -> none  [the longest x1 13 us: local(): wanted = jnp.any(everyone[:, :, :, :, None] == own_ids, axis=(2, 3))]
    transpose x5 -> x0, local copies, waits for them, and re-layouts: 13.9 us -> none  [the longest x1 3.99 us: local(): jnp.moveaxis(key_four, 2, 0)]
  transfers between devices with their start and end apart: 8 -> 8, of which waited for: 2 -> 4; matrix products, arithmetic and copies ran while one was open for 62% -> 12% of each run, Pallas kernels for 0% -> 20%
where the time goes in v1:
time: 309 us; the launch traced here: 307 us
  Pallas kernels  89.2 us (29%)
  blocking collectives  88.9 us (29%)
  local copies, waits for them, and re-layouts  44.8 us (14%)
  starting transfers between devices  25.6 us (8%)
  waiting for transfers between devices  21.3 us (7%)
  matrix products  18.5 us (6%)
  between operations  14 us (5%)
  other arithmetic  4.33 us (1%)
    all_to_all x4, blocking collectives, exchange(): return lax.all_to_all(x, 'kv', split_axis=0, concat_axis=0, tiled=True)  88.9 us
    pallas_call x3, Pallas kernels, attend(): pl.pallas_call(functools.partial(attend_kernel, head=head, first=first, t...  75.9 us
    unnamed x75, local copies, waits for them, and re-layouts  29.9 us
    all_to_all x5, starting transfers between devices, exchange(): return lax.all_to_all(x, 'kv', split_axis=0, concat_axis=0, tiled=True)  25.5 us
    all_to_all x5, waiting for transfers between devices, exchange(): return lax.all_to_all(x, 'kv', split_axis=0, concat_axis=0, tiled=True)  21.2 us
    dot_general x3, matrix products, local(): lax.dot_general(layer_input, everyone, (((0,), (1,)), ((), ())), preferre...  18.5 us
    pallas_call x3, Pallas kernels, land(): pl.pallas_call(functools.partial(land_kernel, head=head, spans=spans), gr...  9.32 us
    convert_element_type x3, local copies, waits for them, and re-layouts, local(): part = lax.dot_general(layer_input, everyone, (((0,), (1,)), ((), ())), p...  7.16 us
  transfers between devices with their start and end apart: 8, of which 4 were waited for; matrix products, arithmetic and copies ran while one was open for 12% of the time, Pallas kernels for 20%

profile of v1, /device:TPU:0, one launch (start us, length us, event | category | flops | bytes accessed | tf_op | source)
XLA Modules:
  0.0 306.7 jit_solution(17303173035345238911)
XLA Ops:
  7.2 1.9 copy.21.chosen_ref
  9.2 1.4 copy-done
  10.6 1.4 copy-done.3
  12.0 3.9 %pack.1 = (bf16[32,2,2,32,128]{4,3,2,1,0:T(8,128)(2,1)S(1)}, bf16[32,2,2,32,128]{4,3,2,1,0:T(8,128)(2,1)S(1)}, bf16[32,2,2,32,128]{4,3,2,1,0:T(8,128)(2,1)S(1)}, s32[8,128]{1,0:T(8,128)S(1)}, f32[3,64,2048]{2,1,0:T(8,128)S(1)}) custom-call(s32[1]{0:T(128)} %bitcast.me_ref, s32[3,2048,12]{2,1,0:T(8,128)S(1)} %copy.21.chosen_ref, ...), custom_call_target="tpu_custom_call" | custom-call | tf_op jit(solution)/shard_map/pack/pallas_call | solution.py:209
  16.9 25.7 %all_to_all.45.refs_6_ = bf16[32,2,2,32,128]{4,3,2,1,0:T(8,128)(2,1)S(1)} all-to-all(bf16[32,2,2,32,128]{4,3,2,1,0:T(8,128)(2,1)S(1)} %get-tuple-element.33), channel_id=1, replica_groups=mesh['kv'=32,'tp'=4] {'kv'}, dimensions={0} | all-to-all | bytes 2097152 | tf_op jit(solution)/shard_map/all_to_all | solution.py:317
  42.6 25.2 %attend0.1 = (bf16[2048,384]{1,0:T(8,128)(2,1)}, bf16[2048,128]{1,0:T(8,128)(2,1)S(1)}, f32[2048,128]{1,0:T(8,128)S(1)}, f32[2048,128]{1,0:T(8,128)S(1)}, bf16[32,2,2,32,128]{4,3,2,1,0:T(8,128)(2,1)S(1)}) custom-call(bf16[2048,384]{1,0:T(8,128)(2,1)S(1)} %copy-done.27, bf16[2048,384]{1,0:T(8,128)(2,1)S(1)} %copy-done.30, bf16[2048,384]{1,0:T(8,128)(2,1)S(1)} %copy-done.1, ...), custom_call_target="tpu_custom_call" | custom-call | flops 5368709120 | bytes 8388608 | tf_op jit(solution)/shard_map/attend0/pallas_call | solution.py:261
  67.9 1.0 copy-done.16
  69.8 1.0 copy-done.22
  71.8 21.3 %all_to_all.46.refs_6_ = bf16[32,2,2,32,128]{4,3,2,1,0:T(8,128)(2,1)S(1)} all-to-all(bf16[32,2,2,32,128]{4,3,2,1,0:T(8,128)(2,1)} %copy-done.19), channel_id=1, replica_groups=mesh['kv'=32,'tp'=4] {'kv'}, dimensions={0} | all-to-all | bytes 2097152 | tf_op jit(solution)/shard_map/all_to_all | solution.py:317
  93.0 1.4 copy-done.28
  94.4 1.4 copy-done.31
  95.8 1.4 copy-done.34
  97.3 25.6 %attend1.1 = (bf16[2048,384]{1,0:T(8,128)(2,1)}, bf16[2048,128]{1,0:T(8,128)(2,1)S(1)}, f32[2048,128]{1,0:T(8,128)S(1)}, f32[2048,128]{1,0:T(8,128)S(1)}, bf16[32,2,2,32,128]{4,3,2,1,0:T(8,128)(2,1)}) custom-call(bf16[2048,384]{1,0:T(8,128)(2,1)S(1)} %copy-done.28, bf16[2048,384]{1,0:T(8,128)(2,1)S(1)} %copy-done.31, ...), custom_call_target="tpu_custom_call", output_to_operand_aliasing={{0}: (7, {})} | custom-call | flops 5368709120 | bytes 8388608 | tf_op jit(solution)/shard_map/attend1/pallas_call | solution.py:261
  125.6 21.3 %all_to_all.47.refs_6_ = bf16[32,2,2,32,128]{4,3,2,1,0:T(8,128)(2,1)S(1)} all-to-all(bf16[32,2,2,32,128]{4,3,2,1,0:T(8,128)(2,1)} %copy-done.15), channel_id=1, replica_groups=mesh['kv'=32,'tp'=4] {'kv'}, dimensions={0} | all-to-all | bytes 2097152 | tf_op jit(solution)/shard_map/all_to_all | solution.py:317
  146.8 20.6 %all_to_all.48.back_ref = bf16[32,2,2,32,128]{4,3,2,1,0:T(8,128)(2,1)S(1)} all-to-all(bf16[32,2,2,32,128]{4,3,2,1,0:T(8,128)(2,1)S(1)} %copy-done.17), channel_id=1, replica_groups=mesh['kv'=32,'tp'=4] {'kv'}, dimensions={0} | all-to-all | bytes 2097152 | tf_op jit(solution)/shard_map/all_to_all | solution.py:317
  167.4 3.9 %all-to-all-start.4 = ((bf16[32,2,2,32,128]{4,3,2,1,0:T(8,128)(2,1)}), bf16[32,2,2,32,128]{4,3,2,1,0:T(8,128)(2,1)S(1)}, u32[]{:S(2)}, u32[]{:S(2)}) async-start(bf16[32,2,2,32,128]{4,3,2,1,0:T(8,128)(2,1)} %get-tuple-element.41), calls=%async_computation.4 | async-start | bytes 2097152 | tf_op jit(solution)/shard_map/all_to_all | solution.py:317
  171.4 1.4 copy-done.2
  172.8 1.4 copy-done.6
  174.3 1.4 copy-done.29
  175.7 1.4 copy-done.32
  177.1 1.4 copy-done.35
  178.5 25.2 %attend2.1 = (bf16[2048,384]{1,0:T(8,128)(2,1)}, bf16[2048,128]{1,0:T(8,128)(2,1)S(1)}, f32[2048,128]{1,0:T(8,128)S(1)}, f32[2048,128]{1,0:T(8,128)S(1)}, bf16[32,2,2,32,128]{4,3,2,1,0:T(8,128)(2,1)S(1)}) custom-call(bf16[2048,384]{1,0:T(8,128)(2,1)S(1)} %copy-done.29, bf16[2048,384]{1,0:T(8,128)(2,1)S(1)} %copy-done.32, ...), custom_call_target="tpu_custom_call", output_to_operand_aliasing={{0}: (7, {})} | custom-call | flops 5368709120 | bytes 8388608 | tf_op jit(solution)/shard_map/attend2/pallas_call | solution.py:261
  204.6 1.0 copy-done.13
  207.5 7.6 %all-to-all-start.3 = ((bf16[32,2,2,32,128]{4,3,2,1,0:T(8,128)(2,1)}), bf16[32,2,2,32,128]{4,3,2,1,0:T(8,128)(2,1)S(1)}, u32[]{:S(2)}, u32[]{:S(2)}) async-start(bf16[32,2,2,32,128]{4,3,2,1,0:T(8,128)(2,1)} %copy-done.18), calls=%async_computation.3 | async-start | bytes 2097152 | tf_op jit(solution)/shard_map/all_to_all | solution.py:317
  215.1 6.2 %fusion.21 = bf16[1024,4,128]{0,2,1:T(8,128)(2,1)} fusion(bf16[4,2048,128]{2,1,0:T(8,128)(2,1)} %bitcast.36, bf16[2048,1024]{1,0:T(8,128)(2,1)} %param.12), kind=kOutput, calls=%fused_computation.14 | convolution fusion | flops 2148007936 | bytes 7340032 | tf_op jit(solution)/shard_map/dot_general | solution.py:338
  221.3 2.4 copy.23
  223.7 2.2 reshape.32
  225.9 6.2 %all-to-all-done.3.back_ref = bf16[32,2,2,32,128]{4,3,2,1,0:T(8,128)(2,1)S(1)} async-done(((bf16[32,2,2,32,128]{4,3,2,1,0:T(8,128)(2,1)}), bf16[32,2,2,32,128]{4,3,2,1,0:T(8,128)(2,1)S(1)}, u32[]{:S(2)}, u32[]{:S(2)}) %all-to-all-start.3) | async-done | bytes 1048608 | tf_op jit(solution)/shard_map/all_to_all | solution.py:317
  232.1 4.7 %all-to-all-start.6 = ((bf16[32,32,512]{2,1,0:T(8,128)(2,1)}), bf16[32,32,512]{2,1,0:T(8,128)(2,1)}, u32[]{:S(2)}, u32[]{:S(2)}) async-start(bf16[32,32,512]{2,1,0:T(8,128)(2,1)} %reshape.32), calls=%async_computation.6 | async-start | bytes 2097152 | tf_op jit(solution)/shard_map/all_to_all | solution.py:317
  236.8 6.1 %fusion.18 = bf16[1024,4,128]{0,2,1:T(8,128)(2,1)} fusion(bf16[4,2048,128]{2,1,0:T(8,128)(2,1)} %bitcast.37, bf16[2048,1024]{1,0:T(8,128)(2,1)} %param.12), kind=kOutput, calls=%fused_computation.13 | convolution fusion | flops 2148007936 | bytes 7340032 | tf_op jit(solution)/shard_map/dot_general | solution.py:338
  243.0 2.4 copy.25
  245.3 2.3 reshape.33
  247.6 6.4 %all-to-all-done.6 = bf16[32,32,512]{2,1,0:T(8,128)(2,1)} async-done(((bf16[32,32,512]{2,1,0:T(8,128)(2,1)}), bf16[32,32,512]{2,1,0:T(8,128)(2,1)}, u32[]{:S(2)}, u32[]{:S(2)}) %all-to-all-start.6) | async-done | bytes 1048608 | tf_op jit(solution)/shard_map/all_to_all | solution.py:317
  254.0 4.7 %all-to-all-start.7 = ((bf16[32,32,512]{2,1,0:T(8,128)(2,1)}), bf16[32,32,512]{2,1,0:T(8,128)(2,1)}, u32[]{:S(2)}, u32[]{:S(2)}) async-start(bf16[32,32,512]{2,1,0:T(8,128)(2,1)} %reshape.33), calls=%async_computation.7 | async-start | bytes 2097152 | tf_op jit(solution)/shard_map/all_to_all | solution.py:317
  258.7 6.1 %fusion.15 = bf16[1024,4,128]{0,2,1:T(8,128)(2,1)} fusion(bf16[4,2048,128]{2,1,0:T(8,128)(2,1)} %bitcast.38, bf16[2048,1024]{1,0:T(8,128)(2,1)} %param.12), kind=kOutput, calls=%fused_computation.12 | convolution fusion | flops 2148007936 | bytes 7340032 | tf_op jit(solution)/shard_map/dot_general | solution.py:338
  264.8 2.4 copy.27
  267.2 2.2 reshape.34
  269.4 6.4 %all-to-all-done.7 = bf16[32,32,512]{2,1,0:T(8,128)(2,1)} async-done(((bf16[32,32,512]{2,1,0:T(8,128)(2,1)}), bf16[32,32,512]{2,1,0:T(8,128)(2,1)}, u32[]{:S(2)}, u32[]{:S(2)}) %all-to-all-start.7) | async-done | bytes 1048608 | tf_op jit(solution)/shard_map/all_to_all | solution.py:317
  275.8 4.7 %all-to-all-start.8 = ((bf16[32,32,512]{2,1,0:T(8,128)(2,1)}), bf16[32,32,512]{2,1,0:T(8,128)(2,1)}, u32[]{:S(2)}, u32[]{:S(2)}) async-start(bf16[32,32,512]{2,1,0:T(8,128)(2,1)} %reshape.34), calls=%async_computation.8 | async-start | bytes 2097152 | tf_op jit(solution)/shard_map/all_to_all | solution.py:317
  280.5 1.4 copy-done.21
  281.9 1.2 copy-done.23
  283.1 3.1 %land0.1 = (f32[2048,384]{1,0:T(8,128)}, f32[2048,384]{1,0:T(8,128)}) custom-call(s32[1]{0:T(128)} %bitcast.me_ref, s32[8,128]{1,0:T(8,128)S(1)} %get-tuple-element.37.tab_ref, bf16[32,2,2,32,128]{4,3,2,1,0:T(8,128)(2,1)S(1)} %all_to_all.48.back_ref, f32[2048,128]{1,0:T(8,128)S(1)} %copy-done.21, f32[2048,128]{1,0:T(8,128)S(1)} %copy-done.23), custom_call_target="tpu_custom_call" | custom-call | tf_op jit(solution)/shard_map/land0/pallas_call | solution.py:304
  286.2 3.1 %land1.1 = (f32[2048,384]{1,0:T(8,128)}, f32[2048,384]{1,0:T(8,128)}) custom-call(s32[1]{0:T(128)} %bitcast.me_ref, s32[8,128]{1,0:T(8,128)S(1)} %get-tuple-element.37.tab_ref, bf16[32,2,2,32,128]{4,3,2,1,0:T(8,128)(2,1)S(1)} %all-to-all-done.4.back_ref, f32[2048,128]{1,0:T(8,128)S(1)} %copy-done.8, ...), custom_call_target="tpu_custom_call", output_to_operand_aliasing={{0}: (5, {}), {1}: (6, {})} | custom-call | tf_op jit(solution)/shard_map/land1/pallas_call | solution.py:304
  289.4 3.1 %land2.1 = (f32[2048,384]{1,0:T(8,128)}, f32[2048,384]{1,0:T(8,128)}) custom-call(s32[1]{0:T(128)} %bitcast.me_ref, s32[8,128]{1,0:T(8,128)S(1)} %get-tuple-element.37.tab_ref, bf16[32,2,2,32,128]{4,3,2,1,0:T(8,128)(2,1)S(1)} %all-to-all-done.3.back_ref, f32[2048,128]{1,0:T(8,128)S(1)} %copy-done.12, ...), custom_call_target="tpu_custom_call", output_to_operand_aliasing={{0}: (5, {}), {1}: (6, {})} | custom-call | tf_op jit(solution)/shard_map/land2/pallas_call | solution.py:304
  292.5 1.4 convert_reduce_fusion.2
  293.9 1.4 convert_reduce_fusion.1
  295.4 2.3 all-to-all-done.8
  297.7 1.4 convert_reduce_fusion
  (74 shorter events, 9.7 us)
Async XLA Ops:
  7.2 207.9 %all-gather.7.cloned.1.call-start = ((), (), s32[]{:S(2)}) async-start(), calls=%async_computation.9 | async-start | bytes 2621440 | tf_op jit(solution)/shard_map/all_gather | solution.py:337
  9.2 1.4 copy-start
  10.6 1.4 copy-start.3
  12.0 30.6 %copy-start.4 = (bf16[2048,384]{1,0:T(8,128)(2,1)S(1)}, bf16[2048,384]{1,0:T(8,128)(2,1)}, u32[]{:S(2)}) copy-start(bf16[2048,384]{1,0:T(8,128)(2,1)} %refs_3_.5) | copy-start | bytes 4718596
  12.0 30.6 %copy-start.27 = (bf16[2048,384]{1,0:T(8,128)(2,1)S(1)}, bf16[2048,384]{1,0:T(8,128)(2,1)}, u32[]{:S(2)}) copy-start(bf16[2048,384]{1,0:T(8,128)(2,1)} %refs_0_.5) | copy-start | bytes 4718596
  12.0 30.6 %copy-start.30 = (bf16[2048,384]{1,0:T(8,128)(2,1)S(1)}, bf16[2048,384]{1,0:T(8,128)(2,1)}, u32[]{:S(2)}) copy-start(bf16[2048,384]{1,0:T(8,128)(2,1)} %refs_1_.5) | copy-start | bytes 4718596
  15.9 1.0 copy-start.15
  16.9 25.7 %copy-start.19 = (bf16[32,2,2,32,128]{4,3,2,1,0:T(8,128)(2,1)}, bf16[32,2,2,32,128]{4,3,2,1,0:T(8,128)(2,1)S(1)}, u32[]{:S(2)}) copy-start(bf16[32,2,2,32,128]{4,3,2,1,0:T(8,128)(2,1)S(1)} %get-tuple-element.32) | copy-start | bytes 3145732
  16.9 51.0 %copy-start.33 = (f32[3,64,2048]{2,1,0:T(8,128)}, f32[3,64,2048]{2,1,0:T(8,128)S(1)}, u32[]{:S(2)}) copy-start(f32[3,64,2048]{2,1,0:T(8,128)S(1)} %get-tuple-element.30.refs_5_) | copy-start | bytes 4718596
  16.9 25.7 %copy-start.1 = (bf16[2048,384]{1,0:T(8,128)(2,1)S(1)}, bf16[2048,384]{1,0:T(8,128)(2,1)}, u32[]{:S(2)}) copy-start(bf16[2048,384]{1,0:T(8,128)(2,1)} %refs_2_.5) | copy-start | bytes 4718596
  16.9 25.8 %copy-start.36 = (f32[3,2048]{1,0:T(4,128)S(1)}, f32[3,2048]{1,0:T(4,128)}, u32[]{:S(2)}) copy-start(f32[3,2048]{1,0:T(4,128)} %refs_4_.5) | copy-start | bytes 73732
  67.9 1.0 copy-start.16
  68.9 1.0 copy-start.20
  69.8 1.0 copy-start.22
  70.9 0.8 copy-start.25
  71.7 21.4 %copy-start.5 = (bf16[2048,384]{1,0:T(8,128)(2,1)S(1)}, bf16[2048,384]{1,0:T(8,128)(2,1)}, u32[]{:S(2)}) copy-start(bf16[2048,384]{1,0:T(8,128)(2,1)} %refs_3_.5) | copy-start | bytes 4718596
  71.7 165.1 %all-gather.9.cloned.1.call-start = ((), (), s32[]{:S(2)}) async-start(), calls=%async_computation.10 | async-start | bytes 2621440 | tf_op jit(solution)/shard_map/all_gather | solution.py:337
  93.0 1.4 copy-start.28
  94.4 1.4 copy-start.31
  95.8 1.4 copy-start.34
  122.8 1.0 copy-start.7
  123.8 1.0 copy-start.9
  124.7 0.8 copy-start.24
  125.5 21.3 %copy-start.17 = (bf16[32,2,2,32,128]{4,3,2,1,0:T(8,128)(2,1)S(1)}, bf16[32,2,2,32,128]{4,3,2,1,0:T(8,128)(2,1)}, u32[]{:S(2)}) copy-start(bf16[32,2,2,32,128]{4,3,2,1,0:T(8,128)(2,1)} %copy-done.16) | copy-start | bytes 3145732
  167.4 40.0 %all-to-all-start.4 = ((bf16[32,2,2,32,128]{4,3,2,1,0:T(8,128)(2,1)}), bf16[32,2,2,32,128]{4,3,2,1,0:T(8,128)(2,1)S(1)}, u32[]{:S(2)}, u32[]{:S(2)}) async-start(bf16[32,2,2,32,128]{4,3,2,1,0:T(8,128)(2,1)} %get-tuple-element.41), calls=%async_computation.4 | async-start | bytes 2097152 | tf_op jit(solution)/shard_map/all_to_all | solution.py:317
  171.4 87.3 %all-gather.11.cloned.1.call-start = ((), (), s32[]{:S(2)}) async-start(), calls=%async_computation.11 | async-start | bytes 2621440 | tf_op jit(solution)/shard_map/all_gather | solution.py:337
  171.4 1.4 copy-start.2
  172.8 1.4 copy-start.6
  174.3 1.4 copy-start.29
  175.7 1.4 copy-start.32
  177.1 1.4 copy-start.35
  203.7 1.0 copy-start.11
  204.6 1.0 copy-start.13
  205.7 1.0 copy-start.18
  206.6 0.8 copy-start.26
  207.5 24.6 %all-to-all-start.3 = ((bf16[32,2,2,32,128]{4,3,2,1,0:T(8,128)(2,1)}), bf16[32,2,2,32,128]{4,3,2,1,0:T(8,128)(2,1)S(1)}, u32[]{:S(2)}, u32[]{:S(2)}) async-start(bf16[32,2,2,32,128]{4,3,2,1,0:T(8,128)(2,1)} %copy-done.18), calls=%async_computation.3 | async-start | bytes 2097152 | tf_op jit(solution)/shard_map/all_to_all | solution.py:317
  232.1 21.9 %all-to-all-start.6 = ((bf16[32,32,512]{2,1,0:T(8,128)(2,1)}), bf16[32,32,512]{2,1,0:T(8,128)(2,1)}, u32[]{:S(2)}, u32[]{:S(2)}) async-start(bf16[32,32,512]{2,1,0:T(8,128)(2,1)} %reshape.32), calls=%async_computation.6 | async-start | bytes 2097152 | tf_op jit(solution)/shard_map/all_to_all | solution.py:317
  254.0 21.9 %all-to-all-start.7 = ((bf16[32,32,512]{2,1,0:T(8,128)(2,1)}), bf16[32,32,512]{2,1,0:T(8,128)(2,1)}, u32[]{:S(2)}, u32[]{:S(2)}) async-start(bf16[32,32,512]{2,1,0:T(8,128)(2,1)} %reshape.33), calls=%async_computation.7 | async-start | bytes 2097152 | tf_op jit(solution)/shard_map/all_to_all | solution.py:317
  275.8 21.9 %all-to-all-start.8 = ((bf16[32,32,512]{2,1,0:T(8,128)(2,1)}), bf16[32,32,512]{2,1,0:T(8,128)(2,1)}, u32[]{:S(2)}, u32[]{:S(2)}) async-start(bf16[32,32,512]{2,1,0:T(8,128)(2,1)} %reshape.34), calls=%async_computation.8 | async-start | bytes 2097152 | tf_op jit(solution)/shard_map/all_to_all | solution.py:317
  280.5 5.7 %copy-start.8 = (f32[2048,128]{1,0:T(8,128)S(1)}, f32[2048,128]{1,0:T(8,128)}, u32[]{:S(2)}) copy-start(f32[2048,128]{1,0:T(8,128)} %copy-done.7) | copy-start | bytes 3145732
  280.5 5.7 %copy-start.10 = (f32[2048,128]{1,0:T(8,128)S(1)}, f32[2048,128]{1,0:T(8,128)}, u32[]{:S(2)}) copy-start(f32[2048,128]{1,0:T(8,128)} %copy-done.9) | copy-start | bytes 3145732
  280.5 1.4 copy-start.21
  281.9 1.2 copy-start.23
  286.2 3.1 %copy-start.12 = (f32[2048,128]{1,0:T(8,128)S(1)}, f32[2048,128]{1,0:T(8,128)}, u32[]{:S(2)}) copy-start(f32[2048,128]{1,0:T(8,128)} %copy-done.11) | copy-start | bytes 3145732
  286.2 3.1 %copy-start.14 = (f32[2048,128]{1,0:T(8,128)S(1)}, f32[2048,128]{1,0:T(8,128)}, u32[]{:S(2)}) copy-start(f32[2048,128]{1,0:T(8,128)} %copy-done.13) | copy-start | bytes 3145732
Sparse Core Ops, SparseCore 0:
  71.8 28.4 all-gather.6
  125.7 28.4 all-gather.8
  207.6 32.1 all-gather.10

commit v2 on v1

v2 whole, which is shorter than its diff:
```python
import functools

import jax
import jax.numpy as jnp
from jax import lax
from jax.experimental import pallas as pl
from jax.experimental.pallas import tpu as pltpu
from jax.sharding import PartitionSpec as P


HEAD_DIM = 128
KEY_BLOCK = 32
CAP = 2
BIG = 1 << 20
LOG2E = 1.4426950408889634
NEG = -1.0e30
TQ = 512
KB = 256


def spread(column):
    wide = jnp.broadcast_to(column.astype(jnp.float32), (column.shape[0], 128))
    wide = jnp.concatenate([wide, jnp.zeros((128 - column.shape[0], 128), jnp.float32)], axis=0)
    return wide.T[0:1, :].astype(jnp.int32)


def copy_blocks(tab_s, k_ref, v_ref, send, h, half, lanes):
    def fill(m, carry):
        for odd in range(2):
            for c in range(CAP):
                b = tab_s[2 * c + odd, h * half + m]
                send[2 * m + odd, c] = k_ref[b, :, lanes]
                send[2 * m + odd, CAP + c] = v_ref[b, :, lanes]
        return carry

    lax.fori_loop(0, half, fill, 0, unroll=2)


def first_kernel(me_ref, chosen_ref, k_ref, v_ref, send, tab_ref, lo_s, hi_s, tab_v, tab_s, sem,
                 *, heads, spans, blocks):
    me = me_ref[0]
    half = spans // 2
    for h in range(heads):
        ids = chosen_ref[h]
        mine = (ids >> 6) == me
        lo = jnp.min(jnp.where(mine, ids, BIG), axis=0, keepdims=True)
        hi = jnp.max(jnp.where(mine, ids, -1), axis=0, keepdims=True)
        for m in range(half):
            lo_s[h * half + m : h * half + m + 1, :] = lo[:, m * 128 : (m + 1) * 128]
            hi_s[h * half + m : h * half + m + 1, :] = hi[:, m * 128 : (m + 1) * 128]
    lane = lax.broadcasted_iota(jnp.int32, (heads * half, 128), 1)
    tab_v[...] = jnp.zeros((8, 128), jnp.int32)
    for odd in range(2):
        ours = (lane // blocks) == odd
        lo = spread(jnp.min(jnp.where(ours, lo_s[...], BIG), axis=1, keepdims=True))
        hi = spread(jnp.max(jnp.where(ours, hi_s[...], -1), axis=1, keepdims=True))
        tab_v[odd : odd + 1, :] = lo & (blocks - 1)
        tab_v[2 + odd : 3 + odd, :] = jnp.maximum(hi, 0) & (blocks - 1)
        tab_v[4 + odd : 5 + odd, :] = (hi >= 0).astype(jnp.int32)
        tab_v[6 + odd : 7 + odd, :] = (hi > lo).astype(jnp.int32)
    tab_ref[...] = tab_v[...]
    copy = pltpu.make_async_copy(tab_v, tab_s, sem)
    copy.start()
    copy.wait()
    copy_blocks(tab_s, k_ref, v_ref, send, 0, half, slice(0, HEAD_DIM))


def pack_kernel(tab_ref, k_ref, v_ref, *sends, spans):
    for n, send in enumerate(sends):
        h = n + 1
        lanes = slice(h * HEAD_DIM, (h + 1) * HEAD_DIM)
        copy_blocks(tab_ref, k_ref, v_ref, send, h, spans // 2, lanes)


def mask_kernel(me_ref, chosen_ref, bias_ref, *, heads, spans, blocks, picks):
    me = me_ref[0]
    slots = spans * CAP
    slot = lax.broadcasted_iota(jnp.int32, (slots, 128), 0)
    lane = lax.broadcasted_iota(jnp.int32, (slots, 128), 1)
    ours = (lane // blocks) == (me % 2)
    place = lax.broadcasted_iota(jnp.int32, (128, blocks * KEY_BLOCK), 1) // KEY_BLOCK
    row = lax.broadcasted_iota(jnp.int32, (128, blocks * KEY_BLOCK), 0)
    expand = ((place + (me % 2) * blocks) == row).astype(jnp.bfloat16)
    start = pl.multiple_of((me // 2) * 128, 128)
    for h in range(heads):
        ids = chosen_ref[h, :, pl.ds(start, 128)]
        cols = [jnp.broadcast_to(ids[c : c + 1, :], (slots, 128)) for c in range(picks)]
        least = jnp.full((slots, 128), BIG, jnp.int32)
        most = jnp.full((slots, 128), -1, jnp.int32)
        for col in cols:
            hit = ((col >> 6) == (slot >> 1)) & ours
            least = jnp.minimum(least, jnp.where(hit, col, BIG))
            most = jnp.maximum(most, jnp.where(hit, col, -1))
        least = jnp.min(least, axis=1, keepdims=True)
        most = jnp.max(most, axis=1, keepdims=True)
        name = jnp.where(
            (slot & 1) == 0, least, jnp.where(most > least, most, -7)
        )
        named = cols[0] == name
        for col in cols[1:]:
            named = named | (col == name)
        hot = jnp.where(named, 1.0, 0.0).astype(jnp.bfloat16)
        full = jnp.dot(hot, expand, preferred_element_type=jnp.float32)
        bias_ref[h] = jnp.where(full > 0.5, 0.0, NEG)


def turn_kernel(x_ref, out_ref):
    rows = x_ref.shape[0]
    for i in range(rows // 256):
        cut = slice(i * 256, (i + 1) * 256)
        out_ref[:, cut] = x_ref[cut, :].T


def weight_kernel(xt_ref, *rest, shards):
    out_ref = rest[-1]
    xt = xt_ref[...]
    shape = (out_ref.shape[0],) + out_ref.shape[2:]
    for at in range(0, shards, 2):
        g = jnp.concatenate([rest[at][...], rest[at + 1][...]], axis=1)
        got = jnp.dot(xt, g, preferred_element_type=jnp.float32).astype(jnp.bfloat16)
        out_ref[:, at] = got[:, :HEAD_DIM].reshape(shape)
        out_ref[:, at + 1] = got[:, HEAD_DIM:].reshape(shape)


def total_kernel(at_ref, got_ref, *rest, head, heads, order):
    out_ref = rest[-1]
    if len(rest) > 1:
        out_ref[...] = rest[0][...]
    me = at_ref[0]
    tp = len(order)
    for p in range(tp):
        acc = got_ref[0, p].astype(jnp.float32)
        for i in range(1, got_ref.shape[0]):
            acc = acc + got_ref[i, p].astype(jnp.float32)
        place = (me + order[p]) % tp
        first = pl.multiple_of((place * heads + head) * HEAD_DIM, HEAD_DIM)
        out_ref[:, pl.ds(first, HEAD_DIM)] = acc


def attend_kernel(me_ref, *refs, head, extra, merge, tiles, far):
    q_ref, g_ref, ko_ref, vo_ref, lse_ref, bias_ref, kv_ref = refs[:7]
    ahead_ref = refs[7] if merge else None
    rest = refs[7 + merge + extra :]
    gqf_ref, gq_ref, dko_ref, dvo_ref, back_ref = rest[:5]
    p_s, dp_s, ds_s, dk_s, dv_s, kt_s = rest[5:]
    step = pl.program_id(0)
    scale = HEAD_DIM**-0.5
    nkb = far // KB
    per = KB // (CAP * KEY_BLOCK)

    @pl.when(step == 0)
    def _():
        dk_s[...] = jnp.zeros_like(dk_s)
        dv_s[...] = jnp.zeros_like(dv_s)
        for i in range(nkb):
            keys = kv_ref[i * per : (i + 1) * per, 0:CAP].reshape(KB, HEAD_DIM)
            kt_s[:, i * KB : (i + 1) * KB] = keys.astype(jnp.float32).T.astype(jnp.bfloat16)

    q = q_ref[...]
    g = g_ref[...]
    lse = lse_ref[head : head + 1, :] * LOG2E
    nt = (((1,), (1,)), ((), ()))

    def ahead(i, dots):
        keys = kv_ref[pl.ds(i * per, per), 0:CAP].reshape(KB, HEAD_DIM)
        values = kv_ref[pl.ds(i * per, per), CAP : 2 * CAP].reshape(KB, HEAD_DIM)
        s = lax.dot_general(keys, q, nt, preferred_element_type=jnp.float32)
        dp = lax.dot_general(values, g, nt, preferred_element_type=jnp.float32)
        shift = bias_ref[pl.ds(i * per * CAP, per * CAP), :] - lse
        s = (s * (scale * LOG2E)).reshape(per * CAP, KEY_BLOCK, TQ) + shift[:, None, :]
        p = jnp.exp2(s).reshape(KB, TQ)
        rows = pl.ds(i * KB, KB)
        p_s[rows, :] = p
        dp_s[rows, :] = dp
        dv_s[rows, :] += jnp.dot(
            p.astype(jnp.bfloat16), g, preferred_element_type=jnp.float32
        )
        return dots + (p * dp).reshape(KB // 8, 8, TQ).sum(axis=0)

    dots = jnp.zeros((8, TQ), jnp.float32)
    for i in range(nkb):
        dots = ahead(i, dots)
    dots = jnp.sum(dots, axis=0, keepdims=True)
    key_at = lax.broadcasted_iota(jnp.int32, (128, 128), 0)
    row_at = lax.broadcasted_iota(jnp.int32, (128, 128), 1)
    near = (key_at // KEY_BLOCK == row_at // KEY_BLOCK) & (key_at <= row_at)
    own = []
    own_dots = []
    for t in range(TQ // 128):
        cut = slice(t * 128, (t + 1) * 128)
        s = lax.dot_general(ko_ref[cut, :], q[cut], nt, preferred_element_type=jnp.float32)
        dp = lax.dot_general(vo_ref[cut, :], g[cut], nt, preferred_element_type=jnp.float32)
        p = jnp.exp2(jnp.where(near, s * (scale * LOG2E) - lse[:, cut], NEG))
        own.append((p, dp))
        own_dots.append(jnp.sum(p * dp, axis=0, keepdims=True))
        dvo_ref[cut, :] = jnp.dot(
            p.astype(jnp.bfloat16), g[cut], preferred_element_type=jnp.float32
        )
    dots = dots + jnp.concatenate(own_dots, axis=1)

    def behind(i, carry):
        rows = pl.ds(i * KB, KB)
        ds = (p_s[rows, :] * (dp_s[rows, :] - dots)).astype(jnp.bfloat16)
        ds_s[rows, :] = ds
        dk_s[rows, :] += jnp.dot(ds, q, preferred_element_type=jnp.float32)
        part = jnp.dot(kt_s[:, rows], ds, preferred_element_type=jnp.float32)
        return part if carry is None else carry + part

    total = None
    for i in range(nkb):
        total = behind(i, total)
    for t in range(TQ // 128):
        cut = slice(t * 128, (t + 1) * 128)
        p, dp = own[t]
        ds = (p * (dp - dots[:, cut])).astype(jnp.bfloat16)
        dko_ref[cut, :] = scale * jnp.dot(ds, q[cut], preferred_element_type=jnp.float32)
        kt = ko_ref[cut, :].astype(jnp.float32).T.astype(jnp.bfloat16)
        part = total[:, cut] + jnp.dot(kt, ds, preferred_element_type=jnp.float32)
        out = (scale * part).T.astype(jnp.bfloat16)
        gq_ref[cut, :] = out
        gqf_ref[cut, :] = out

    @pl.when(step == tiles - 1)
    def _():
        shape = (far // (CAP * KEY_BLOCK), CAP, KEY_BLOCK, HEAD_DIM)
        dk = (scale * dk_s[...]).astype(jnp.bfloat16).reshape(shape)
        dv = dv_s[...].astype(jnp.bfloat16).reshape(shape)
        if merge:
            me = me_ref[0]
            for n in range(shape[0]):

                @pl.when(n < me)
                def _(n=n):
                    back_ref[n, 0:CAP] = dk[n]
                    back_ref[n, CAP : 2 * CAP] = dv[n]

                @pl.when(n >= me)
                def _(n=n):
                    back_ref[n] = ahead_ref[n]
        else:
            back_ref[:, 0:CAP] = dk
            back_ref[:, CAP : 2 * CAP] = dv


def land_kernel(me_ref, tab_ref, back_ref, dko_ref, dvo_ref, *rest, head, spans):
    gk_ref, gv_ref = rest[-2:]
    gk_ref[...] = dko_ref[...]
    gv_ref[...] = dvo_ref[...]
    me = me_ref[0]
    half = spans // 2

    def one(n, carry):
        at = head * half + n // 2
        odd = n % 2
        for c in range(CAP):

            @pl.when(tab_ref[4 + 2 * c + odd, at] > 0)
            def _(c=c):
                first = tab_ref[2 * c + odd, at] * KEY_BLOCK
                rows = pl.ds(pl.multiple_of(first, KEY_BLOCK), KEY_BLOCK)
                gk_ref[rows, :] += back_ref[n, c].astype(jnp.float32)
                gv_ref[rows, :] += back_ref[n, CAP + c].astype(jnp.float32)

        return carry

    lax.fori_loop(me + 1, spans, one, 0)


SMEM = pl.BlockSpec(memory_space=pltpu.SMEM)
VMEM = pl.BlockSpec(memory_space=pltpu.VMEM)
ANY = pl.BlockSpec(memory_space=pl.ANY)


def params(**more):
    return pltpu.CompilerParams(vmem_limit_bytes=60 * 1024 * 1024, **more)


def cost(flops, data=1 << 20):
    return pl.CostEstimate(flops=flops, transcendentals=0, bytes_accessed=data)


def five(spans, slots=1):
    return (spans, slots, 2 * CAP, KEY_BLOCK, HEAD_DIM)


def slotted(spans, slot):
    return pl.BlockSpec(
        (spans, None, 2 * CAP, KEY_BLOCK, HEAD_DIM), lambda i: (0, slot, 0, 0, 0)
    )


def pack_first(me, ids, key_blocks, value_blocks, heads, spans):
    blocks = key_blocks.shape[0]
    column = pl.BlockSpec((blocks, KEY_BLOCK, HEAD_DIM), lambda i: (0, 0, 0))
    return pl.pallas_call(
        functools.partial(first_kernel, heads=heads, spans=spans, blocks=blocks),
        grid=(1,),
        out_shape=[
            jax.ShapeDtypeStruct(five(spans), jnp.bfloat16),
            jax.ShapeDtypeStruct((8, 128), jnp.int32),
        ],
        in_specs=[SMEM, VMEM, column, column],
        out_specs=[slotted(spans, 0), VMEM],
        scratch_shapes=[
            pltpu.VMEM((heads * spans // 2, 128), jnp.int32),
            pltpu.VMEM((heads * spans // 2, 128), jnp.int32),
            pltpu.VMEM((8, 128), jnp.int32),
            pltpu.SMEM((8, 128), jnp.int32),
            pltpu.SemaphoreType.DMA,
        ],
        compiler_params=params(),
        cost_estimate=cost(1 << 26),
        name="first",
    )(me, ids, key_blocks, value_blocks)


def pack_rest(tab, key_blocks, value_blocks, heads, spans):
    return pl.pallas_call(
        functools.partial(pack_kernel, spans=spans),
        grid=(1,),
        out_shape=[jax.ShapeDtypeStruct(five(spans), jnp.bfloat16)] * (heads - 1),
        in_specs=[SMEM, VMEM, VMEM],
        out_specs=[slotted(spans, 0)] * (heads - 1),
        compiler_params=params(),
        cost_estimate=cost(1 << 26),
        name="pack",
    )(tab, key_blocks, value_blocks)


def mask(me, ids, spans, blocks):
    heads, picks, _ = ids.shape
    return pl.pallas_call(
        functools.partial(mask_kernel, heads=heads, spans=spans, blocks=blocks, picks=picks),
        out_shape=jax.ShapeDtypeStruct((heads, spans * CAP, blocks * KEY_BLOCK), jnp.float32),
        in_specs=[SMEM, VMEM],
        out_specs=VMEM,
        compiler_params=params(),
        cost_estimate=cost(1 << 26),
        name="mask",
    )(me, ids)


def turn(x):
    rows, cols = x.shape
    return pl.pallas_call(
        turn_kernel,
        grid=(cols // 256,),
        out_shape=jax.ShapeDtypeStruct((cols, rows), x.dtype),
        in_specs=[pl.BlockSpec((rows, 256), lambda i: (0, i))],
        out_specs=pl.BlockSpec((256, rows), lambda i: (i, 0)),
        compiler_params=params(),
        cost_estimate=cost(1 << 26),
        name="turn",
    )(x)


def attend(head, me, q, g, k, v, lse, bias, far_kv, gq_full, ahead, slots):
    rows, width = q.shape
    heads = lse.shape[0]
    tiles = rows // TQ
    spans = far_kv.shape[0]
    far = spans * CAP * KEY_BLOCK
    column = pl.BlockSpec((TQ, HEAD_DIM), lambda i: (i, head))
    alone = pl.BlockSpec((TQ, HEAD_DIM), lambda i: (i, 0))
    in_specs = [
        SMEM,
        column,
        column,
        column,
        column,
        pl.BlockSpec((heads, TQ), lambda i: (0, i)),
        pl.BlockSpec((None, spans * CAP, TQ), lambda i: (head, 0, i)),
        slotted(spans, 0),
    ]
    args = [me, q, g, k, v, lse, bias, far_kv]
    merge = ahead is not None
    if merge:
        in_specs.append(slotted(spans, 0))
        args.append(ahead)
    aliases = {}
    if gq_full is not None:
        aliases[len(args)] = 0
        in_specs.append(ANY)
        args.append(gq_full)
    return pl.pallas_call(
        functools.partial(
            attend_kernel, head=head, extra=len(aliases), merge=int(merge), tiles=tiles, far=far
        ),
        grid=(tiles,),
        in_specs=in_specs,
        out_specs=[column, alone, alone, alone, slotted(spans, 0)],
        out_shape=[
            jax.ShapeDtypeStruct((rows, width), jnp.bfloat16),
            jax.ShapeDtypeStruct((rows, HEAD_DIM), jnp.bfloat16),
            jax.ShapeDtypeStruct((rows, HEAD_DIM), jnp.float32),
            jax.ShapeDtypeStruct((rows, HEAD_DIM), jnp.float32),
            jax.ShapeDtypeStruct(five(spans, slots), jnp.bfloat16),
        ],
        scratch_shapes=[
            pltpu.VMEM((far, TQ), jnp.float32),
            pltpu.VMEM((far, TQ), jnp.float32),
            pltpu.VMEM((far, TQ), jnp.bfloat16),
            pltpu.VMEM((far, HEAD_DIM), jnp.float32),
            pltpu.VMEM((far, HEAD_DIM), jnp.float32),
            pltpu.VMEM((HEAD_DIM, far), jnp.bfloat16),
        ],
        input_output_aliases=aliases,
        cost_estimate=cost(10 * rows * far * HEAD_DIM, 8 << 20),
        compiler_params=params(dimension_semantics=("arbitrary",)),
    )(*args)


def weigh(xt, shards, buffer, spans, slot, slots):
    cols, rows = xt.shape
    tall = pl.BlockSpec((rows, HEAD_DIM), lambda i: (0, 0))
    tall_rows = 256
    in_specs = [pl.BlockSpec((tall_rows, rows), lambda i: (i, 0))] + [tall] * len(shards)
    args = [xt, *shards]
    aliases = {}
    if buffer is not None:
        aliases[len(args)] = 0
        in_specs.append(ANY)
        args.append(buffer)
    owned = cols // spans
    per = tall_rows // owned
    return pl.pallas_call(
        functools.partial(weight_kernel, shards=len(shards)),
        grid=(cols // tall_rows,),
        in_specs=in_specs,
        out_specs=pl.BlockSpec(
            (per, None, len(shards), owned, HEAD_DIM), lambda i: (i, slot, 0, 0, 0)
        ),
        out_shape=jax.ShapeDtypeStruct(five(spans, slots), jnp.bfloat16),
        input_output_aliases=aliases,
        compiler_params=params(),
        cost_estimate=cost(2 * cols * rows * len(shards) * HEAD_DIM, 8 << 20),
        name="weigh",
    )(*args)


def total(place, got, slot, buffer, head, heads, order):
    spans = got.shape[0]
    args = [place, got]
    in_specs = [SMEM, slotted(spans, slot)]
    aliases = {}
    if buffer is not None:
        aliases = {2: 0}
        in_specs.append(VMEM)
        args.append(buffer)
    return pl.pallas_call(
        functools.partial(total_kernel, head=head, heads=heads, order=order),
        grid=(1,),
        in_specs=in_specs,
        out_specs=VMEM,
        out_shape=jax.ShapeDtypeStruct(
            (KEY_BLOCK, len(order) * heads * HEAD_DIM), jnp.float32
        ),
        input_output_aliases=aliases,
        compiler_params=params(),
        cost_estimate=cost(1 << 24),
        name="total",
    )(*args)


def land(head, me, tab, home, dko, dvo, full, rows, width):
    spans = home.shape[0]
    column = pl.BlockSpec((rows, HEAD_DIM), lambda i: (0, head))
    alone = pl.BlockSpec((rows, HEAD_DIM), lambda i: (0, 0))
    in_specs = [SMEM, SMEM, slotted(spans, 0), alone, alone]
    args = [me, tab, home, dko, dvo]
    aliases = {}
    if full is not None:
        in_specs += [ANY, ANY]
        args += list(full)
        aliases = {5: 0, 6: 1}
    return pl.pallas_call(
        functools.partial(land_kernel, head=head, spans=spans),
        grid=(1,),
        in_specs=in_specs,
        out_specs=[column, column],
        out_shape=[jax.ShapeDtypeStruct((rows, width), jnp.float32)] * 2,
        input_output_aliases=aliases,
        compiler_params=params(),
        cost_estimate=cost(1 << 24),
    )(*args)


def exchange(x):
    return lax.all_to_all(x, "kv", split_axis=0, concat_axis=0, tiled=True)


def shift(x, by, tp):
    return lax.ppermute(x, "tp", [(i, (i + by) % tp) for i in range(tp)])


def program(query_rows, key_rows, value_rows, log_sums, cotangent, layer_input, chosen):
    spans = lax.axis_size("kv")
    tp = lax.axis_size("tp")
    heads = log_sums.shape[0]
    rows, width = query_rows.shape
    blocks = rows // KEY_BLOCK
    me = lax.axis_index("kv").astype(jnp.int32).reshape(1)
    place = lax.axis_index("tp").astype(jnp.int32).reshape(1)
    ids = jnp.transpose(chosen, (0, 2, 1))
    key_blocks = key_rows.reshape(blocks, KEY_BLOCK, width)
    value_blocks = value_rows.reshape(blocks, KEY_BLOCK, width)
    order = (0, 1, 3, 2)

    send0, tab = pack_first(me, ids, key_blocks, value_blocks, heads, spans)
    far0 = exchange(send0)
    send1, send2 = pack_rest(tab, key_blocks, value_blocks, heads, spans)
    xt = turn(layer_input)
    bias = mask(me, ids, spans, blocks)

    def attention(h, far, gq_full, ahead, slots):
        return attend(
            h, me, query_rows, cotangent, key_rows, value_rows, log_sums, bias, far,
            gq_full, ahead, slots,
        )

    def gathered(gq):
        right = shift(gq, -1, tp)
        left = shift(gq, 1, tp)
        across = shift(gq, 2, tp)
        return gq, right, left, across

    def product(shards, buffer, slot, slots):
        return weigh(xt, shards, buffer, spans, slot, slots)

    far1 = exchange(send1)
    gq_full, gq, *own0, out = attention(0, far0, None, send2, 1)
    shards0 = gathered(gq)
    far2 = exchange(out)
    gq_full, gq, *own1, out = attention(1, far1, gq_full, None, 2)
    shards1 = gathered(gq)
    home1 = exchange(product(shards0, out, 1, 2))
    gq_full, gq, *own2, out = attention(2, far2, gq_full, None, 2)
    shards2 = gathered(gq)
    home2 = exchange(product(shards1, out, 1, 2))
    last = exchange(product(shards2, None, 0, 1))

    full = None
    for h, (home, own) in enumerate(((far2, own0), (home1, own1), (home2, own2))):
        full = land(h, me, tab, home, *own, full, rows, width)
    grad_weight = None
    for h, (got, slot) in enumerate(((home1, 1), (home2, 1), (last, 0))):
        grad_weight = total(place, got, slot, grad_weight, h, heads, order)
    return gq_full, full[0], full[1], grad_weight


def solution(mesh):
    placed = (
        P("kv", "tp"),
        P("kv", "tp"),
        P("kv", "tp"),
        P("tp", "kv"),
        P("kv", "tp"),
        P("kv", "tp"),
        P("tp", None, None),
    )
    return jax.shard_map(
        program,
        mesh=mesh,
        in_specs=placed,
        out_specs=(P("kv", "tp"), P("kv", "tp"), P("kv", "tp"), P(("tp", "kv"), None)),
        check_vma=False,
    )
```

time: 309 us -> 221 us (0.72)
  blocking collectives: 88.9 us -> 0 us
  local copies, waits for them, and re-layouts: 44.8 us -> 6.85 us
  starting transfers between devices: 25.6 us -> 54.5 us
  waiting for transfers between devices: 21.3 us -> 45.7 us
  Pallas kernels: 89.2 us -> 110 us
  matrix products: 18.5 us -> 0 us
  between operations: 14 us -> 0.84 us
  other arithmetic: 4.33 us -> 0 us
    all_to_all x4 -> x0, blocking collectives: 88.9 us -> none  [exchange(): return lax.all_to_all(x, 'kv', split_axis=0, concat_axis=0, tiled=True)]
    ppermute x0 -> x9, waiting for transfers between devices: none -> 28.7 us  [shift(): return lax.ppermute(x, 'tp', [(i, (i + by) % tp) for i in range(tp)])]
    unnamed x75 -> x30, local copies, waits for them, and re-layouts: 29.9 us -> 6.85 us
    dot_general x3 -> x0, matrix products: 18.5 us -> none  [local(): lax.dot_general(layer_input, everyone, (((0,), (1,)), ((), ())), preferre...]
    pallas_call x4 -> x13, Pallas kernels: 79.9 us -> 96.3 us  [the longest x3 55.9 us: attend(): pl.pallas_call(functools.partial(attend_kernel, head=head, extra=len(alia...]
    all_to_all x5 -> x6, starting transfers between devices: 25.5 us -> 41.9 us  [exchange(): return lax.all_to_all(x, 'kv', split_axis=0, concat_axis=0, tiled=True)]
    ppermute x0 -> x9, starting transfers between devices: none -> 12.7 us  [shift(): return lax.ppermute(x, 'tp', [(i, (i + by) % tp) for i in range(tp)])]
    reshape x4 -> x0, local copies, waits for them, and re-layouts: 7.51 us -> none  [the longest x3 6.73 us: local(): mine = exchange(part.reshape(spans, -1, part.shape[1] * HEAD_DIM))]
  transfers between devices with their start and end apart: 8 -> 15, of which waited for: 4 -> 6; matrix products, arithmetic and copies ran while one was open for 12% -> 0% of each run, Pallas kernels for 20% -> 46%
where the time goes in v2:
time: 221 us; the launch traced here: 218 us
  Pallas kernels  110 us (50%)
  starting transfers between devices  54.5 us (25%)
  waiting for transfers between devices  45.7 us (21%)
  local copies, waits for them, and re-layouts  6.85 us (3%)
    pallas_call x3, Pallas kernels, attend(): pl.pallas_call(functools.partial(attend_kernel, head=head, extra=len(alia...  55.9 us
    all_to_all x6, starting transfers between devices, exchange(): return lax.all_to_all(x, 'kv', split_axis=0, concat_axis=0, tiled=True)  41.9 us
    ppermute x9, waiting for transfers between devices, shift(): return lax.ppermute(x, 'tp', [(i, (i + by) % tp) for i in range(tp)])  28.7 us
    pallas_call x3, Pallas kernels, weigh(): pl.pallas_call(functools.partial(weight_kernel, shards=len(shards)), grid...  18.3 us
    all_to_all x6, waiting for transfers between devices, exchange(): return lax.all_to_all(x, 'kv', split_axis=0, concat_axis=0, tiled=True)  17 us
    pallas_call x3, Pallas kernels, land(): pl.pallas_call(functools.partial(land_kernel, head=head, spans=spans), gr...  14 us
    ppermute x9, starting transfers between devices, shift(): return lax.ppermute(x, 'tp', [(i, (i + by) % tp) for i in range(tp)])  12.7 us
    unnamed x30, local copies, waits for them, and re-layouts  6.85 us
  transfers between devices with their start and end apart: 15, of which 6 were waited for; matrix products, arithmetic and copies ran while one was open for 0% of the time, Pallas kernels for 46%

profile of v2, /device:TPU:0, one launch (start us, length us, event | category | flops | bytes accessed | tf_op | source)
XLA Modules:
  0.0 218.4 jit_solution(115402617048320861)
XLA Ops:
  0.6 3.6 %first.1 = (bf16[32,1,4,32,128]{4,3,2,1,0:T(8,128)(2,1)}, s32[8,128]{1,0:T(8,128)}) custom-call(s32[1]{0:T(128)} %bitcast.me_ref, s32[3,12,2048]{2,1,0:T(8,128)} %bitcast.9, bf16[64,32,384]{2,1,0:T(8,128)(2,1)} %bitcast.5, bf16[64,32,384]{2,1,0:T(8,128)(2,1)} %bitcast.7), custom_call_target="tpu_custom_call" | custom-call | flops 67108864 | bytes 1048576 | tf_op jit(solution)/shard_map/first/pallas_call | solution.py:295
  4.2 8.5 %all-to-all-start = ((bf16[32,1,4,32,128]{4,3,2,1,0:T(8,128)(2,1)}), bf16[32,1,4,32,128]{4,3,2,1,0:T(8,128)(2,1)S(1)}, u32[]{:S(2)}, u32[]{:S(2)}) async-start(bf16[32,1,4,32,128]{4,3,2,1,0:T(8,128)(2,1)} %get-tuple-element.29), calls=%async_computation | async-start | bytes 2097152 | tf_op jit(solution)/shard_map/all_to_all | solution.py:489
  12.7 3.9 %pack.1 = (bf16[32,1,4,32,128]{4,3,2,1,0:T(8,128)(2,1)}, bf16[32,1,4,32,128]{4,3,2,1,0:T(8,128)(2,1)}) custom-call(s32[8,128]{1,0:T(8,128)} %get-tuple-element.30.tab_ref, bf16[64,32,384]{2,1,0:T(8,128)(2,1)} %bitcast.6, bf16[64,32,384]{2,1,0:T(8,128)(2,1)} %bitcast.8), custom_call_target="tpu_custom_call" | custom-call | flops 67108864 | bytes 1048576 | tf_op jit(solution)/shard_map/pack/pallas_call | solution.py:318
  16.6 13.3 %all-to-all-done.refs_6_ = bf16[32,1,4,32,128]{4,3,2,1,0:T(8,128)(2,1)S(1)} async-done(((bf16[32,1,4,32,128]{4,3,2,1,0:T(8,128)(2,1)}), bf16[32,1,4,32,128]{4,3,2,1,0:T(8,128)(2,1)S(1)}, u32[]{:S(2)}, u32[]{:S(2)}) %all-to-all-start) | async-done | bytes 1048608 | tf_op jit(solution)/shard_map/all_to_all | solution.py:489
  29.9 3.9 %all-to-all-start.2 = ((bf16[32,1,4,32,128]{4,3,2,1,0:T(8,128)(2,1)}), bf16[32,1,4,32,128]{4,3,2,1,0:T(8,128)(2,1)S(1)}, u32[]{:S(2)}, u32[]{:S(2)}) async-start(bf16[32,1,4,32,128]{4,3,2,1,0:T(8,128)(2,1)} %get-tuple-element.33), calls=%async_computation.2 | async-start | bytes 2097152 | tf_op jit(solution)/shard_map/all_to_all | solution.py:489
  33.8 3.1 %mask.1.refs_5_ = f32[3,64,2048]{2,1,0:T(8,128)} custom-call(s32[1]{0:T(128)} %bitcast.me_ref, s32[3,12,2048]{2,1,0:T(8,128)} %bitcast.10), custom_call_target="tpu_custom_call" | custom-call | flops 67108864 | bytes 1048576 | tf_op jit(solution)/shard_map/mask/pallas_call | solution.py:332
  36.9 19.0 %shard_map.102 = (bf16[2048,384]{1,0:T(8,128)(2,1)}, bf16[2048,128]{1,0:T(8,128)(2,1)}, f32[2048,128]{1,0:T(8,128)}, f32[2048,128]{1,0:T(8,128)}, bf16[32,1,4,32,128]{4,3,2,1,0:T(8,128)(2,1)}) custom-call(s32[1]{0:T(128)} %bitcast.me_ref, bf16[2048,384]{1,0:T(8,128)(2,1)} %refs_0_.5, bf16[2048,384]{1,0:T(8,128)(2,1)} %refs_1_.5, bf16[2048,384]{1,0:T(8,128)(2,1)} %refs_2_.5, ...), custom_call_target="tpu_custom_call" | custom-call | flops 5368709120 | bytes 8388608 | tf_op jit(solution)/shard_map/pallas_call | solution.py:385
  56.0 0.0 all-to-all-done.2.refs_6_
  56.0 0.0 copy-start.3
  56.0 7.6 %all-to-all-start.1 = ((bf16[32,1,4,32,128]{4,3,2,1,0:T(8,128)(2,1)}), bf16[32,1,4,32,128]{4,3,2,1,0:T(8,128)(2,1)S(1)}, u32[]{:S(2)}, u32[]{:S(2)}) async-start(bf16[32,1,4,32,128]{4,3,2,1,0:T(8,128)(2,1)} %get-tuple-element.32), calls=%async_computation.1 | async-start | bytes 2097152 | tf_op jit(solution)/shard_map/all_to_all | solution.py:489
  63.6 2.8 %collective-permute-start.3 = (bf16[2048,128]{1,0:T(8,128)(2,1)S(1)}, bf16[2048,128]{1,0:T(8,128)(2,1)S(1)}, u32[]{:S(2)}, u32[]{:S(2)}) collective-permute-start(bf16[2048,128]{1,0:T(8,128)(2,1)S(1)} %copy-done.5), channel_id=1, source_target_pairs={{0,3},{1,0},{2,1},{3,2},{4,7},{5,4},{6,5},{7,6},{8,11},{9,8},{10,9... | collective-permute-start | bytes 1572872 | tf_op jit(solution)/shard_map/ppermute | solution.py:493
  66.4 2.3 %collective-permute-start.5 = (bf16[2048,128]{1,0:T(8,128)(2,1)S(1)}, bf16[2048,128]{1,0:T(8,128)(2,1)}, u32[]{:S(2)}, u32[]{:S(2)}) collective-permute-start(bf16[2048,128]{1,0:T(8,128)(2,1)S(1)} %copy-done.5), channel_id=1, source_target_pairs={{0,2},{1,3},{2,0},{3,1},{4,6},{5,7},{6,4},{7,5},{8,10},{9,11},{10,... | collective-permute-start | bytes 1572872 | tf_op jit(solution)/shard_map/ppermute | solution.py:493
  68.7 5.3 %turn.1.xt_ref = bf16[1024,2048]{1,0:T(8,128)(2,1)} custom-call(bf16[2048,1024]{1,0:T(8,128)(2,1)} %x_ref.1), custom_call_target="tpu_custom_call" | custom-call | flops 67108864 | bytes 1048576 | tf_op jit(solution)/shard_map/turn/pallas_call | solution.py:345
  74.0 18.5 %shard_map.103 = (bf16[2048,384]{1,0:T(8,128)(2,1)}, bf16[2048,128]{1,0:T(8,128)(2,1)}, f32[2048,128]{1,0:T(8,128)}, f32[2048,128]{1,0:T(8,128)}, bf16[32,2,4,32,128]{4,3,2,1,0:T(8,128)(2,1)}) custom-call(s32[1]{0:T(128)} %bitcast.me_ref, bf16[2048,384]{1,0:T(8,128)(2,1)} %refs_0_.5, bf16[2048,384]{1,0:T(8,128)(2,1)} %refs_1_.5, ...), custom_call_target="tpu_custom_call", output_to_operand_aliasing={{0}: (8, {})} | custom-call | flops 5368709120 | bytes 8388608 | tf_op jit(solution)/shard_map/pallas_call | solution.py:385
  92.4 0.0 copy-start.6
  92.5 0.2 collective-permute-done.4.rest_2_
  92.7 0.6 copy-done.6
  93.2 0.3 copy-done.8
  93.5 6.1 %weigh.4 = bf16[32,2,4,32,128]{4,3,2,1,0:T(8,128)(2,1)} custom-call(bf16[1024,2048]{1,0:T(8,128)(2,1)} %turn.1.xt_ref, bf16[2048,128]{1,0:T(8,128)(2,1)} %get-tuple-element.41.rest_0_, bf16[2048,128]{1,0:T(8,128)(2,1)} %copy-done.6, bf16[2048,128]{1,0:T(8,128)(2,1)} %copy-done.8, ...), custom_call_target="tpu_custom_call", output_to_operand_aliasing={{}: (5, {})} | custom-call | flops 2147483648 | bytes 8388608 | tf_op jit(solution)/shard_map/weigh/pallas_call | solution.py:426
  99.7 1.0 copy-done.2
  100.7 7.3 %all-to-all-start.4 = ((bf16[32,2,4,32,128]{4,3,2,1,0:T(8,128)(2,1)}), bf16[32,2,4,32,128]{4,3,2,1,0:T(8,128)(2,1)S(1)}, u32[]{:S(2)}, u32[]{:S(2)}) async-start(bf16[32,2,4,32,128]{4,3,2,1,0:T(8,128)(2,1)} %weigh.4), calls=%async_computation.4 | async-start | bytes 4194304 | tf_op jit(solution)/shard_map/all_to_all | solution.py:489
  108.0 1.2 collective-permute-start
  109.2 0.9 collective-permute-start.1
  110.1 1.8 collective-permute-start.2
  111.9 18.5 %shard_map.104 = (bf16[2048,384]{1,0:T(8,128)(2,1)}, bf16[2048,128]{1,0:T(8,128)(2,1)}, f32[2048,128]{1,0:T(8,128)}, f32[2048,128]{1,0:T(8,128)}, bf16[32,2,4,32,128]{4,3,2,1,0:T(8,128)(2,1)}) custom-call(s32[1]{0:T(128)} %bitcast.me_ref, bf16[2048,384]{1,0:T(8,128)(2,1)} %refs_0_.5, bf16[2048,384]{1,0:T(8,128)(2,1)} %refs_1_.5, ...), custom_call_target="tpu_custom_call", output_to_operand_aliasing={{0}: (8, {})} | custom-call | flops 5368709120 | bytes 8388608 | tf_op jit(solution)/shard_map/pallas_call | solution.py:385
  130.4 5.3 %collective-permute-done.1.rest_2_ = bf16[2048,128]{1,0:T(8,128)(2,1)S(1)} collective-permute-done((bf16[2048,128]{1,0:T(8,128)(2,1)}, bf16[2048,128]{1,0:T(8,128)(2,1)S(1)}, u32[]{:S(2)}, u32[]{:S(2)}) %collective-permute-start.1) | collective-permute-done | bytes 524320 | tf_op jit(solution)/shard_map/ppermute | solution.py:493
  135.7 0.8 copy-done.9
  136.5 0.2 copy-done.10
  136.7 6.1 %weigh.3 = bf16[32,2,4,32,128]{4,3,2,1,0:T(8,128)(2,1)} custom-call(bf16[1024,2048]{1,0:T(8,128)(2,1)} %turn.1.xt_ref, bf16[2048,128]{1,0:T(8,128)(2,1)} %get-tuple-element.37.rest_0_, bf16[2048,128]{1,0:T(8,128)(2,1)} %copy-done.7, bf16[2048,128]{1,0:T(8,128)(2,1)} %copy-done.9, bf16[2048,128]{1,0:T(8,128)(2,1)} %copy-done.10, ...), custom_call_target="tpu_custom_call", output_to_operand_aliasing={{}: (5, {})} | custom-call | flops 2147483648 | bytes 8388608 | tf_op jit(solution)/shard_map/weigh/pallas_call | solution.py:426
  142.8 1.4 copy-done
  144.2 7.4 %all-to-all-start.3 = ((bf16[32,2,4,32,128]{4,3,2,1,0:T(8,128)(2,1)}), bf16[32,2,4,32,128]{4,3,2,1,0:T(8,128)(2,1)}, u32[]{:S(2)}, u32[]{:S(2)}) async-start(bf16[32,2,4,32,128]{4,3,2,1,0:T(8,128)(2,1)} %weigh.3), calls=%async_computation.3 | async-start | bytes 4194304 | tf_op jit(solution)/shard_map/all_to_all | solution.py:489
  151.6 0.6 collective-permute-start.6
  152.2 1.5 collective-permute-start.7
  153.7 1.5 collective-permute-start.8
  155.2 11.2 %collective-permute-done.6.rest_1_ = bf16[2048,128]{1,0:T(8,128)(2,1)S(1)} collective-permute-done((bf16[2048,128]{1,0:T(8,128)(2,1)S(1)}, bf16[2048,128]{1,0:T(8,128)(2,1)S(1)}, u32[]{:S(2)}, u32[]{:S(2)}) %collective-permute-start.6) | collective-permute-done | bytes 524320 | tf_op jit(solution)/shard_map/ppermute | solution.py:493
  166.4 12.0 %collective-permute-done.7.rest_2_ = bf16[2048,128]{1,0:T(8,128)(2,1)S(1)} collective-permute-done((bf16[2048,128]{1,0:T(8,128)(2,1)S(1)}, bf16[2048,128]{1,0:T(8,128)(2,1)S(1)}, u32[]{:S(2)}, u32[]{:S(2)}) %collective-permute-start.7) | collective-permute-done | bytes 524320 | tf_op jit(solution)/shard_map/ppermute | solution.py:493
  178.4 0.8 copy-done.13
  179.3 0.8 copy-done.14
  180.0 6.1 %weigh.5 = bf16[32,1,4,32,128]{4,3,2,1,0:T(8,128)(2,1)} custom-call(bf16[1024,2048]{1,0:T(8,128)(2,1)} %turn.1.xt_ref, bf16[2048,128]{1,0:T(8,128)(2,1)} %get-tuple-element.53.rest_0_, bf16[2048,128]{1,0:T(8,128)(2,1)} %copy-done.12, bf16[2048,128]{1,0:T(8,128)(2,1)} %copy-done.13, bf16[2048,128]{1,0:T(8,128)(2,1)} %copy-done.14), custom_call_target="tpu_custom_call" | custom-call | flops 2147483648 | bytes 8388608 | tf_op jit(solution)/shard_map/weigh/pallas_call | solution.py:426
  186.1 7.2 %all-to-all-start.5 = ((bf16[32,1,4,32,128]{4,3,2,1,0:T(8,128)(2,1)}), bf16[32,1,4,32,128]{4,3,2,1,0:T(8,128)(2,1)S(1)}, u32[]{:S(2)}, u32[]{:S(2)}) async-start(bf16[32,1,4,32,128]{4,3,2,1,0:T(8,128)(2,1)} %weigh.5), calls=%async_computation.5 | async-start | bytes 2097152 | tf_op jit(solution)/shard_map/all_to_all | solution.py:489
  193.4 4.7 %shard_map.105 = (f32[2048,384]{1,0:T(8,128)}, f32[2048,384]{1,0:T(8,128)}) custom-call(s32[1]{0:T(128)} %bitcast.me_ref, s32[8,128]{1,0:T(8,128)} %get-tuple-element.30.tab_ref, bf16[32,1,4,32,128]{4,3,2,1,0:T(8,128)(2,1)} %copy-done.2, f32[2048,128]{1,0:T(8,128)} %get-tuple-element.45.dko_ref, f32[2048,128]{1,0:T(8,128)} %get-tuple-element.46.dvo_ref), custom_call_target="tpu_custom_call" | custom-call | flops 16777216 | bytes 1048576 | tf_op jit(solution)/shard_map/pallas_call | solution.py:476
  198.1 2.1 total.3.rest_0_
  200.1 4.7 %shard_map.106 = (f32[2048,384]{1,0:T(8,128)}, f32[2048,384]{1,0:T(8,128)}) custom-call(s32[1]{0:T(128)} %bitcast.me_ref, s32[8,128]{1,0:T(8,128)} %get-tuple-element.30.tab_ref, bf16[32,2,4,32,128]{4,3,2,1,0:T(8,128)(2,1)} %copy-done, f32[2048,128]{1,0:T(8,128)} %get-tuple-element.43.dko_ref, ...), custom_call_target="tpu_custom_call", output_to_operand_aliasing={{0}: (5, {}), {1}: (6, {})} | custom-call | flops 16777216 | bytes 1048576 | tf_op jit(solution)/shard_map/pallas_call | solution.py:476
  204.8 2.1 total.4.rest_0_
  206.9 3.7 %all-to-all-done.5.got_ref = bf16[32,1,4,32,128]{4,3,2,1,0:T(8,128)(2,1)S(1)} async-done(((bf16[32,1,4,32,128]{4,3,2,1,0:T(8,128)(2,1)}), bf16[32,1,4,32,128]{4,3,2,1,0:T(8,128)(2,1)S(1)}, u32[]{:S(2)}, u32[]{:S(2)}) %all-to-all-start.5) | async-done | bytes 1048608 | tf_op jit(solution)/shard_map/all_to_all | solution.py:489
  210.6 1.0 copy-done.1
  211.6 2.1 total.5
  213.7 4.7 %shard_map.107 = (f32[2048,384]{1,0:T(8,128)}, f32[2048,384]{1,0:T(8,128)}) custom-call(s32[1]{0:T(128)} %bitcast.me_ref, s32[8,128]{1,0:T(8,128)} %get-tuple-element.30.tab_ref, bf16[32,2,4,32,128]{4,3,2,1,0:T(8,128)(2,1)} %all-to-all-done.3.back_ref.got_ref, f32[2048,128]{1,0:T(8,128)} %get-tuple-element.39.dko_ref, ...), custom_call_target="tpu_custom_call", output_to_operand_aliasing={{0}: (5, {}), {1}: (6, {})} | custom-call | flops 16777216 | bytes 1048576 | tf_op jit(solution)/shard_map/pallas_call | solution.py:476
  (28 shorter events, 0.1 us)
Async XLA Ops:
  4.2 25.7 %all-to-all-start = ((bf16[32,1,4,32,128]{4,3,2,1,0:T(8,128)(2,1)}), bf16[32,1,4,32,128]{4,3,2,1,0:T(8,128)(2,1)S(1)}, u32[]{:S(2)}, u32[]{:S(2)}) async-start(bf16[32,1,4,32,128]{4,3,2,1,0:T(8,128)(2,1)} %get-tuple-element.29), calls=%async_computation | async-start | bytes 2097152 | tf_op jit(solution)/shard_map/all_to_all | solution.py:489
  29.9 7.0 %copy-start.4 = (bf16[32,1,4,32,128]{4,3,2,1,0:T(8,128)(2,1)}, bf16[32,1,4,32,128]{4,3,2,1,0:T(8,128)(2,1)S(1)}, u32[]{:S(2)}) copy-start(bf16[32,1,4,32,128]{4,3,2,1,0:T(8,128)(2,1)S(1)} %all-to-all-done.refs_6_) | copy-start | bytes 3145732
  29.9 26.1 %all-to-all-start.2 = ((bf16[32,1,4,32,128]{4,3,2,1,0:T(8,128)(2,1)}), bf16[32,1,4,32,128]{4,3,2,1,0:T(8,128)(2,1)S(1)}, u32[]{:S(2)}, u32[]{:S(2)}) async-start(bf16[32,1,4,32,128]{4,3,2,1,0:T(8,128)(2,1)} %get-tuple-element.33), calls=%async_computation.2 | async-start | bytes 2097152 | tf_op jit(solution)/shard_map/all_to_all | solution.py:489
  56.0 7.6 %copy-start.5 = (bf16[2048,128]{1,0:T(8,128)(2,1)S(1)}, bf16[2048,128]{1,0:T(8,128)(2,1)}, u32[]{:S(2)}) copy-start(bf16[2048,128]{1,0:T(8,128)(2,1)} %get-tuple-element.41.rest_0_) | copy-start | bytes 1572868
  56.0 18.0 %copy-start.3 = (bf16[32,1,4,32,128]{4,3,2,1,0:T(8,128)(2,1)}, bf16[32,1,4,32,128]{4,3,2,1,0:T(8,128)(2,1)S(1)}, u32[]{:S(2)}) copy-start(bf16[32,1,4,32,128]{4,3,2,1,0:T(8,128)(2,1)S(1)} %all-to-all-done.2.refs_6_) | copy-start | bytes 3145732
  56.0 43.6 %all-to-all-start.1 = ((bf16[32,1,4,32,128]{4,3,2,1,0:T(8,128)(2,1)}), bf16[32,1,4,32,128]{4,3,2,1,0:T(8,128)(2,1)S(1)}, u32[]{:S(2)}, u32[]{:S(2)}) async-start(bf16[32,1,4,32,128]{4,3,2,1,0:T(8,128)(2,1)} %get-tuple-element.32), calls=%async_computation.1 | async-start | bytes 2097152 | tf_op jit(solution)/shard_map/all_to_all | solution.py:489
  63.6 28.9 %collective-permute-start.3 = (bf16[2048,128]{1,0:T(8,128)(2,1)S(1)}, bf16[2048,128]{1,0:T(8,128)(2,1)S(1)}, u32[]{:S(2)}, u32[]{:S(2)}) collective-permute-start(bf16[2048,128]{1,0:T(8,128)(2,1)S(1)} %copy-done.5), channel_id=1, source_target_pairs={{0,3},{1,0},{2,1},{3,2},{4,7},{5,4},{6,5},{7,6},{8,11},{9,8},{10,9... | collective-permute-start | bytes 1572872 | tf_op jit(solution)/shard_map/ppermute | solution.py:493
  66.4 26.3 %collective-permute-start.4 = (bf16[2048,128]{1,0:T(8,128)(2,1)S(1)}, bf16[2048,128]{1,0:T(8,128)(2,1)S(1)}, u32[]{:S(2)}, u32[]{:S(2)}) collective-permute-start(bf16[2048,128]{1,0:T(8,128)(2,1)S(1)} %copy-done.5), channel_id=1, source_target_pairs={{0,1},{1,2},{2,3},{3,0},{4,5},{5,6},{6,7},{7,4},{8,9},{9,10},{10,1... | collective-permute-start | bytes 1572872 | tf_op jit(solution)/shard_map/ppermute | solution.py:493
  66.4 26.3 %collective-permute-start.5 = (bf16[2048,128]{1,0:T(8,128)(2,1)S(1)}, bf16[2048,128]{1,0:T(8,128)(2,1)}, u32[]{:S(2)}, u32[]{:S(2)}) collective-permute-start(bf16[2048,128]{1,0:T(8,128)(2,1)S(1)} %copy-done.5), channel_id=1, source_target_pairs={{0,2},{1,3},{2,0},{3,1},{4,6},{5,7},{6,4},{7,5},{8,10},{9,11},{10,... | collective-permute-start | bytes 1572872 | tf_op jit(solution)/shard_map/ppermute | solution.py:493
  92.4 0.8 copy-start.6
  92.7 0.8 copy-start.8
  99.6 1.0 copy-start.2
  100.7 42.1 %all-to-all-start.4 = ((bf16[32,2,4,32,128]{4,3,2,1,0:T(8,128)(2,1)}), bf16[32,2,4,32,128]{4,3,2,1,0:T(8,128)(2,1)S(1)}, u32[]{:S(2)}, u32[]{:S(2)}) async-start(bf16[32,2,4,32,128]{4,3,2,1,0:T(8,128)(2,1)} %weigh.4), calls=%async_computation.4 | async-start | bytes 4194304 | tf_op jit(solution)/shard_map/all_to_all | solution.py:489
  108.0 22.4 %collective-permute-start = (bf16[2048,128]{1,0:T(8,128)(2,1)}, bf16[2048,128]{1,0:T(8,128)(2,1)S(1)}, u32[]{:S(2)}, u32[]{:S(2)}) collective-permute-start(bf16[2048,128]{1,0:T(8,128)(2,1)} %get-tuple-element.37.rest_0_), channel_id=1, source_target_pairs={{0,3},{1,0},{2,1},{3,2},{4,7},{5,4},{6,5},{7,6},{8,11},{9,8},{10,9... | collective-permute-start | bytes 1572872 | tf_op jit(solution)/shard_map/ppermute | solution.py:493
  109.2 26.5 %collective-permute-start.1 = (bf16[2048,128]{1,0:T(8,128)(2,1)}, bf16[2048,128]{1,0:T(8,128)(2,1)S(1)}, u32[]{:S(2)}, u32[]{:S(2)}) collective-permute-start(bf16[2048,128]{1,0:T(8,128)(2,1)} %get-tuple-element.37.rest_0_), channel_id=1, source_target_pairs={{0,1},{1,2},{2,3},{3,0},{4,5},{5,6},{6,7},{7,4},{8,9},{9,10},{10,1... | collective-permute-start | bytes 1572872 | tf_op jit(solution)/shard_map/ppermute | solution.py:493
  110.1 25.6 %collective-permute-start.2 = (bf16[2048,128]{1,0:T(8,128)(2,1)}, bf16[2048,128]{1,0:T(8,128)(2,1)S(1)}, u32[]{:S(2)}, u32[]{:S(2)}) collective-permute-start(bf16[2048,128]{1,0:T(8,128)(2,1)} %get-tuple-element.37.rest_0_), channel_id=1, source_target_pairs={{0,2},{1,3},{2,0},{3,1},{4,6},{5,7},{6,4},{7,5},{8,10},{9,11},{10,... | collective-permute-start | bytes 1572872 | tf_op jit(solution)/shard_map/ppermute | solution.py:493
  130.4 5.3 %copy-start.7 = (bf16[2048,128]{1,0:T(8,128)(2,1)}, bf16[2048,128]{1,0:T(8,128)(2,1)S(1)}, u32[]{:S(2)}) copy-start(bf16[2048,128]{1,0:T(8,128)(2,1)S(1)} %collective-permute-done.rest_1_) | copy-start | bytes 1572868
  135.7 0.8 copy-start.9
  135.7 1.0 copy-start.10
  142.8 8.8 %copy-start.11 = (bf16[2048,128]{1,0:T(8,128)(2,1)S(1)}, bf16[2048,128]{1,0:T(8,128)(2,1)}, u32[]{:S(2)}) copy-start(bf16[2048,128]{1,0:T(8,128)(2,1)} %get-tuple-element.53.rest_0_) | copy-start | bytes 1572868
  142.8 1.4 copy-start
  144.2 41.9 %all-to-all-start.3 = ((bf16[32,2,4,32,128]{4,3,2,1,0:T(8,128)(2,1)}), bf16[32,2,4,32,128]{4,3,2,1,0:T(8,128)(2,1)}, u32[]{:S(2)}, u32[]{:S(2)}) async-start(bf16[32,2,4,32,128]{4,3,2,1,0:T(8,128)(2,1)} %weigh.3), calls=%async_computation.3 | async-start | bytes 4194304 | tf_op jit(solution)/shard_map/all_to_all | solution.py:489
  151.6 14.9 %collective-permute-start.6 = (bf16[2048,128]{1,0:T(8,128)(2,1)S(1)}, bf16[2048,128]{1,0:T(8,128)(2,1)S(1)}, u32[]{:S(2)}, u32[]{:S(2)}) collective-permute-start(bf16[2048,128]{1,0:T(8,128)(2,1)S(1)} %copy-done.11), channel_id=1, source_target_pairs={{0,3},{1,0},{2,1},{3,2},{4,7},{5,4},{6,5},{7,6},{8,11},{9,8},{10,9... | collective-permute-start | bytes 1572872 | tf_op jit(solution)/shard_map/ppermute | solution.py:493
  152.2 26.3 %collective-permute-start.7 = (bf16[2048,128]{1,0:T(8,128)(2,1)S(1)}, bf16[2048,128]{1,0:T(8,128)(2,1)S(1)}, u32[]{:S(2)}, u32[]{:S(2)}) collective-permute-start(bf16[2048,128]{1,0:T(8,128)(2,1)S(1)} %copy-done.11), channel_id=1, source_target_pairs={{0,1},{1,2},{2,3},{3,0},{4,5},{5,6},{6,7},{7,4},{8,9},{9,10},{10,1... | collective-permute-start | bytes 1572872 | tf_op jit(solution)/shard_map/ppermute | solution.py:493
  153.7 24.8 %collective-permute-start.8 = (bf16[2048,128]{1,0:T(8,128)(2,1)S(1)}, bf16[2048,128]{1,0:T(8,128)(2,1)S(1)}, u32[]{:S(2)}, u32[]{:S(2)}) collective-permute-start(bf16[2048,128]{1,0:T(8,128)(2,1)S(1)} %copy-done.11), channel_id=1, source_target_pairs={{0,2},{1,3},{2,0},{3,1},{4,6},{5,7},{6,4},{7,5},{8,10},{9,11},{10,... | collective-permute-start | bytes 1572872 | tf_op jit(solution)/shard_map/ppermute | solution.py:493
  166.4 12.0 %copy-start.12 = (bf16[2048,128]{1,0:T(8,128)(2,1)}, bf16[2048,128]{1,0:T(8,128)(2,1)S(1)}, u32[]{:S(2)}) copy-start(bf16[2048,128]{1,0:T(8,128)(2,1)S(1)} %collective-permute-done.6.rest_1_) | copy-start | bytes 1572868
  178.4 0.8 copy-start.13
  179.3 0.8 copy-start.14
  186.1 24.4 %all-to-all-start.5 = ((bf16[32,1,4,32,128]{4,3,2,1,0:T(8,128)(2,1)}), bf16[32,1,4,32,128]{4,3,2,1,0:T(8,128)(2,1)S(1)}, u32[]{:S(2)}, u32[]{:S(2)}) async-start(bf16[32,1,4,32,128]{4,3,2,1,0:T(8,128)(2,1)} %weigh.5), calls=%async_computation.5 | async-start | bytes 2097152 | tf_op jit(solution)/shard_map/all_to_all | solution.py:489
  210.6 1.0 copy-start.1

commit v3 on v2

--- a/solution.py
+++ b/solution.py
@@ -15,6 +15,8 @@
 LOG2E = 1.4426950408889634
 NEG = -1.0e30
 TQ = 512
+VMEM_LIMIT = 60960 * 1024
+WEIGH_ROWS = 512
 KB = 256
 
 
@@ -111,30 +113,57 @@
         out_ref[:, cut] = x_ref[cut, :].T
 
 
-def weight_kernel(xt_ref, *rest, shards):
-    out_ref = rest[-1]
-    xt = xt_ref[...]
-    shape = (out_ref.shape[0],) + out_ref.shape[2:]
+def weight_kernel(me_ref, xt_ref, *rest, shards, steps, halves):
+    span = xt_ref.shape[0] // steps
+    xt = xt_ref[pl.ds(pl.multiple_of(pl.program_id(0) * span, span), span), :]
+    core = me_ref[0] % 2
+    shape = (span // KEY_BLOCK, KEY_BLOCK, HEAD_DIM)
+    sums = []
     for at in range(0, shards, 2):
         g = jnp.concatenate([rest[at][...], rest[at + 1][...]], axis=1)
         got = jnp.dot(xt, g, preferred_element_type=jnp.float32).astype(jnp.bfloat16)
-        out_ref[:, at] = got[:, :HEAD_DIM].reshape(shape)
-        out_ref[:, at + 1] = got[:, HEAD_DIM:].reshape(shape)
-
-
-def total_kernel(at_ref, got_ref, *rest, head, heads, order):
+        sums += [got[:, :HEAD_DIM].reshape(shape), got[:, HEAD_DIM:].reshape(shape)]
+    if halves:
+        keep_ref, give_ref = rest[-2:]
+        for p in range(2):
+            keep_ref[:, p] = jnp.where(core == 0, sums[p], sums[2 + p])
+            give_ref[:, p] = jnp.where(core == 0, sums[2 + p], sums[p])
+    else:
+        for p in range(shards):
+            rest[-1][:, p] = sums[p]
+
+
+def join_kernel(keep_ref, got_ref, *rest):
     out_ref = rest[-1]
-    if len(rest) > 1:
-        out_ref[...] = rest[0][...]
-    me = at_ref[0]
+    both = keep_ref[...].astype(jnp.float32) + got_ref[...].astype(jnp.float32)
+    out_ref[...] = both.astype(jnp.bfloat16)
+
+
+def put_sum(out_ref, got_ref, sources, column, first):
+    acc = got_ref[sources[0], column].astype(jnp.float32)
+    for i in sources[1:]:
+        acc = acc + got_ref[i, column].astype(jnp.float32)
+    out_ref[:, pl.ds(pl.multiple_of(first, HEAD_DIM), HEAD_DIM)] = acc
+
+
+def total_kernel(at_ref, got_ref, out_ref, *, head, heads, order):
     tp = len(order)
+    out_ref[...] = jnp.zeros_like(out_ref)
     for p in range(tp):
-        acc = got_ref[0, p].astype(jnp.float32)
-        for i in range(1, got_ref.shape[0]):
-            acc = acc + got_ref[i, p].astype(jnp.float32)
-        place = (me + order[p]) % tp
-        first = pl.multiple_of((place * heads + head) * HEAD_DIM, HEAD_DIM)
-        out_ref[:, pl.ds(first, HEAD_DIM)] = acc
+        place = (at_ref[0] + order[p]) % tp
+        sources = range(got_ref.shape[0])
+        put_sum(out_ref, got_ref, sources, p, (place * heads + head) * HEAD_DIM)
+
+
+def pair_total_kernel(at_ref, *refs, first, heads, order):
+    before_ref, out_ref = refs[-2:]
+    tp = len(order)
+    out_ref[...] = before_ref[...]
+    for n, got_ref in enumerate(refs[:-2]):
+        for p in range(tp):
+            place = (at_ref[0] + order[p]) % tp
+            sources = range(p // 2, got_ref.shape[0], 2)
+            put_sum(out_ref, got_ref, sources, p % 2, (place * heads + first + n) * HEAD_DIM)
 
 
 def attend_kernel(me_ref, *refs, head, extra, merge, tiles, far):
@@ -142,86 +171,108 @@
     ahead_ref = refs[7] if merge else None
     rest = refs[7 + merge + extra :]
     gqf_ref, gq_ref, dko_ref, dvo_ref, back_ref = rest[:5]
-    p_s, dp_s, ds_s, dk_s, dv_s, kt_s = rest[5:]
+    p_s, dp_s, po_s, dpo_s, dots_s, dk_s, dv_s, kt_s, qq_s, kk_s = rest[5:]
     step = pl.program_id(0)
     scale = HEAD_DIM**-0.5
     nkb = far // KB
     per = KB // (CAP * KEY_BLOCK)
+    parts = TQ // 128
+    nt = (((1,), (1,)), ((), ()))
+
+    def cut(t):
+        return slice(t * 128, (t + 1) * 128)
+
+    def ahead(first, behind):
+        q = q_ref[...]
+        g = g_ref[...]
+        lse = lse_ref[head : head + 1, :] * LOG2E
+        key_at = lax.broadcasted_iota(jnp.int32, (128, 128), 0)
+        row_at = lax.broadcasted_iota(jnp.int32, (128, 128), 1)
+        near = (key_at // KEY_BLOCK == row_at // KEY_BLOCK) & (key_at <= row_at)
+        dots = jnp.zeros((8, TQ), jnp.float32)
+        own_dots = []
+        for i in range(nkb):
+            rows = slice(i * KB, (i + 1) * KB)
+            if behind is not None:
+                behind(i)
+            keys = kv_ref[i * per : (i + 1) * per, 0:CAP].reshape(KB, HEAD_DIM)
+            values = kv_ref[i * per : (i + 1) * per, CAP : 2 * CAP].reshape(KB, HEAD_DIM)
+            s = lax.dot_general(keys, q, nt, preferred_element_type=jnp.float32)
+            dp = lax.dot_general(values, g, nt, preferred_element_type=jnp.float32)
+            shift = bias_ref[i * per * CAP : (i + 1) * per * CAP, :] - lse
+            s = (s * (scale * LOG2E)).reshape(per * CAP, KEY_BLOCK, TQ) + shift[:, None, :]
+            p = jnp.exp2(s).reshape(KB, TQ)
+            p_s[rows, :] = p
+            dp_s[rows, :] = dp
+            dv = jnp.dot(p.astype(jnp.bfloat16), g, preferred_element_type=jnp.float32)
+            dv_s[rows, :] = dv if first else dv_s[rows, :] + dv
+            dots = dots + (p * dp).reshape(KB // 8, 8, TQ).sum(axis=0)
+            if i < parts:
+                c = cut(i)
+                s = lax.dot_general(ko_ref[c, :], q[c], nt, preferred_element_type=jnp.float32)
+                dp = lax.dot_general(vo_ref[c, :], g[c], nt, preferred_element_type=jnp.float32)
+                p = jnp.exp2(jnp.where(near, s * (scale * LOG2E) - lse[:, c], NEG))
+                po_s[c, :] = p
+                dpo_s[c, :] = dp
+                own_dots.append(jnp.sum(p * dp, axis=0, keepdims=True))
+                dvo_ref[c, :] = jnp.dot(
+                    p.astype(jnp.bfloat16), g[c], preferred_element_type=jnp.float32
+                )
+        return jnp.sum(dots, axis=0, keepdims=True) + jnp.concatenate(own_dots, axis=1)
+
+    def second_half(first):
+        q = qq_s[...]
+        dots = dots_s[...]
+        held = []
+        own = []
+
+        def behind(i):
+            rows = slice(i * KB, (i + 1) * KB)
+            ds = (p_s[rows, :] * (dp_s[rows, :] - dots)).astype(jnp.bfloat16)
+            dk = jnp.dot(ds, q, preferred_element_type=jnp.float32)
+            dk_s[rows, :] = dk if first else dk_s[rows, :] + dk
+            part = jnp.dot(kt_s[:, rows], ds, preferred_element_type=jnp.float32)
+            held[:] = [held[0] + part] if held else [part]
+            if i < parts:
+                c = cut(i)
+                ds = (po_s[c, :] * (dpo_s[c, :] - dots[:, c])).astype(jnp.bfloat16)
+                dko_ref[c, :] = scale * jnp.dot(ds, q[c], preferred_element_type=jnp.float32)
+                own.append(jnp.dot(kk_s[c, :].T, ds, preferred_element_type=jnp.float32))
+
+        def finish():
+            for t in range(parts):
+                out = (scale * (held[0][:, cut(t)] + own[t])).T.astype(jnp.bfloat16)
+                gq_ref[cut(t), :] = out
+                gqf_ref[cut(t), :] = out
+
+        return behind, finish
+
+    def keep(dots):
+        dots_s[...] = dots
+        qq_s[...] = q_ref[...]
+        kk_s[...] = ko_ref[...]
 
     @pl.when(step == 0)
     def _():
-        dk_s[...] = jnp.zeros_like(dk_s)
-        dv_s[...] = jnp.zeros_like(dv_s)
         for i in range(nkb):
             keys = kv_ref[i * per : (i + 1) * per, 0:CAP].reshape(KB, HEAD_DIM)
-            kt_s[:, i * KB : (i + 1) * KB] = keys.astype(jnp.float32).T.astype(jnp.bfloat16)
-
-    q = q_ref[...]
-    g = g_ref[...]
-    lse = lse_ref[head : head + 1, :] * LOG2E
-    nt = (((1,), (1,)), ((), ()))
-
-    def ahead(i, dots):
-        keys = kv_ref[pl.ds(i * per, per), 0:CAP].reshape(KB, HEAD_DIM)
-        values = kv_ref[pl.ds(i * per, per), CAP : 2 * CAP].reshape(KB, HEAD_DIM)
-        s = lax.dot_general(keys, q, nt, preferred_element_type=jnp.float32)
-        dp = lax.dot_general(values, g, nt, preferred_element_type=jnp.float32)
-        shift = bias_ref[pl.ds(i * per * CAP, per * CAP), :] - lse
-        s = (s * (scale * LOG2E)).reshape(per * CAP, KEY_BLOCK, TQ) + shift[:, None, :]
-        p = jnp.exp2(s).reshape(KB, TQ)
-        rows = pl.ds(i * KB, KB)
-        p_s[rows, :] = p
-        dp_s[rows, :] = dp
-        dv_s[rows, :] += jnp.dot(
-            p.astype(jnp.bfloat16), g, preferred_element_type=jnp.float32
-        )
-        return dots + (p * dp).reshape(KB // 8, 8, TQ).sum(axis=0)
-
-    dots = jnp.zeros((8, TQ), jnp.float32)
-    for i in range(nkb):
-        dots = ahead(i, dots)
-    dots = jnp.sum(dots, axis=0, keepdims=True)
-    key_at = lax.broadcasted_iota(jnp.int32, (128, 128), 0)
-    row_at = lax.broadcasted_iota(jnp.int32, (128, 128), 1)
-    near = (key_at // KEY_BLOCK == row_at // KEY_BLOCK) & (key_at <= row_at)
-    own = []
-    own_dots = []
-    for t in range(TQ // 128):
-        cut = slice(t * 128, (t + 1) * 128)
-        s = lax.dot_general(ko_ref[cut, :], q[cut], nt, preferred_element_type=jnp.float32)
-        dp = lax.dot_general(vo_ref[cut, :], g[cut], nt, preferred_element_type=jnp.float32)
-        p = jnp.exp2(jnp.where(near, s * (scale * LOG2E) - lse[:, cut], NEG))
-        own.append((p, dp))
-        own_dots.append(jnp.sum(p * dp, axis=0, keepdims=True))
-        dvo_ref[cut, :] = jnp.dot(
-            p.astype(jnp.bfloat16), g[cut], preferred_element_type=jnp.float32
-        )
-    dots = dots + jnp.concatenate(own_dots, axis=1)
-
-    def behind(i, carry):
-        rows = pl.ds(i * KB, KB)
-        ds = (p_s[rows, :] * (dp_s[rows, :] - dots)).astype(jnp.bfloat16)
-        ds_s[rows, :] = ds
-        dk_s[rows, :] += jnp.dot(ds, q, preferred_element_type=jnp.float32)
-        part = jnp.dot(kt_s[:, rows], ds, preferred_element_type=jnp.float32)
-        return part if carry is None else carry + part
-
-    total = None
-    for i in range(nkb):
-        total = behind(i, total)
-    for t in range(TQ // 128):
-        cut = slice(t * 128, (t + 1) * 128)
-        p, dp = own[t]
-        ds = (p * (dp - dots[:, cut])).astype(jnp.bfloat16)
-        dko_ref[cut, :] = scale * jnp.dot(ds, q[cut], preferred_element_type=jnp.float32)
-        kt = ko_ref[cut, :].astype(jnp.float32).T.astype(jnp.bfloat16)
-        part = total[:, cut] + jnp.dot(kt, ds, preferred_element_type=jnp.float32)
-        out = (scale * part).T.astype(jnp.bfloat16)
-        gq_ref[cut, :] = out
-        gqf_ref[cut, :] = out
-
-    @pl.when(step == tiles - 1)
+            kt_s[:, i * KB : (i + 1) * KB] = keys.T
+        keep(ahead(True, None))
+        dk_s[...] = jnp.zeros_like(dk_s)
+
+    @pl.when((step > 0) & (step < tiles))
     def _():
+        behind, finish = second_half(False)
+        dots = ahead(False, behind)
+        finish()
+        keep(dots)
+
+    @pl.when(step == tiles)
+    def _():
+        behind, finish = second_half(False)
+        for i in range(nkb):
+            behind(i)
+        finish()
         shape = (far // (CAP * KEY_BLOCK), CAP, KEY_BLOCK, HEAD_DIM)
         dk = (scale * dk_s[...]).astype(jnp.bfloat16).reshape(shape)
         dv = dv_s[...].astype(jnp.bfloat16).reshape(shape)
@@ -272,7 +323,7 @@
 
 
 def params(**more):
-    return pltpu.CompilerParams(vmem_limit_bytes=60 * 1024 * 1024, **more)
+    return pltpu.CompilerParams(vmem_limit_bytes=VMEM_LIMIT, **more)
 
 
 def cost(flops, data=1 << 20):
@@ -345,7 +396,7 @@
     return pl.pallas_call(
         turn_kernel,
         grid=(cols // 256,),
-        out_shape=jax.ShapeDtypeStruct((cols, rows), x.dtype),
+        out_shape=pltpu.VMEM((cols, rows), x.dtype),
         in_specs=[pl.BlockSpec((rows, 256), lambda i: (0, i))],
         out_specs=pl.BlockSpec((256, rows), lambda i: (i, 0)),
         compiler_params=params(),
@@ -360,16 +411,25 @@
     tiles = rows // TQ
     spans = far_kv.shape[0]
     far = spans * CAP * KEY_BLOCK
-    column = pl.BlockSpec((TQ, HEAD_DIM), lambda i: (i, head))
-    alone = pl.BlockSpec((TQ, HEAD_DIM), lambda i: (i, 0))
+
+    def now(i):
+        return jnp.minimum(i, tiles - 1)
+
+    def then(i):
+        return jnp.maximum(i - 1, 0)
+
+    column = pl.BlockSpec((TQ, HEAD_DIM), lambda i: (now(i), head))
+    alone = pl.BlockSpec((TQ, HEAD_DIM), lambda i: (now(i), 0))
+    late_column = pl.BlockSpec((TQ, HEAD_DIM), lambda i: (then(i), head))
+    late = pl.BlockSpec((TQ, HEAD_DIM), lambda i: (then(i), 0))
     in_specs = [
         SMEM,
         column,
         column,
         column,
         column,
-        pl.BlockSpec((heads, TQ), lambda i: (0, i)),
-        pl.BlockSpec((None, spans * CAP, TQ), lambda i: (head, 0, i)),
+        pl.BlockSpec((heads, TQ), lambda i: (0, now(i))),
+        pl.BlockSpec((None, spans * CAP, TQ), lambda i: (head, 0, now(i))),
         slotted(spans, 0),
     ]
     args = [me, q, g, k, v, lse, bias, far_kv]
@@ -386,9 +446,9 @@
         functools.partial(
             attend_kernel, head=head, extra=len(aliases), merge=int(merge), tiles=tiles, far=far
         ),
-        grid=(tiles,),
+        grid=(tiles + 1,),
         in_specs=in_specs,
-        out_specs=[column, alone, alone, alone, slotted(spans, 0)],
+        out_specs=[late_column, late, late, alone, slotted(spans, 0)],
         out_shape=[
             jax.ShapeDtypeStruct((rows, width), jnp.bfloat16),
             jax.ShapeDtypeStruct((rows, HEAD_DIM), jnp.bfloat16),
@@ -399,10 +459,14 @@
         scratch_shapes=[
             pltpu.VMEM((far, TQ), jnp.float32),
             pltpu.VMEM((far, TQ), jnp.float32),
-            pltpu.VMEM((far, TQ), jnp.bfloat16),
+            pltpu.VMEM((TQ, 128), jnp.float32),
+            pltpu.VMEM((TQ, 128), jnp.float32),
+            pltpu.VMEM((1, TQ), jnp.float32),
             pltpu.VMEM((far, HEAD_DIM), jnp.float32),
             pltpu.VMEM((far, HEAD_DIM), jnp.float32),
             pltpu.VMEM((HEAD_DIM, far), jnp.bfloat16),
+            pltpu.VMEM((TQ, HEAD_DIM), jnp.bfloat16),
+            pltpu.VMEM((TQ, HEAD_DIM), jnp.bfloat16),
         ],
         input_output_aliases=aliases,
         cost_estimate=cost(10 * rows * far * HEAD_DIM, 8 << 20),
@@ -410,27 +474,36 @@
     )(*args)
 
 
-def weigh(xt, shards, buffer, spans, slot, slots):
+def weigh(me, xt, shards, buffer, spans, slot, slots, halves=False):
     cols, rows = xt.shape
     tall = pl.BlockSpec((rows, HEAD_DIM), lambda i: (0, 0))
-    tall_rows = 256
-    in_specs = [pl.BlockSpec((tall_rows, rows), lambda i: (i, 0))] + [tall] * len(shards)
-    args = [xt, *shards]
+    in_specs = [SMEM, VMEM] + [tall] * len(shards)
+    args = [me, pltpu.with_memory_space_constraint(xt, pltpu.VMEM), *shards]
     aliases = {}
     if buffer is not None:
         aliases[len(args)] = 0
         in_specs.append(ANY)
         args.append(buffer)
     owned = cols // spans
-    per = tall_rows // owned
-    return pl.pallas_call(
-        functools.partial(weight_kernel, shards=len(shards)),
-        grid=(cols // tall_rows,),
+    per = WEIGH_ROWS // owned
+    if halves:
+        shape = (spans, len(shards) // 2, owned, HEAD_DIM)
+        out_spec = pl.BlockSpec((per,) + shape[1:], lambda i: (i, 0, 0, 0))
+        out_specs = [out_spec] * 2
+        out_shape = [jax.ShapeDtypeStruct(shape, jnp.bfloat16)] * 2
+    else:
+        out_specs = pl.BlockSpec(
+            (per, None, len(shards), owned, HEAD_DIM), lambda i: (i, slot, 0, 0, 0)
+        )
+        out_shape = jax.ShapeDtypeStruct(five(spans, slots), jnp.bfloat16)
+    return pl.pallas_call(
+        functools.partial(
+            weight_kernel, shards=len(shards), steps=cols // WEIGH_ROWS, halves=halves
+        ),
+        grid=(cols // WEIGH_ROWS,),
         in_specs=in_specs,
-        out_specs=pl.BlockSpec(
-            (per, None, len(shards), owned, HEAD_DIM), lambda i: (i, slot, 0, 0, 0)
-        ),
-        out_shape=jax.ShapeDtypeStruct(five(spans, slots), jnp.bfloat16),
+        out_specs=out_specs,
+        out_shape=out_shape,
         input_output_aliases=aliases,
         compiler_params=params(),
         cost_estimate=cost(2 * cols * rows * len(shards) * HEAD_DIM, 8 << 20),
@@ -438,28 +511,61 @@
     )(*args)
 
 
-def total(place, got, slot, buffer, head, heads, order):
-    spans = got.shape[0]
-    args = [place, got]
-    in_specs = [SMEM, slotted(spans, slot)]
-    aliases = {}
+def join(keep, got, buffer, slot, slots):
+    spans = keep.shape[0]
+    whole = pl.BlockSpec(keep.shape, lambda i: (0, 0, 0, 0))
+    args, in_specs, aliases = [keep, got], [whole, whole], {}
     if buffer is not None:
         aliases = {2: 0}
-        in_specs.append(VMEM)
         args.append(buffer)
+        in_specs.append(ANY)
+    return pl.pallas_call(
+        join_kernel,
+        grid=(1,),
+        in_specs=in_specs,
+        out_specs=pl.BlockSpec(
+            (spans, None) + keep.shape[1:], lambda i: (0, slot, 0, 0, 0)
+        ),
+        out_shape=jax.ShapeDtypeStruct((spans, slots) + keep.shape[1:], jnp.bfloat16),
+        input_output_aliases=aliases,
+        compiler_params=params(),
+        cost_estimate=cost(1 << 24),
+        name="join",
+    )(*args)
+
+
+def total(place, got, slot, head, heads, order):
     return pl.pallas_call(
         functools.partial(total_kernel, head=head, heads=heads, order=order),
         grid=(1,),
-        in_specs=in_specs,
+        in_specs=[SMEM, slotted(got.shape[0], slot)],
         out_specs=VMEM,
         out_shape=jax.ShapeDtypeStruct(
             (KEY_BLOCK, len(order) * heads * HEAD_DIM), jnp.float32
         ),
-        input_output_aliases=aliases,
         compiler_params=params(),
         cost_estimate=cost(1 << 24),
         name="total",
-    )(*args)
+    )(place, got)
+
+
+def pair_total(place, got, buffer, first, heads, order):
+    spans, count = got.shape[:2]
+    specs = [
+        pl.BlockSpec((spans, None) + got.shape[2:], lambda i, n=n: (0, n, 0, 0, 0))
+        for n in range(count)
+    ]
+    return pl.pallas_call(
+        functools.partial(pair_total_kernel, first=first, heads=heads, order=order),
+        grid=(1,),
+        in_specs=[SMEM, *specs, VMEM],
+        out_specs=VMEM,
+        out_shape=jax.ShapeDtypeStruct(buffer.shape, buffer.dtype),
+        input_output_aliases={1 + count: 0},
+        compiler_params=params(),
+        cost_estimate=cost(1 << 24),
+        name="pairtotal",
+    )(place, *[got] * count, buffer)
 
 
 def land(head, me, tab, home, dko, dvo, full, rows, width):
@@ -524,8 +630,8 @@
         across = shift(gq, 2, tp)
         return gq, right, left, across
 
-    def product(shards, buffer, slot, slots):
-        return weigh(xt, shards, buffer, spans, slot, slots)
+    def swapped(x):
+        return lax.ppermute(x, "kv", [(i, i ^ 1) for i in range(spans)])
 
     far1 = exchange(send1)
     gq_full, gq, *own0, out = attention(0, far0, None, send2, 1)
@@ -533,18 +639,23 @@
     far2 = exchange(out)
     gq_full, gq, *own1, out = attention(1, far1, gq_full, None, 2)
     shards1 = gathered(gq)
-    home1 = exchange(product(shards0, out, 1, 2))
-    gq_full, gq, *own2, out = attention(2, far2, gq_full, None, 2)
+    out = weigh(me, xt, shards0, out, spans, 1, 2)
+    home1 = exchange(out)
+    gq_full, gq, *own2, out = attention(2, far2, gq_full, None, 1)
     shards2 = gathered(gq)
-    home2 = exchange(product(shards1, out, 1, 2))
-    last = exchange(product(shards2, None, 0, 1))
+    home2 = exchange(out)
+    joined = None
+    for h, shards in ((1, shards1), (2, shards2)):
+        keep, give = weigh(me, xt, shards, None, spans, 0, 1, halves=True)
+        got = swapped(give)
+        joined = join(keep, got, joined, h - 1, heads - 1)
+    last = exchange(joined)
 
     full = None
     for h, (home, own) in enumerate(((far2, own0), (home1, own1), (home2, own2))):
         full = land(h, me, tab, home, *own, full, rows, width)
-    grad_weight = None
-    for h, (got, slot) in enumerate(((home1, 1), (home2, 1), (last, 0))):
-        grad_weight = total(place, got, slot, grad_weight, h, heads, order)
+    grad_weight = total(place, home1, 1, 0, heads, order)
+    grad_weight = pair_total(place, last, grad_weight, 1, heads, order)
     return gq_full, full[0], full[1], grad_weight
 
 

time: 221 us -> 236 us (1.068)
  waiting for transfers between devices: 45.7 us -> 71.5 us
  Pallas kernels: 110 us -> 101 us
    ppermute x9, waiting for transfers between devices: 28.7 us -> 56.6 us  [shift(): return lax.ppermute(x, 'tp', [(i, (i + by) % tp) for i in range(tp)])]
    pallas_call x3, Pallas kernels: 55.9 us -> 50.3 us  [attend(): pl.pallas_call(functools.partial(attend_kernel, head=head, extra=len(alia...]
    pallas_call x3 -> x1, Pallas kernels: 6.22 us -> 2.06 us  [total(): pl.pallas_call(functools.partial(total_kernel, head=head, heads=heads, or...]
    unnamed x30 -> x20, local copies, waits for them, and re-layouts: 6.85 us -> 7.77 us
    pallas_call x4 -> x7, Pallas kernels: 23.6 us -> 24.5 us  [the longest x3 14.5 us: weigh(): pl.pallas_call(functools.partial(weight_kernel, shards=len(shards), steps...]
  transfers between devices with their start and end apart: 15 -> 17, of which waited for: 6 -> 9; matrix products, arithmetic and copies ran while one was open for 0% -> 0% of each run, Pallas kernels for 46% -> 34%
where the time goes in v3:
time: 236 us; the launch traced here: 234 us
  Pallas kernels  101 us (43%)
  waiting for transfers between devices  71.5 us (30%)
  starting transfers between devices  52.2 us (22%)
  local copies, waits for them, and re-layouts  7.77 us (3%)
    ppermute x9, waiting for transfers between devices, shift(): return lax.ppermute(x, 'tp', [(i, (i + by) % tp) for i in range(tp)])  56.6 us
    pallas_call x3, Pallas kernels, attend(): pl.pallas_call(functools.partial(attend_kernel, head=head, extra=len(alia...  50.3 us
    all_to_all x6, starting transfers between devices, exchange(): return lax.all_to_all(x, 'kv', split_axis=0, concat_axis=0, tiled=True)  41.7 us
    all_to_all x6, waiting for transfers between devices, exchange(): return lax.all_to_all(x, 'kv', split_axis=0, concat_axis=0, tiled=True)  15 us
    pallas_call x3, Pallas kernels, weigh(): pl.pallas_call(functools.partial(weight_kernel, shards=len(shards), steps...  14.5 us
    pallas_call x3, Pallas kernels, land(): pl.pallas_call(functools.partial(land_kernel, head=head, spans=spans), gr...  14 us
    ppermute x9, starting transfers between devices, shift(): return lax.ppermute(x, 'tp', [(i, (i + by) % tp) for i in range(tp)])  10.5 us
    unnamed x20, local copies, waits for them, and re-layouts  7.77 us
  transfers between devices with their start and end apart: 17, of which 9 were waited for; matrix products, arithmetic and copies ran while one was open for 0% of the time, Pallas kernels for 34%

profile of v3, /device:TPU:0, one launch (start us, length us, event | category | flops | bytes accessed | tf_op | source)
XLA Modules:
  0.0 233.7 jit_solution(10431539831738243624)
XLA Ops:
  0.6 3.6 %first.1 = (bf16[32,1,4,32,128]{4,3,2,1,0:T(8,128)(2,1)}, s32[8,128]{1,0:T(8,128)}) custom-call(s32[1]{0:T(128)} %bitcast.me_ref, s32[3,12,2048]{2,1,0:T(8,128)} %bitcast.9, bf16[64,32,384]{2,1,0:T(8,128)(2,1)} %bitcast.5, bf16[64,32,384]{2,1,0:T(8,128)(2,1)} %bitcast.7), custom_call_target="tpu_custom_call" | custom-call | flops 67108864 | bytes 1048576 | tf_op jit(solution)/shard_map/first/pallas_call | solution.py:346
  4.2 8.5 %all-to-all-start = ((bf16[32,1,4,32,128]{4,3,2,1,0:T(8,128)(2,1)}), bf16[32,1,4,32,128]{4,3,2,1,0:T(8,128)(2,1)S(1)}, u32[]{:S(2)}, u32[]{:S(2)}) async-start(bf16[32,1,4,32,128]{4,3,2,1,0:T(8,128)(2,1)} %get-tuple-element.33), calls=%async_computation | async-start | bytes 2097152 | tf_op jit(solution)/shard_map/all_to_all | solution.py:595
  12.7 3.9 %pack.1 = (bf16[32,1,4,32,128]{4,3,2,1,0:T(8,128)(2,1)}, bf16[32,1,4,32,128]{4,3,2,1,0:T(8,128)(2,1)}) custom-call(s32[8,128]{1,0:T(8,128)} %get-tuple-element.34.tab_ref, bf16[64,32,384]{2,1,0:T(8,128)(2,1)} %bitcast.6, bf16[64,32,384]{2,1,0:T(8,128)(2,1)} %bitcast.8), custom_call_target="tpu_custom_call" | custom-call | flops 67108864 | bytes 1048576 | tf_op jit(solution)/shard_map/pack/pallas_call | solution.py:369
  16.5 13.3 %all-to-all-done.refs_6_ = bf16[32,1,4,32,128]{4,3,2,1,0:T(8,128)(2,1)S(1)} async-done(((bf16[32,1,4,32,128]{4,3,2,1,0:T(8,128)(2,1)}), bf16[32,1,4,32,128]{4,3,2,1,0:T(8,128)(2,1)S(1)}, u32[]{:S(2)}, u32[]{:S(2)}) %all-to-all-start) | async-done | bytes 1048608 | tf_op jit(solution)/shard_map/all_to_all | solution.py:595
  29.9 3.9 %all-to-all-start.2 = ((bf16[32,1,4,32,128]{4,3,2,1,0:T(8,128)(2,1)}), bf16[32,1,4,32,128]{4,3,2,1,0:T(8,128)(2,1)S(1)}, u32[]{:S(2)}, u32[]{:S(2)}) async-start(bf16[32,1,4,32,128]{4,3,2,1,0:T(8,128)(2,1)} %get-tuple-element.37), calls=%async_computation.2 | async-start | bytes 2097152 | tf_op jit(solution)/shard_map/all_to_all | solution.py:595
  33.8 3.1 %mask.1.refs_5_ = f32[3,64,2048]{2,1,0:T(8,128)} custom-call(s32[1]{0:T(128)} %bitcast.me_ref, s32[3,12,2048]{2,1,0:T(8,128)} %bitcast.10), custom_call_target="tpu_custom_call" | custom-call | flops 67108864 | bytes 1048576 | tf_op jit(solution)/shard_map/mask/pallas_call | solution.py:383
  36.9 17.1 %shard_map.102 = (bf16[2048,384]{1,0:T(8,128)(2,1)}, bf16[2048,128]{1,0:T(8,128)(2,1)}, f32[2048,128]{1,0:T(8,128)}, f32[2048,128]{1,0:T(8,128)}, bf16[32,1,4,32,128]{4,3,2,1,0:T(8,128)(2,1)}) custom-call(s32[1]{0:T(128)} %bitcast.me_ref, bf16[2048,384]{1,0:T(8,128)(2,1)} %refs_0_.5, bf16[2048,384]{1,0:T(8,128)(2,1)} %refs_1_.5, bf16[2048,384]{1,0:T(8,128)(2,1)} %refs_2_.5, ...), custom_call_target="tpu_custom_call" | custom-call | flops 5368709120 | bytes 8388608 | tf_op jit(solution)/shard_map/pallas_call | solution.py:445
  54.0 0.0 all-to-all-done.2.refs_6_
  54.0 7.6 %all-to-all-start.1 = ((bf16[32,1,4,32,128]{4,3,2,1,0:T(8,128)(2,1)}), bf16[32,1,4,32,128]{4,3,2,1,0:T(8,128)(2,1)S(1)}, u32[]{:S(2)}, u32[]{:S(2)}) async-start(bf16[32,1,4,32,128]{4,3,2,1,0:T(8,128)(2,1)} %get-tuple-element.36), calls=%async_computation.1 | async-start | bytes 2097152 | tf_op jit(solution)/shard_map/all_to_all | solution.py:595
  61.6 16.5 %shard_map.103 = (bf16[2048,384]{1,0:T(8,128)(2,1)}, bf16[2048,128]{1,0:T(8,128)(2,1)}, f32[2048,128]{1,0:T(8,128)}, f32[2048,128]{1,0:T(8,128)}, bf16[32,2,4,32,128]{4,3,2,1,0:T(8,128)(2,1)}) custom-call(s32[1]{0:T(128)} %bitcast.me_ref, bf16[2048,384]{1,0:T(8,128)(2,1)} %refs_0_.5, bf16[2048,384]{1,0:T(8,128)(2,1)} %refs_1_.5, ...), custom_call_target="tpu_custom_call", output_to_operand_aliasing={{0}: (8, {})} | custom-call | flops 5368709120 | bytes 8388608 | tf_op jit(solution)/shard_map/pallas_call | solution.py:445
  78.2 0.5 all-to-all-done.1.refs_6_.back_ref
  78.7 1.0 copy-done.3
  79.6 16.8 %shard_map.104 = (bf16[2048,384]{1,0:T(8,128)(2,1)}, bf16[2048,128]{1,0:T(8,128)(2,1)}, f32[2048,128]{1,0:T(8,128)}, f32[2048,128]{1,0:T(8,128)}, bf16[32,1,4,32,128]{4,3,2,1,0:T(8,128)(2,1)}) custom-call(s32[1]{0:T(128)} %bitcast.me_ref, bf16[2048,384]{1,0:T(8,128)(2,1)} %refs_0_.5, bf16[2048,384]{1,0:T(8,128)(2,1)} %refs_1_.5, ...), custom_call_target="tpu_custom_call", output_to_operand_aliasing={{0}: (8, {})} | custom-call | flops 5368709120 | bytes 8388608 | tf_op jit(solution)/shard_map/pallas_call | solution.py:445
  96.4 6.9 %all-to-all-start.3 = ((bf16[32,1,4,32,128]{4,3,2,1,0:T(8,128)(2,1)}), bf16[32,1,4,32,128]{4,3,2,1,0:T(8,128)(2,1)}, u32[]{:S(2)}, u32[]{:S(2)}) async-start(bf16[32,1,4,32,128]{4,3,2,1,0:T(8,128)(2,1)} %get-tuple-element.41), calls=%async_computation.3 | async-start | bytes 2097152 | tf_op jit(solution)/shard_map/all_to_all | solution.py:595
  103.3 2.8 %collective-permute-start = (bf16[2048,128]{1,0:T(8,128)(2,1)}, bf16[2048,128]{1,0:T(8,128)(2,1)}, u32[]{:S(2)}, u32[]{:S(2)}) collective-permute-start(bf16[2048,128]{1,0:T(8,128)(2,1)} %get-tuple-element.44.rest_0_), channel_id=1, source_target_pairs={{0,3},{1,0},{2,1},{3,2},{4,7},{5,4},{6,5},{7,6},{8,11},{9,8},{10,9... | collective-permute-start | bytes 1572872 | tf_op jit(solution)/shard_map/ppermute | solution.py:599
  106.1 2.3 collective-permute-start.2
  108.4 3.6 %turn.1.xt_ref = bf16[1024,2048]{1,0:T(8,128)(2,1)S(1)} custom-call(bf16[2048,1024]{1,0:T(8,128)(2,1)} %x_ref.1), custom_call_target="tpu_custom_call" | custom-call | flops 67108864 | bytes 1048576 | tf_op jit(solution)/shard_map/turn/pallas_call | solution.py:396
  112.0 17.2 %collective-permute-done.rest_1_ = bf16[2048,128]{1,0:T(8,128)(2,1)} collective-permute-done((bf16[2048,128]{1,0:T(8,128)(2,1)}, bf16[2048,128]{1,0:T(8,128)(2,1)}, u32[]{:S(2)}, u32[]{:S(2)}) %collective-permute-start) | collective-permute-done | bytes 524320 | tf_op jit(solution)/shard_map/ppermute | solution.py:599
  129.3 3.4 %collective-permute-done.1.rest_2_ = bf16[2048,128]{1,0:T(8,128)(2,1)} collective-permute-done((bf16[2048,128]{1,0:T(8,128)(2,1)}, bf16[2048,128]{1,0:T(8,128)(2,1)}, u32[]{:S(2)}, u32[]{:S(2)}) %collective-permute-start.1) | collective-permute-done | bytes 524320 | tf_op jit(solution)/shard_map/ppermute | solution.py:599
  132.6 0.0 collective-permute-done.2.rest_3_
  132.6 4.8 %weigh.3 = bf16[32,2,4,32,128]{4,3,2,1,0:T(8,128)(2,1)} custom-call(s32[1]{0:T(128)} %bitcast.me_ref, bf16[1024,2048]{1,0:T(8,128)(2,1)S(1)} %turn.1.xt_ref, bf16[2048,128]{1,0:T(8,128)(2,1)} %get-tuple-element.44.rest_0_, bf16[2048,128]{1,0:T(8,128)(2,1)} %collective-permute-done.rest_1_, ...), custom_call_target="tpu_custom_call", output_to_operand_aliasing={{}: (6, {})} | custom-call | flops 2147483648 | bytes 8388608 | tf_op jit(solution)/shard_map/weigh/pallas_call | solution.py:499
  137.5 2.0 copy-done
  139.5 0.0 all-to-all-done.3.back_ref
  139.5 7.5 %all-to-all-start.4 = ((bf16[32,2,4,32,128]{4,3,2,1,0:T(8,128)(2,1)}), bf16[32,2,4,32,128]{4,3,2,1,0:T(8,128)(2,1)}, u32[]{:S(2)}, u32[]{:S(2)}) async-start(bf16[32,2,4,32,128]{4,3,2,1,0:T(8,128)(2,1)} %weigh.3), calls=%async_computation.4 | async-start | bytes 4194304 | tf_op jit(solution)/shard_map/all_to_all | solution.py:595
  147.0 0.4 collective-permute-start.7
  147.3 1.7 collective-permute-start.8
  149.1 0.6 collective-permute-start.9
  149.7 2.1 collective-permute-start.3
  151.7 10.1 %collective-permute-done.7.rest_1_ = bf16[2048,128]{1,0:T(8,128)(2,1)S(1)} collective-permute-done((bf16[2048,128]{1,0:T(8,128)(2,1)S(1)}, bf16[2048,128]{1,0:T(8,128)(2,1)S(1)}, u32[]{:S(2)}, u32[]{:S(2)}) %collective-permute-start.7) | collective-permute-done | bytes 524320 | tf_op jit(solution)/shard_map/ppermute | solution.py:599
  161.8 0.6 collective-permute-start.5
  162.4 12.1 %collective-permute-done.8.rest_2_ = bf16[2048,128]{1,0:T(8,128)(2,1)S(1)} collective-permute-done((bf16[2048,128]{1,0:T(8,128)(2,1)S(1)}, bf16[2048,128]{1,0:T(8,128)(2,1)S(1)}, u32[]{:S(2)}, u32[]{:S(2)}) %collective-permute-start.8) | collective-permute-done | bytes 524320 | tf_op jit(solution)/shard_map/ppermute | solution.py:599
  174.6 0.8 copy-done.9
  175.4 2.2 copy-done.1
  177.6 4.9 %weigh.5 = (bf16[32,2,32,128]{3,2,1,0:T(8,128)(2,1)}, bf16[32,2,32,128]{3,2,1,0:T(8,128)(2,1)}) custom-call(s32[1]{0:T(128)} %bitcast.me_ref, bf16[1024,2048]{1,0:T(8,128)(2,1)S(1)} %copy-done.1, bf16[2048,128]{1,0:T(8,128)(2,1)} %get-tuple-element.59.rest_0_, bf16[2048,128]{1,0:T(8,128)(2,1)} %copy-done.8, bf16[2048,128]{1,0:T(8,128)(2,1)} %copy-done.9, ...), custom_call_target="tpu_custom_call" | custom-call | flops 2147483648 | bytes 8388608 | tf_op jit(solution)/shard_map/weigh/pallas_call | solution.py:499
  182.5 2.0 collective-permute-done.3.rest_1_
  184.5 11.7 %collective-permute-done.4.rest_2_ = bf16[2048,128]{1,0:T(8,128)(2,1)} collective-permute-done((bf16[2048,128]{1,0:T(8,128)(2,1)}, bf16[2048,128]{1,0:T(8,128)(2,1)}, u32[]{:S(2)}, u32[]{:S(2)}) %collective-permute-start.4) | collective-permute-done | bytes 524320 | tf_op jit(solution)/shard_map/ppermute | solution.py:599
  196.2 4.8 %weigh.4 = (bf16[32,2,32,128]{3,2,1,0:T(8,128)(2,1)}, bf16[32,2,32,128]{3,2,1,0:T(8,128)(2,1)}) custom-call(s32[1]{0:T(128)} %bitcast.me_ref, bf16[1024,2048]{1,0:T(8,128)(2,1)S(1)} %copy-done.1, bf16[2048,128]{1,0:T(8,128)(2,1)} %get-tuple-element.56.rest_0_, bf16[2048,128]{1,0:T(8,128)(2,1)} %collective-permute-done.3.rest_1_, ...), custom_call_target="tpu_custom_call" | custom-call | flops 2147483648 | bytes 8388608 | tf_op jit(solution)/shard_map/weigh/pallas_call | solution.py:499
  201.0 2.1 join.2.rest_0_
  203.2 0.8 copy-done.6
  204.0 2.1 join.3
  206.1 7.3 %all-to-all-start.5 = ((bf16[32,2,2,32,128]{4,3,2,1,0:T(8,128)(2,1)}), bf16[32,2,2,32,128]{4,3,2,1,0:T(8,128)(2,1)S(1)}, u32[]{:S(2)}, u32[]{:S(2)}) async-start(bf16[32,2,2,32,128]{4,3,2,1,0:T(8,128)(2,1)} %join.3), calls=%async_computation.5 | async-start | bytes 2097152 | tf_op jit(solution)/shard_map/all_to_all | solution.py:595
  213.4 4.7 %shard_map.105 = (f32[2048,384]{1,0:T(8,128)}, f32[2048,384]{1,0:T(8,128)}) custom-call(s32[1]{0:T(128)} %bitcast.me_ref, s32[8,128]{1,0:T(8,128)} %get-tuple-element.34.tab_ref, bf16[32,1,4,32,128]{4,3,2,1,0:T(8,128)(2,1)} %copy-done.3, f32[2048,128]{1,0:T(8,128)} %get-tuple-element.48.dko_ref, f32[2048,128]{1,0:T(8,128)} %get-tuple-element.49.dvo_ref), custom_call_target="tpu_custom_call" | custom-call | flops 16777216 | bytes 1048576 | tf_op jit(solution)/shard_map/pallas_call | solution.py:582
  218.1 2.1 total.1.refs_2_
  220.2 4.7 %shard_map.106 = (f32[2048,384]{1,0:T(8,128)}, f32[2048,384]{1,0:T(8,128)}) custom-call(s32[1]{0:T(128)} %bitcast.me_ref, s32[8,128]{1,0:T(8,128)} %get-tuple-element.34.tab_ref, bf16[32,2,4,32,128]{4,3,2,1,0:T(8,128)(2,1)} %all-to-all-done.4.back_ref.got_ref, f32[2048,128]{1,0:T(8,128)} %get-tuple-element.46.dko_ref, ...), custom_call_target="tpu_custom_call", output_to_operand_aliasing={{0}: (5, {}), {1}: (6, {})} | custom-call | flops 16777216 | bytes 1048576 | tf_op jit(solution)/shard_map/pallas_call | solution.py:582
  224.9 4.7 %shard_map.107 = (f32[2048,384]{1,0:T(8,128)}, f32[2048,384]{1,0:T(8,128)}) custom-call(s32[1]{0:T(128)} %bitcast.me_ref, s32[8,128]{1,0:T(8,128)} %get-tuple-element.34.tab_ref, bf16[32,1,4,32,128]{4,3,2,1,0:T(8,128)(2,1)} %all-to-all-done.3.back_ref, f32[2048,128]{1,0:T(8,128)} %get-tuple-element.42.dko_ref, ...), custom_call_target="tpu_custom_call", output_to_operand_aliasing={{0}: (5, {}), {1}: (6, {})} | custom-call | flops 16777216 | bytes 1048576 | tf_op jit(solution)/shard_map/pallas_call | solution.py:582
  229.5 1.1 all-to-all-done.5.refs_0_.refs_1_
  230.7 1.0 copy-done.2
  231.7 2.1 pairtotal.1
  (23 shorter events, 0.0 us)
Async XLA Ops:
  4.2 25.7 %all-to-all-start = ((bf16[32,1,4,32,128]{4,3,2,1,0:T(8,128)(2,1)}), bf16[32,1,4,32,128]{4,3,2,1,0:T(8,128)(2,1)S(1)}, u32[]{:S(2)}, u32[]{:S(2)}) async-start(bf16[32,1,4,32,128]{4,3,2,1,0:T(8,128)(2,1)} %get-tuple-element.33), calls=%async_computation | async-start | bytes 2097152 | tf_op jit(solution)/shard_map/all_to_all | solution.py:595
  29.9 7.0 %copy-start.5 = (bf16[32,1,4,32,128]{4,3,2,1,0:T(8,128)(2,1)}, bf16[32,1,4,32,128]{4,3,2,1,0:T(8,128)(2,1)S(1)}, u32[]{:S(2)}) copy-start(bf16[32,1,4,32,128]{4,3,2,1,0:T(8,128)(2,1)S(1)} %all-to-all-done.refs_6_) | copy-start | bytes 3145732
  29.9 24.1 %all-to-all-start.2 = ((bf16[32,1,4,32,128]{4,3,2,1,0:T(8,128)(2,1)}), bf16[32,1,4,32,128]{4,3,2,1,0:T(8,128)(2,1)S(1)}, u32[]{:S(2)}, u32[]{:S(2)}) async-start(bf16[32,1,4,32,128]{4,3,2,1,0:T(8,128)(2,1)} %get-tuple-element.37), calls=%async_computation.2 | async-start | bytes 2097152 | tf_op jit(solution)/shard_map/all_to_all | solution.py:595
  54.0 7.6 %copy-start.4 = (bf16[32,1,4,32,128]{4,3,2,1,0:T(8,128)(2,1)}, bf16[32,1,4,32,128]{4,3,2,1,0:T(8,128)(2,1)S(1)}, u32[]{:S(2)}) copy-start(bf16[32,1,4,32,128]{4,3,2,1,0:T(8,128)(2,1)S(1)} %all-to-all-done.2.refs_6_) | copy-start | bytes 3145732
  54.0 24.7 %all-to-all-start.1 = ((bf16[32,1,4,32,128]{4,3,2,1,0:T(8,128)(2,1)}), bf16[32,1,4,32,128]{4,3,2,1,0:T(8,128)(2,1)S(1)}, u32[]{:S(2)}, u32[]{:S(2)}) async-start(bf16[32,1,4,32,128]{4,3,2,1,0:T(8,128)(2,1)} %get-tuple-element.36), calls=%async_computation.1 | async-start | bytes 2097152 | tf_op jit(solution)/shard_map/all_to_all | solution.py:595
  78.7 1.0 copy-start.3
  96.4 43.1 %all-to-all-start.3 = ((bf16[32,1,4,32,128]{4,3,2,1,0:T(8,128)(2,1)}), bf16[32,1,4,32,128]{4,3,2,1,0:T(8,128)(2,1)}, u32[]{:S(2)}, u32[]{:S(2)}) async-start(bf16[32,1,4,32,128]{4,3,2,1,0:T(8,128)(2,1)} %get-tuple-element.41), calls=%async_computation.3 | async-start | bytes 2097152 | tf_op jit(solution)/shard_map/all_to_all | solution.py:595
  103.3 26.0 %collective-permute-start = (bf16[2048,128]{1,0:T(8,128)(2,1)}, bf16[2048,128]{1,0:T(8,128)(2,1)}, u32[]{:S(2)}, u32[]{:S(2)}) collective-permute-start(bf16[2048,128]{1,0:T(8,128)(2,1)} %get-tuple-element.44.rest_0_), channel_id=1, source_target_pairs={{0,3},{1,0},{2,1},{3,2},{4,7},{5,4},{6,5},{7,6},{8,11},{9,8},{10,9... | collective-permute-start | bytes 1572872 | tf_op jit(solution)/shard_map/ppermute | solution.py:599
  106.1 26.5 %collective-permute-start.1 = (bf16[2048,128]{1,0:T(8,128)(2,1)}, bf16[2048,128]{1,0:T(8,128)(2,1)}, u32[]{:S(2)}, u32[]{:S(2)}) collective-permute-start(bf16[2048,128]{1,0:T(8,128)(2,1)} %get-tuple-element.44.rest_0_), channel_id=1, source_target_pairs={{0,1},{1,2},{2,3},{3,0},{4,5},{5,6},{6,7},{7,4},{8,9},{9,10},{10,1... | collective-permute-start | bytes 1572872 | tf_op jit(solution)/shard_map/ppermute | solution.py:599
  106.1 26.5 %collective-permute-start.2 = (bf16[2048,128]{1,0:T(8,128)(2,1)}, bf16[2048,128]{1,0:T(8,128)(2,1)}, u32[]{:S(2)}, u32[]{:S(2)}) collective-permute-start(bf16[2048,128]{1,0:T(8,128)(2,1)} %get-tuple-element.44.rest_0_), channel_id=1, source_target_pairs={{0,2},{1,3},{2,0},{3,1},{4,6},{5,7},{6,4},{7,5},{8,10},{9,11},{10,... | collective-permute-start | bytes 1572872 | tf_op jit(solution)/shard_map/ppermute | solution.py:599
  137.5 2.0 copy-start
  139.5 7.5 %copy-start.7 = (bf16[2048,128]{1,0:T(8,128)(2,1)S(1)}, bf16[2048,128]{1,0:T(8,128)(2,1)}, u32[]{:S(2)}) copy-start(bf16[2048,128]{1,0:T(8,128)(2,1)} %get-tuple-element.59.rest_0_) | copy-start | bytes 1572868
  139.5 66.6 %all-to-all-start.4 = ((bf16[32,2,4,32,128]{4,3,2,1,0:T(8,128)(2,1)}), bf16[32,2,4,32,128]{4,3,2,1,0:T(8,128)(2,1)}, u32[]{:S(2)}, u32[]{:S(2)}) async-start(bf16[32,2,4,32,128]{4,3,2,1,0:T(8,128)(2,1)} %weigh.3), calls=%async_computation.4 | async-start | bytes 4194304 | tf_op jit(solution)/shard_map/all_to_all | solution.py:595
  147.0 14.9 %collective-permute-start.7 = (bf16[2048,128]{1,0:T(8,128)(2,1)S(1)}, bf16[2048,128]{1,0:T(8,128)(2,1)S(1)}, u32[]{:S(2)}, u32[]{:S(2)}) collective-permute-start(bf16[2048,128]{1,0:T(8,128)(2,1)S(1)} %copy-done.7), channel_id=1, source_target_pairs={{0,3},{1,0},{2,1},{3,2},{4,7},{5,4},{6,5},{7,6},{8,11},{9,8},{10,9... | collective-permute-start | bytes 1572872 | tf_op jit(solution)/shard_map/ppermute | solution.py:599
  147.3 27.2 %collective-permute-start.8 = (bf16[2048,128]{1,0:T(8,128)(2,1)S(1)}, bf16[2048,128]{1,0:T(8,128)(2,1)S(1)}, u32[]{:S(2)}, u32[]{:S(2)}) collective-permute-start(bf16[2048,128]{1,0:T(8,128)(2,1)S(1)} %copy-done.7), channel_id=1, source_target_pairs={{0,1},{1,2},{2,3},{3,0},{4,5},{5,6},{6,7},{7,4},{8,9},{9,10},{10,1... | collective-permute-start | bytes 1572872 | tf_op jit(solution)/shard_map/ppermute | solution.py:599
  149.1 26.3 %collective-permute-start.9 = (bf16[2048,128]{1,0:T(8,128)(2,1)S(1)}, bf16[2048,128]{1,0:T(8,128)(2,1)}, u32[]{:S(2)}, u32[]{:S(2)}) collective-permute-start(bf16[2048,128]{1,0:T(8,128)(2,1)S(1)} %copy-done.7), channel_id=1, source_target_pairs={{0,2},{1,3},{2,0},{3,1},{4,6},{5,7},{6,4},{7,5},{8,10},{9,11},{10,... | collective-permute-start | bytes 1572872 | tf_op jit(solution)/shard_map/ppermute | solution.py:599
  149.7 34.8 %collective-permute-start.3 = (bf16[2048,128]{1,0:T(8,128)(2,1)}, bf16[2048,128]{1,0:T(8,128)(2,1)}, u32[]{:S(2)}, u32[]{:S(2)}) collective-permute-start(bf16[2048,128]{1,0:T(8,128)(2,1)} %get-tuple-element.56.rest_0_), channel_id=1, source_target_pairs={{0,3},{1,0},{2,1},{3,2},{4,7},{5,4},{6,5},{7,6},{8,11},{9,8},{10,9... | collective-permute-start | bytes 1572872 | tf_op jit(solution)/shard_map/ppermute | solution.py:599
  151.7 44.4 %collective-permute-start.4 = (bf16[2048,128]{1,0:T(8,128)(2,1)}, bf16[2048,128]{1,0:T(8,128)(2,1)}, u32[]{:S(2)}, u32[]{:S(2)}) collective-permute-start(bf16[2048,128]{1,0:T(8,128)(2,1)} %get-tuple-element.56.rest_0_), channel_id=1, source_target_pairs={{0,1},{1,2},{2,3},{3,0},{4,5},{5,6},{6,7},{7,4},{8,9},{9,10},{10,1... | collective-permute-start | bytes 1572872 | tf_op jit(solution)/shard_map/ppermute | solution.py:599
  161.8 12.8 %copy-start.8 = (bf16[2048,128]{1,0:T(8,128)(2,1)}, bf16[2048,128]{1,0:T(8,128)(2,1)S(1)}, u32[]{:S(2)}) copy-start(bf16[2048,128]{1,0:T(8,128)(2,1)S(1)} %collective-permute-done.7.rest_1_) | copy-start | bytes 1572868
  161.8 34.3 %collective-permute-start.5 = (bf16[2048,128]{1,0:T(8,128)(2,1)}, bf16[2048,128]{1,0:T(8,128)(2,1)}, u32[]{:S(2)}, u32[]{:S(2)}) collective-permute-start(bf16[2048,128]{1,0:T(8,128)(2,1)} %get-tuple-element.56.rest_0_), channel_id=1, source_target_pairs={{0,2},{1,3},{2,0},{3,1},{4,6},{5,7},{6,4},{7,5},{8,10},{9,11},{10,... | collective-permute-start | bytes 1572872 | tf_op jit(solution)/shard_map/ppermute | solution.py:599
  174.6 0.8 copy-start.9
  175.4 2.2 copy-start.1
  182.5 18.6 %collective-permute-start.10 = (bf16[32,2,32,128]{3,2,1,0:T(8,128)(2,1)}, bf16[32,2,32,128]{3,2,1,0:T(8,128)(2,1)}, u32[]{:S(2)}, u32[]{:S(2)}) collective-permute-start(bf16[32,2,32,128]{3,2,1,0:T(8,128)(2,1)} %get-tuple-element.61), channel_id=1, source_target_pairs={{0,4},{4,0},{8,12},{12,8},{16,20},{20,16},{24,28},{28,24},{32,36},... | collective-permute-start | bytes 1572872 | tf_op jit(solution)/shard_map/ppermute | solution.py:634
  201.0 2.1 collective-permute-start.6
  203.2 0.8 copy-start.6
  206.1 24.6 %all-to-all-start.5 = ((bf16[32,2,2,32,128]{4,3,2,1,0:T(8,128)(2,1)}), bf16[32,2,2,32,128]{4,3,2,1,0:T(8,128)(2,1)S(1)}, u32[]{:S(2)}, u32[]{:S(2)}) async-start(bf16[32,2,2,32,128]{4,3,2,1,0:T(8,128)(2,1)} %join.3), calls=%async_computation.5 | async-start | bytes 2097152 | tf_op jit(solution)/shard_map/all_to_all | solution.py:595
  230.7 1.0 copy-start.2

commit v4 on v3

--- a/solution.py
+++ b/solution.py
@@ -155,15 +155,13 @@
         put_sum(out_ref, got_ref, sources, p, (place * heads + head) * HEAD_DIM)
 
 
-def pair_total_kernel(at_ref, *refs, first, heads, order):
-    before_ref, out_ref = refs[-2:]
+def pair_total_kernel(at_ref, got_ref, before_ref, out_ref, *, head, heads, order):
     tp = len(order)
     out_ref[...] = before_ref[...]
-    for n, got_ref in enumerate(refs[:-2]):
-        for p in range(tp):
-            place = (at_ref[0] + order[p]) % tp
-            sources = range(p // 2, got_ref.shape[0], 2)
-            put_sum(out_ref, got_ref, sources, p % 2, (place * heads + first + n) * HEAD_DIM)
+    for p in range(tp):
+        place = (at_ref[0] + order[p]) % tp
+        sources = range(p // 2, got_ref.shape[0], 2)
+        put_sum(out_ref, got_ref, sources, p % 2, (place * heads + head) * HEAD_DIM)
 
 
 def attend_kernel(me_ref, *refs, head, extra, merge, tiles, far):
@@ -340,6 +338,10 @@
     )
 
 
+def back_spec(spans, shape):
+    return slotted(spans, 0) if len(shape) == 5 else tiles_of(spans, 2 * CAP, 0)
+
+
 def pack_first(me, ids, key_blocks, value_blocks, heads, spans):
     blocks = key_blocks.shape[0]
     column = pl.BlockSpec((blocks, KEY_BLOCK, HEAD_DIM), lambda i: (0, 0, 0))
@@ -405,7 +407,7 @@
     )(x)
 
 
-def attend(head, me, q, g, k, v, lse, bias, far_kv, gq_full, ahead, slots):
+def attend(head, me, q, g, k, v, lse, bias, far_kv, gq_full, ahead, back_shape):
     rows, width = q.shape
     heads = lse.shape[0]
     tiles = rows // TQ
@@ -448,13 +450,13 @@
         ),
         grid=(tiles + 1,),
         in_specs=in_specs,
-        out_specs=[late_column, late, late, alone, slotted(spans, 0)],
+        out_specs=[late_column, late, late, alone, back_spec(spans, back_shape)],
         out_shape=[
             jax.ShapeDtypeStruct((rows, width), jnp.bfloat16),
             jax.ShapeDtypeStruct((rows, HEAD_DIM), jnp.bfloat16),
             jax.ShapeDtypeStruct((rows, HEAD_DIM), jnp.float32),
             jax.ShapeDtypeStruct((rows, HEAD_DIM), jnp.float32),
-            jax.ShapeDtypeStruct(five(spans, slots), jnp.bfloat16),
+            jax.ShapeDtypeStruct(back_shape, jnp.bfloat16),
         ],
         scratch_shapes=[
             pltpu.VMEM((far, TQ), jnp.float32),
@@ -511,22 +513,25 @@
     )(*args)
 
 
-def join(keep, got, buffer, slot, slots):
-    spans = keep.shape[0]
-    whole = pl.BlockSpec(keep.shape, lambda i: (0, 0, 0, 0))
-    args, in_specs, aliases = [keep, got], [whole, whole], {}
+def tiles_of(spans, count, at):
+    return pl.BlockSpec((spans, count, KEY_BLOCK, HEAD_DIM), lambda i: (0, at, 0, 0))
+
+
+def join(keep, got, buffer, at):
+    spans, count = keep.shape[:2]
+    args, in_specs, aliases = [keep, got], [tiles_of(spans, count, 0)] * 2, {}
+    out_shape = jax.ShapeDtypeStruct(keep.shape, keep.dtype)
     if buffer is not None:
         aliases = {2: 0}
         args.append(buffer)
         in_specs.append(ANY)
+        out_shape = jax.ShapeDtypeStruct(buffer.shape, buffer.dtype)
     return pl.pallas_call(
         join_kernel,
         grid=(1,),
         in_specs=in_specs,
-        out_specs=pl.BlockSpec(
-            (spans, None) + keep.shape[1:], lambda i: (0, slot, 0, 0, 0)
-        ),
-        out_shape=jax.ShapeDtypeStruct((spans, slots) + keep.shape[1:], jnp.bfloat16),
+        out_specs=tiles_of(spans, count, at),
+        out_shape=out_shape,
         input_output_aliases=aliases,
         compiler_params=params(),
         cost_estimate=cost(1 << 24),
@@ -549,30 +554,25 @@
     )(place, got)
 
 
-def pair_total(place, got, buffer, first, heads, order):
-    spans, count = got.shape[:2]
-    specs = [
-        pl.BlockSpec((spans, None) + got.shape[2:], lambda i, n=n: (0, n, 0, 0, 0))
-        for n in range(count)
-    ]
-    return pl.pallas_call(
-        functools.partial(pair_total_kernel, first=first, heads=heads, order=order),
+def pair_total(place, got, at, buffer, head, heads, order):
+    return pl.pallas_call(
+        functools.partial(pair_total_kernel, head=head, heads=heads, order=order),
         grid=(1,),
-        in_specs=[SMEM, *specs, VMEM],
+        in_specs=[SMEM, tiles_of(got.shape[0], len(order) // 2, at), VMEM],
         out_specs=VMEM,
         out_shape=jax.ShapeDtypeStruct(buffer.shape, buffer.dtype),
-        input_output_aliases={1 + count: 0},
+        input_output_aliases={2: 0},
         compiler_params=params(),
         cost_estimate=cost(1 << 24),
         name="pairtotal",
-    )(place, *[got] * count, buffer)
+    )(place, got, buffer)
 
 
 def land(head, me, tab, home, dko, dvo, full, rows, width):
     spans = home.shape[0]
     column = pl.BlockSpec((rows, HEAD_DIM), lambda i: (0, head))
     alone = pl.BlockSpec((rows, HEAD_DIM), lambda i: (0, 0))
-    in_specs = [SMEM, SMEM, slotted(spans, 0), alone, alone]
+    in_specs = [SMEM, SMEM, back_spec(spans, home.shape), alone, alone]
     args = [me, tab, home, dko, dvo]
     aliases = {}
     if full is not None:
@@ -618,10 +618,10 @@
     xt = turn(layer_input)
     bias = mask(me, ids, spans, blocks)
 
-    def attention(h, far, gq_full, ahead, slots):
+    def attention(h, far, gq_full, ahead, back_shape):
         return attend(
             h, me, query_rows, cotangent, key_rows, value_rows, log_sums, bias, far,
-            gq_full, ahead, slots,
+            gq_full, ahead, back_shape,
         )
 
     def gathered(gq):
@@ -634,28 +634,31 @@
         return lax.ppermute(x, "kv", [(i, i ^ 1) for i in range(spans)])
 
     far1 = exchange(send1)
-    gq_full, gq, *own0, out = attention(0, far0, None, send2, 1)
+    gq_full, gq, *own0, out = attention(0, far0, None, send2, five(spans))
     shards0 = gathered(gq)
     far2 = exchange(out)
-    gq_full, gq, *own1, out = attention(1, far1, gq_full, None, 2)
+    gq_full, gq, *own1, out = attention(1, far1, gq_full, None, five(spans, 2))
     shards1 = gathered(gq)
     out = weigh(me, xt, shards0, out, spans, 1, 2)
     home1 = exchange(out)
-    gq_full, gq, *own2, out = attention(2, far2, gq_full, None, 1)
+    room = (spans, 2 * CAP + tp // 2, KEY_BLOCK, HEAD_DIM)
+    gq_full, gq, *own2, out = attention(2, far2, gq_full, None, room)
     shards2 = gathered(gq)
-    home2 = exchange(out)
-    joined = None
-    for h, shards in ((1, shards1), (2, shards2)):
+
+    def shared(shards, buffer, at):
         keep, give = weigh(me, xt, shards, None, spans, 0, 1, halves=True)
         got = swapped(give)
-        joined = join(keep, got, joined, h - 1, heads - 1)
-    last = exchange(joined)
+        return join(keep, got, buffer, at)
+
+    home2 = exchange(shared(shards1, out, 2))
+    last = exchange(shared(shards2, None, 0))
 
     full = None
     for h, (home, own) in enumerate(((far2, own0), (home1, own1), (home2, own2))):
         full = land(h, me, tab, home, *own, full, rows, width)
     grad_weight = total(place, home1, 1, 0, heads, order)
-    grad_weight = pair_total(place, last, grad_weight, 1, heads, order)
+    grad_weight = pair_total(place, home2, 2, grad_weight, 1, heads, order)
+    grad_weight = pair_total(place, last, 0, grad_weight, 2, heads, order)
     return gq_full, full[0], full[1], grad_weight
 
 

time: 236 us -> 235 us (level)
  waiting for transfers between devices: 71.5 us -> 65.6 us
  Pallas kernels: 101 us -> 104 us
    ppermute x9, waiting for transfers between devices: 56.6 us -> 50.2 us  [shift(): return lax.ppermute(x, 'tp', [(i, (i + by) % tp) for i in range(tp)])]
    pallas_call x3 -> x4, Pallas kernels: 6.35 us -> 8.01 us  [the longest x2 4.31 us: join(): pl.pallas_call(join_kernel, grid=(1,), in_specs=in_specs, out_specs=tiles...]
    unnamed x20 -> x28, local copies, waits for them, and re-layouts: 7.77 us -> 8.41 us
  transfers between devices with their start and end apart: 17 -> 17, of which waited for: 9 -> 7; matrix products, arithmetic and copies ran while one was open for 0% -> 0% of each run, Pallas kernels for 34% -> 41%
where the time goes in v4:
time: 235 us; the launch traced here: 233 us
  Pallas kernels  104 us (44%)
  waiting for transfers between devices  65.6 us (28%)
  starting transfers between devices  53.4 us (23%)
  local copies, waits for them, and re-layouts  8.41 us (4%)
    pallas_call x3, Pallas kernels, attend(): pl.pallas_call(functools.partial(attend_kernel, head=head, extra=len(alia...  51.6 us
    ppermute x9, waiting for transfers between devices, shift(): return lax.ppermute(x, 'tp', [(i, (i + by) % tp) for i in range(tp)])  50.2 us
    all_to_all x6, starting transfers between devices, exchange(): return lax.all_to_all(x, 'kv', split_axis=0, concat_axis=0, tiled=True)  42.3 us
    pallas_call x3, Pallas kernels, weigh(): pl.pallas_call(functools.partial(weight_kernel, shards=len(shards), steps...  14.6 us
    pallas_call x3, Pallas kernels, land(): pl.pallas_call(functools.partial(land_kernel, head=head, spans=spans), gr...  14 us
    all_to_all x6, waiting for transfers between devices, exchange(): return lax.all_to_all(x, 'kv', split_axis=0, concat_axis=0, tiled=True)  13.3 us
    ppermute x9, starting transfers between devices, shift(): return lax.ppermute(x, 'tp', [(i, (i + by) % tp) for i in range(tp)])  11.1 us
    unnamed x28, local copies, waits for them, and re-layouts  8.41 us
  transfers between devices with their start and end apart: 17, of which 7 were waited for; matrix products, arithmetic and copies ran while one was open for 0% of the time, Pallas kernels for 41%

profile of v4, /device:TPU:0, one launch (start us, length us, event | category | flops | bytes accessed | tf_op | source)
XLA Modules:
  0.0 232.6 jit_solution(7929974616197049897)
XLA Ops:
  0.6 3.6 %first.1 = (bf16[32,1,4,32,128]{4,3,2,1,0:T(8,128)(2,1)}, s32[8,128]{1,0:T(8,128)}) custom-call(s32[1]{0:T(128)} %bitcast.me_ref, s32[3,12,2048]{2,1,0:T(8,128)} %bitcast.9, bf16[64,32,384]{2,1,0:T(8,128)(2,1)} %bitcast.5, bf16[64,32,384]{2,1,0:T(8,128)(2,1)} %bitcast.7), custom_call_target="tpu_custom_call" | custom-call | flops 67108864 | bytes 1048576 | tf_op jit(solution)/shard_map/first/pallas_call | solution.py:348
  4.2 8.5 %all-to-all-start = ((bf16[32,1,4,32,128]{4,3,2,1,0:T(8,128)(2,1)}), bf16[32,1,4,32,128]{4,3,2,1,0:T(8,128)(2,1)S(1)}, u32[]{:S(2)}, u32[]{:S(2)}) async-start(bf16[32,1,4,32,128]{4,3,2,1,0:T(8,128)(2,1)} %get-tuple-element.33), calls=%async_computation | async-start | bytes 2097152 | tf_op jit(solution)/shard_map/all_to_all | solution.py:595
  12.7 3.9 %pack.1 = (bf16[32,1,4,32,128]{4,3,2,1,0:T(8,128)(2,1)}, bf16[32,1,4,32,128]{4,3,2,1,0:T(8,128)(2,1)}) custom-call(s32[8,128]{1,0:T(8,128)} %get-tuple-element.34.tab_ref, bf16[64,32,384]{2,1,0:T(8,128)(2,1)} %bitcast.6, bf16[64,32,384]{2,1,0:T(8,128)(2,1)} %bitcast.8), custom_call_target="tpu_custom_call" | custom-call | flops 67108864 | bytes 1048576 | tf_op jit(solution)/shard_map/pack/pallas_call | solution.py:371
  16.6 13.3 %all-to-all-done.refs_6_ = bf16[32,1,4,32,128]{4,3,2,1,0:T(8,128)(2,1)S(1)} async-done(((bf16[32,1,4,32,128]{4,3,2,1,0:T(8,128)(2,1)}), bf16[32,1,4,32,128]{4,3,2,1,0:T(8,128)(2,1)S(1)}, u32[]{:S(2)}, u32[]{:S(2)}) %all-to-all-start) | async-done | bytes 1048608 | tf_op jit(solution)/shard_map/all_to_all | solution.py:595
  29.9 3.9 %all-to-all-start.2 = ((bf16[32,1,4,32,128]{4,3,2,1,0:T(8,128)(2,1)}), bf16[32,1,4,32,128]{4,3,2,1,0:T(8,128)(2,1)S(1)}, u32[]{:S(2)}, u32[]{:S(2)}) async-start(bf16[32,1,4,32,128]{4,3,2,1,0:T(8,128)(2,1)} %get-tuple-element.37), calls=%async_computation.2 | async-start | bytes 2097152 | tf_op jit(solution)/shard_map/all_to_all | solution.py:595
  33.8 3.1 %mask.1.refs_5_ = f32[3,64,2048]{2,1,0:T(8,128)} custom-call(s32[1]{0:T(128)} %bitcast.me_ref, s32[3,12,2048]{2,1,0:T(8,128)} %bitcast.10), custom_call_target="tpu_custom_call" | custom-call | flops 67108864 | bytes 1048576 | tf_op jit(solution)/shard_map/mask/pallas_call | solution.py:385
  36.9 17.1 %shard_map.102 = (bf16[2048,384]{1,0:T(8,128)(2,1)}, bf16[2048,128]{1,0:T(8,128)(2,1)}, f32[2048,128]{1,0:T(8,128)}, f32[2048,128]{1,0:T(8,128)}, bf16[32,1,4,32,128]{4,3,2,1,0:T(8,128)(2,1)}) custom-call(s32[1]{0:T(128)} %bitcast.me_ref, bf16[2048,384]{1,0:T(8,128)(2,1)} %refs_0_.5, bf16[2048,384]{1,0:T(8,128)(2,1)} %refs_1_.5, bf16[2048,384]{1,0:T(8,128)(2,1)} %refs_2_.5, ...), custom_call_target="tpu_custom_call" | custom-call | flops 5368709120 | bytes 8388608 | tf_op jit(solution)/shard_map/pallas_call | solution.py:447
  54.0 7.6 %all-to-all-start.1 = ((bf16[32,1,4,32,128]{4,3,2,1,0:T(8,128)(2,1)}), bf16[32,1,4,32,128]{4,3,2,1,0:T(8,128)(2,1)}, u32[]{:S(2)}, u32[]{:S(2)}) async-start(bf16[32,1,4,32,128]{4,3,2,1,0:T(8,128)(2,1)} %get-tuple-element.36), calls=%async_computation.1 | async-start | bytes 2097152 | tf_op jit(solution)/shard_map/all_to_all | solution.py:595
  61.6 2.8 %collective-permute-start.4 = (bf16[2048,128]{1,0:T(8,128)(2,1)}, bf16[2048,128]{1,0:T(8,128)(2,1)}, u32[]{:S(2)}, u32[]{:S(2)}) collective-permute-start(bf16[2048,128]{1,0:T(8,128)(2,1)} %get-tuple-element.47.rest_0_), channel_id=1, source_target_pairs={{0,3},{1,0},{2,1},{3,2},{4,7},{5,4},{6,5},{7,6},{8,11},{9,8},{10,9... | collective-permute-start | bytes 1572872 | tf_op jit(solution)/shard_map/ppermute | solution.py:599
  64.4 2.3 collective-permute-start.6
  66.7 3.6 %turn.1.xt_ref = bf16[1024,2048]{1,0:T(8,128)(2,1)S(1)} custom-call(bf16[2048,1024]{1,0:T(8,128)(2,1)} %x_ref.1), custom_call_target="tpu_custom_call" | custom-call | flops 67108864 | bytes 1048576 | tf_op jit(solution)/shard_map/turn/pallas_call | solution.py:398
  70.3 18.0 %shard_map.103 = (bf16[2048,384]{1,0:T(8,128)(2,1)}, bf16[2048,128]{1,0:T(8,128)(2,1)}, f32[2048,128]{1,0:T(8,128)}, f32[2048,128]{1,0:T(8,128)}, bf16[32,2,4,32,128]{4,3,2,1,0:T(8,128)(2,1)}) custom-call(s32[1]{0:T(128)} %bitcast.me_ref, bf16[2048,384]{1,0:T(8,128)(2,1)} %refs_0_.5, bf16[2048,384]{1,0:T(8,128)(2,1)} %refs_1_.5, ...), custom_call_target="tpu_custom_call", output_to_operand_aliasing={{0}: (8, {})} | custom-call | flops 5368709120 | bytes 8388608 | tf_op jit(solution)/shard_map/pallas_call | solution.py:447
  88.3 2.6 %collective-permute-done.5.rest_2_ = bf16[2048,128]{1,0:T(8,128)(2,1)} collective-permute-done((bf16[2048,128]{1,0:T(8,128)(2,1)}, bf16[2048,128]{1,0:T(8,128)(2,1)}, u32[]{:S(2)}, u32[]{:S(2)}) %collective-permute-start.5) | collective-permute-done | bytes 524320 | tf_op jit(solution)/shard_map/ppermute | solution.py:599
  90.9 4.9 %weigh.4 = bf16[32,2,4,32,128]{4,3,2,1,0:T(8,128)(2,1)} custom-call(s32[1]{0:T(128)} %bitcast.me_ref, bf16[1024,2048]{1,0:T(8,128)(2,1)S(1)} %turn.1.xt_ref, bf16[2048,128]{1,0:T(8,128)(2,1)} %get-tuple-element.47.rest_0_, bf16[2048,128]{1,0:T(8,128)(2,1)} %collective-permute-done.4.rest_1_, ...), custom_call_target="tpu_custom_call", output_to_operand_aliasing={{}: (6, {})} | custom-call | flops 2147483648 | bytes 8388608 | tf_op jit(solution)/shard_map/weigh/pallas_call | solution.py:501
  95.8 7.5 %all-to-all-start.4 = ((bf16[32,2,4,32,128]{4,3,2,1,0:T(8,128)(2,1)}), bf16[32,2,4,32,128]{4,3,2,1,0:T(8,128)(2,1)}, u32[]{:S(2)}, u32[]{:S(2)}) async-start(bf16[32,2,4,32,128]{4,3,2,1,0:T(8,128)(2,1)} %weigh.4), calls=%async_computation.4 | async-start | bytes 4194304 | tf_op jit(solution)/shard_map/all_to_all | solution.py:595
  103.3 0.4 collective-permute-start
  103.7 1.7 collective-permute-start.1
  105.4 0.6 collective-permute-start.2
  106.0 12.2 %collective-permute-done.rest_1_ = bf16[2048,128]{1,0:T(8,128)(2,1)S(1)} collective-permute-done((bf16[2048,128]{1,0:T(8,128)(2,1)S(1)}, bf16[2048,128]{1,0:T(8,128)(2,1)S(1)}, u32[]{:S(2)}, u32[]{:S(2)}) %collective-permute-start) | collective-permute-done | bytes 524320 | tf_op jit(solution)/shard_map/ppermute | solution.py:599
  118.2 11.8 %collective-permute-done.1.rest_2_ = bf16[2048,128]{1,0:T(8,128)(2,1)S(1)} collective-permute-done((bf16[2048,128]{1,0:T(8,128)(2,1)S(1)}, bf16[2048,128]{1,0:T(8,128)(2,1)S(1)}, u32[]{:S(2)}, u32[]{:S(2)}) %collective-permute-start.1) | collective-permute-done | bytes 524320 | tf_op jit(solution)/shard_map/ppermute | solution.py:599
  129.9 0.8 copy-done.13
  130.8 2.2 copy-done.1
  133.0 4.9 %weigh.3 = (bf16[32,2,32,128]{3,2,1,0:T(8,128)(2,1)}, bf16[32,2,32,128]{3,2,1,0:T(8,128)(2,1)}) custom-call(s32[1]{0:T(128)} %bitcast.me_ref, bf16[1024,2048]{1,0:T(8,128)(2,1)S(1)} %copy-done.1, bf16[2048,128]{1,0:T(8,128)(2,1)} %get-tuple-element.41.rest_0_, bf16[2048,128]{1,0:T(8,128)(2,1)} %copy-done.11, bf16[2048,128]{1,0:T(8,128)(2,1)} %copy-done.13, ...), custom_call_target="tpu_custom_call" | custom-call | flops 2147483648 | bytes 8388608 | tf_op jit(solution)/shard_map/weigh/pallas_call | solution.py:501
  137.8 0.0 collective-permute-start.3
  137.8 16.5 %shard_map.104 = (bf16[2048,384]{1,0:T(8,128)(2,1)}, bf16[2048,128]{1,0:T(8,128)(2,1)}, f32[2048,128]{1,0:T(8,128)}, f32[2048,128]{1,0:T(8,128)}, bf16[32,6,32,128]{3,2,1,0:T(8,128)(2,1)}) custom-call(s32[1]{0:T(128)} %bitcast.me_ref, bf16[2048,384]{1,0:T(8,128)(2,1)} %refs_0_.5, bf16[2048,384]{1,0:T(8,128)(2,1)} %refs_1_.5, ...), custom_call_target="tpu_custom_call", output_to_operand_aliasing={{0}: (8, {})} | custom-call | flops 5368709120 | bytes 8388608 | tf_op jit(solution)/shard_map/pallas_call | solution.py:447
  154.4 0.0 copy-start.7
  154.4 0.8 copy-done.7
  155.2 2.2 join.2
  157.4 7.6 %all-to-all-start.3 = ((bf16[32,6,32,128]{3,2,1,0:T(8,128)(2,1)}), bf16[32,6,32,128]{3,2,1,0:T(8,128)(2,1)}, u32[]{:S(2)}, u32[]{:S(2)}) async-start(bf16[32,6,32,128]{3,2,1,0:T(8,128)(2,1)} %join.2), calls=%async_computation.3 | async-start | bytes 3145728 | tf_op jit(solution)/shard_map/all_to_all | solution.py:595
  165.0 0.7 collective-permute-start.7
  165.7 1.4 collective-permute-start.8
  167.1 1.2 collective-permute-start.9
  168.3 11.6 %collective-permute-done.7.rest_1_ = bf16[2048,128]{1,0:T(8,128)(2,1)S(1)} collective-permute-done((bf16[2048,128]{1,0:T(8,128)(2,1)S(1)}, bf16[2048,128]{1,0:T(8,128)(2,1)S(1)}, u32[]{:S(2)}, u32[]{:S(2)}) %collective-permute-start.7) | collective-permute-done | bytes 524320 | tf_op jit(solution)/shard_map/ppermute | solution.py:599
  179.9 12.1 %collective-permute-done.8.rest_2_ = bf16[2048,128]{1,0:T(8,128)(2,1)S(1)} collective-permute-done((bf16[2048,128]{1,0:T(8,128)(2,1)S(1)}, bf16[2048,128]{1,0:T(8,128)(2,1)S(1)}, u32[]{:S(2)}, u32[]{:S(2)}) %collective-permute-start.8) | collective-permute-done | bytes 524320 | tf_op jit(solution)/shard_map/ppermute | solution.py:599
  191.9 0.8 copy-done.12
  192.7 2.2 copy-done.2
  194.9 4.8 %weigh.5 = (bf16[32,2,32,128]{3,2,1,0:T(8,128)(2,1)}, bf16[32,2,32,128]{3,2,1,0:T(8,128)(2,1)}) custom-call(s32[1]{0:T(128)} %bitcast.me_ref, bf16[1024,2048]{1,0:T(8,128)(2,1)S(1)} %copy-done.2, bf16[2048,128]{1,0:T(8,128)(2,1)} %get-tuple-element.59.rest_0_, bf16[2048,128]{1,0:T(8,128)(2,1)} %copy-done.10, bf16[2048,128]{1,0:T(8,128)(2,1)} %copy-done.12, ...), custom_call_target="tpu_custom_call" | custom-call | flops 2147483648 | bytes 8388608 | tf_op jit(solution)/shard_map/weigh/pallas_call | solution.py:501
  199.8 2.1 collective-permute-done.10.got_ref
  201.9 0.8 copy-done.6
  202.7 2.1 join.3
  204.8 7.2 %all-to-all-start.5 = ((bf16[32,2,32,128]{3,2,1,0:T(8,128)(2,1)}), bf16[32,2,32,128]{3,2,1,0:T(8,128)(2,1)S(1)}, u32[]{:S(2)}, u32[]{:S(2)}) async-start(bf16[32,2,32,128]{3,2,1,0:T(8,128)(2,1)} %join.3), calls=%async_computation.5 | async-start | bytes 1048576 | tf_op jit(solution)/shard_map/all_to_all | solution.py:595
  212.0 4.7 %shard_map.105 = (f32[2048,384]{1,0:T(8,128)}, f32[2048,384]{1,0:T(8,128)}) custom-call(s32[1]{0:T(128)} %bitcast.me_ref, s32[8,128]{1,0:T(8,128)} %get-tuple-element.34.tab_ref, bf16[32,1,4,32,128]{4,3,2,1,0:T(8,128)(2,1)} %all-to-all-done.1.refs_6_.back_ref, f32[2048,128]{1,0:T(8,128)} %get-tuple-element.51.dko_ref, f32[2048,128]{1,0:T(8,128)} %get-tuple-element.52.dvo_ref), custom_call_target="tpu_custom_call" | custom-call | flops 16777216 | bytes 1048576 | tf_op jit(solution)/shard_map/pallas_call | solution.py:582
  216.7 2.1 total.1.before_ref
  218.8 4.7 %shard_map.106 = (f32[2048,384]{1,0:T(8,128)}, f32[2048,384]{1,0:T(8,128)}) custom-call(s32[1]{0:T(128)} %bitcast.me_ref, s32[8,128]{1,0:T(8,128)} %get-tuple-element.34.tab_ref, bf16[32,2,4,32,128]{4,3,2,1,0:T(8,128)(2,1)} %all-to-all-done.4.back_ref.got_ref, f32[2048,128]{1,0:T(8,128)} %get-tuple-element.49.dko_ref, ...), custom_call_target="tpu_custom_call", output_to_operand_aliasing={{0}: (5, {}), {1}: (6, {})} | custom-call | flops 16777216 | bytes 1048576 | tf_op jit(solution)/shard_map/pallas_call | solution.py:582
  223.5 1.8 pairtotal.2.before_ref
  225.3 0.8 copy-done.3
  226.1 1.8 pairtotal.3
  228.0 4.7 %shard_map.107 = (f32[2048,384]{1,0:T(8,128)}, f32[2048,384]{1,0:T(8,128)}) custom-call(s32[1]{0:T(128)} %bitcast.me_ref, s32[8,128]{1,0:T(8,128)} %get-tuple-element.34.tab_ref, bf16[32,6,32,128]{3,2,1,0:T(8,128)(2,1)} %all-to-all-done.3.back_ref.got_ref, f32[2048,128]{1,0:T(8,128)} %get-tuple-element.45.dko_ref, ...), custom_call_target="tpu_custom_call", output_to_operand_aliasing={{0}: (5, {}), {1}: (6, {})} | custom-call | flops 16777216 | bytes 1048576 | tf_op jit(solution)/shard_map/pallas_call | solution.py:582
  (32 shorter events, 0.1 us)
Async XLA Ops:
  4.2 25.7 %all-to-all-start = ((bf16[32,1,4,32,128]{4,3,2,1,0:T(8,128)(2,1)}), bf16[32,1,4,32,128]{4,3,2,1,0:T(8,128)(2,1)S(1)}, u32[]{:S(2)}, u32[]{:S(2)}) async-start(bf16[32,1,4,32,128]{4,3,2,1,0:T(8,128)(2,1)} %get-tuple-element.33), calls=%async_computation | async-start | bytes 2097152 | tf_op jit(solution)/shard_map/all_to_all | solution.py:595
  29.9 7.0 %copy-start.5 = (bf16[32,1,4,32,128]{4,3,2,1,0:T(8,128)(2,1)}, bf16[32,1,4,32,128]{4,3,2,1,0:T(8,128)(2,1)S(1)}, u32[]{:S(2)}) copy-start(bf16[32,1,4,32,128]{4,3,2,1,0:T(8,128)(2,1)S(1)} %all-to-all-done.refs_6_) | copy-start | bytes 3145732
  29.9 24.1 %all-to-all-start.2 = ((bf16[32,1,4,32,128]{4,3,2,1,0:T(8,128)(2,1)}), bf16[32,1,4,32,128]{4,3,2,1,0:T(8,128)(2,1)S(1)}, u32[]{:S(2)}, u32[]{:S(2)}) async-start(bf16[32,1,4,32,128]{4,3,2,1,0:T(8,128)(2,1)} %get-tuple-element.37), calls=%async_computation.2 | async-start | bytes 2097152 | tf_op jit(solution)/shard_map/all_to_all | solution.py:595
  54.0 10.4 %copy-start.4 = (bf16[32,1,4,32,128]{4,3,2,1,0:T(8,128)(2,1)}, bf16[32,1,4,32,128]{4,3,2,1,0:T(8,128)(2,1)S(1)}, u32[]{:S(2)}) copy-start(bf16[32,1,4,32,128]{4,3,2,1,0:T(8,128)(2,1)S(1)} %all-to-all-done.2.refs_6_) | copy-start | bytes 3145732
  54.0 41.8 %all-to-all-start.1 = ((bf16[32,1,4,32,128]{4,3,2,1,0:T(8,128)(2,1)}), bf16[32,1,4,32,128]{4,3,2,1,0:T(8,128)(2,1)}, u32[]{:S(2)}, u32[]{:S(2)}) async-start(bf16[32,1,4,32,128]{4,3,2,1,0:T(8,128)(2,1)} %get-tuple-element.36), calls=%async_computation.1 | async-start | bytes 2097152 | tf_op jit(solution)/shard_map/all_to_all | solution.py:595
  61.6 26.7 %collective-permute-start.4 = (bf16[2048,128]{1,0:T(8,128)(2,1)}, bf16[2048,128]{1,0:T(8,128)(2,1)}, u32[]{:S(2)}, u32[]{:S(2)}) collective-permute-start(bf16[2048,128]{1,0:T(8,128)(2,1)} %get-tuple-element.47.rest_0_), channel_id=1, source_target_pairs={{0,3},{1,0},{2,1},{3,2},{4,7},{5,4},{6,5},{7,6},{8,11},{9,8},{10,9... | collective-permute-start | bytes 1572872 | tf_op jit(solution)/shard_map/ppermute | solution.py:599
  64.4 26.5 %collective-permute-start.5 = (bf16[2048,128]{1,0:T(8,128)(2,1)}, bf16[2048,128]{1,0:T(8,128)(2,1)}, u32[]{:S(2)}, u32[]{:S(2)}) collective-permute-start(bf16[2048,128]{1,0:T(8,128)(2,1)} %get-tuple-element.47.rest_0_), channel_id=1, source_target_pairs={{0,1},{1,2},{2,3},{3,0},{4,5},{5,6},{6,7},{7,4},{8,9},{9,10},{10,1... | collective-permute-start | bytes 1572872 | tf_op jit(solution)/shard_map/ppermute | solution.py:599
  64.4 26.5 %collective-permute-start.6 = (bf16[2048,128]{1,0:T(8,128)(2,1)}, bf16[2048,128]{1,0:T(8,128)(2,1)}, u32[]{:S(2)}, u32[]{:S(2)}) collective-permute-start(bf16[2048,128]{1,0:T(8,128)(2,1)} %get-tuple-element.47.rest_0_), channel_id=1, source_target_pairs={{0,2},{1,3},{2,0},{3,1},{4,6},{5,7},{6,4},{7,5},{8,10},{9,11},{10,... | collective-permute-start | bytes 1572872 | tf_op jit(solution)/shard_map/ppermute | solution.py:599
  70.3 20.6 %copy-start = (bf16[1024,2048]{1,0:T(8,128)(2,1)}, bf16[1024,2048]{1,0:T(8,128)(2,1)S(1)}, u32[]{:S(2)}) copy-start(bf16[1024,2048]{1,0:T(8,128)(2,1)S(1)} %turn.1.xt_ref) | copy-start | bytes 12582916
  95.8 7.5 %copy-start.8 = (bf16[2048,128]{1,0:T(8,128)(2,1)S(1)}, bf16[2048,128]{1,0:T(8,128)(2,1)}, u32[]{:S(2)}) copy-start(bf16[2048,128]{1,0:T(8,128)(2,1)} %get-tuple-element.41.rest_0_) | copy-start | bytes 1572868
  95.8 61.6 %all-to-all-start.4 = ((bf16[32,2,4,32,128]{4,3,2,1,0:T(8,128)(2,1)}), bf16[32,2,4,32,128]{4,3,2,1,0:T(8,128)(2,1)}, u32[]{:S(2)}, u32[]{:S(2)}) async-start(bf16[32,2,4,32,128]{4,3,2,1,0:T(8,128)(2,1)} %weigh.4), calls=%async_computation.4 | async-start | bytes 4194304 | tf_op jit(solution)/shard_map/all_to_all | solution.py:595
  103.3 14.9 %collective-permute-start = (bf16[2048,128]{1,0:T(8,128)(2,1)S(1)}, bf16[2048,128]{1,0:T(8,128)(2,1)S(1)}, u32[]{:S(2)}, u32[]{:S(2)}) collective-permute-start(bf16[2048,128]{1,0:T(8,128)(2,1)S(1)} %copy-done.8), channel_id=1, source_target_pairs={{0,3},{1,0},{2,1},{3,2},{4,7},{5,4},{6,5},{7,6},{8,11},{9,8},{10,9... | collective-permute-start | bytes 1572872 | tf_op jit(solution)/shard_map/ppermute | solution.py:599
  103.7 26.3 %collective-permute-start.1 = (bf16[2048,128]{1,0:T(8,128)(2,1)S(1)}, bf16[2048,128]{1,0:T(8,128)(2,1)S(1)}, u32[]{:S(2)}, u32[]{:S(2)}) collective-permute-start(bf16[2048,128]{1,0:T(8,128)(2,1)S(1)} %copy-done.8), channel_id=1, source_target_pairs={{0,1},{1,2},{2,3},{3,0},{4,5},{5,6},{6,7},{7,4},{8,9},{9,10},{10,1... | collective-permute-start | bytes 1572872 | tf_op jit(solution)/shard_map/ppermute | solution.py:599
  105.4 25.4 %collective-permute-start.2 = (bf16[2048,128]{1,0:T(8,128)(2,1)S(1)}, bf16[2048,128]{1,0:T(8,128)(2,1)}, u32[]{:S(2)}, u32[]{:S(2)}) collective-permute-start(bf16[2048,128]{1,0:T(8,128)(2,1)S(1)} %copy-done.8), channel_id=1, source_target_pairs={{0,2},{1,3},{2,0},{3,1},{4,6},{5,7},{6,4},{7,5},{8,10},{9,11},{10,... | collective-permute-start | bytes 1572872 | tf_op jit(solution)/shard_map/ppermute | solution.py:599
  118.2 11.8 %copy-start.11 = (bf16[2048,128]{1,0:T(8,128)(2,1)}, bf16[2048,128]{1,0:T(8,128)(2,1)S(1)}, u32[]{:S(2)}) copy-start(bf16[2048,128]{1,0:T(8,128)(2,1)S(1)} %collective-permute-done.rest_1_) | copy-start | bytes 1572868
  129.9 0.8 copy-start.13
  130.8 2.2 copy-start.1
  137.8 16.6 %collective-permute-start.3 = (bf16[32,2,32,128]{3,2,1,0:T(8,128)(2,1)}, bf16[32,2,32,128]{3,2,1,0:T(8,128)(2,1)S(1)}, u32[]{:S(2)}, u32[]{:S(2)}) collective-permute-start(bf16[32,2,32,128]{3,2,1,0:T(8,128)(2,1)} %get-tuple-element.43), channel_id=1, source_target_pairs={{0,4},{4,0},{8,12},{12,8},{16,20},{20,16},{24,28},{28,24},{32,36},... | collective-permute-start | bytes 1572872 | tf_op jit(solution)/shard_map/ppermute | solution.py:634
  154.4 0.8 copy-start.7
  157.4 7.6 %copy-start.9 = (bf16[2048,128]{1,0:T(8,128)(2,1)S(1)}, bf16[2048,128]{1,0:T(8,128)(2,1)}, u32[]{:S(2)}) copy-start(bf16[2048,128]{1,0:T(8,128)(2,1)} %get-tuple-element.59.rest_0_) | copy-start | bytes 1572868
  157.4 47.4 %all-to-all-start.3 = ((bf16[32,6,32,128]{3,2,1,0:T(8,128)(2,1)}), bf16[32,6,32,128]{3,2,1,0:T(8,128)(2,1)}, u32[]{:S(2)}, u32[]{:S(2)}) async-start(bf16[32,6,32,128]{3,2,1,0:T(8,128)(2,1)} %join.2), calls=%async_computation.3 | async-start | bytes 3145728 | tf_op jit(solution)/shard_map/all_to_all | solution.py:595
  165.0 14.9 %collective-permute-start.7 = (bf16[2048,128]{1,0:T(8,128)(2,1)S(1)}, bf16[2048,128]{1,0:T(8,128)(2,1)S(1)}, u32[]{:S(2)}, u32[]{:S(2)}) collective-permute-start(bf16[2048,128]{1,0:T(8,128)(2,1)S(1)} %copy-done.9), channel_id=1, source_target_pairs={{0,3},{1,0},{2,1},{3,2},{4,7},{5,4},{6,5},{7,6},{8,11},{9,8},{10,9... | collective-permute-start | bytes 1572872 | tf_op jit(solution)/shard_map/ppermute | solution.py:599
  165.7 26.2 %collective-permute-start.8 = (bf16[2048,128]{1,0:T(8,128)(2,1)S(1)}, bf16[2048,128]{1,0:T(8,128)(2,1)S(1)}, u32[]{:S(2)}, u32[]{:S(2)}) collective-permute-start(bf16[2048,128]{1,0:T(8,128)(2,1)S(1)} %copy-done.9), channel_id=1, source_target_pairs={{0,1},{1,2},{2,3},{3,0},{4,5},{5,6},{6,7},{7,4},{8,9},{9,10},{10,1... | collective-permute-start | bytes 1572872 | tf_op jit(solution)/shard_map/ppermute | solution.py:599
  167.1 25.6 %collective-permute-start.9 = (bf16[2048,128]{1,0:T(8,128)(2,1)S(1)}, bf16[2048,128]{1,0:T(8,128)(2,1)}, u32[]{:S(2)}, u32[]{:S(2)}) collective-permute-start(bf16[2048,128]{1,0:T(8,128)(2,1)S(1)} %copy-done.9), channel_id=1, source_target_pairs={{0,2},{1,3},{2,0},{3,1},{4,6},{5,7},{6,4},{7,5},{8,10},{9,11},{10,... | collective-permute-start | bytes 1572872 | tf_op jit(solution)/shard_map/ppermute | solution.py:599
  179.9 12.1 %copy-start.10 = (bf16[2048,128]{1,0:T(8,128)(2,1)}, bf16[2048,128]{1,0:T(8,128)(2,1)S(1)}, u32[]{:S(2)}) copy-start(bf16[2048,128]{1,0:T(8,128)(2,1)S(1)} %collective-permute-done.7.rest_1_) | copy-start | bytes 1572868
  191.9 0.8 copy-start.12
  192.7 2.2 copy-start.2
  199.8 2.1 collective-permute-start.10
  201.9 0.8 copy-start.6
  204.8 20.5 %all-to-all-start.5 = ((bf16[32,2,32,128]{3,2,1,0:T(8,128)(2,1)}), bf16[32,2,32,128]{3,2,1,0:T(8,128)(2,1)S(1)}, u32[]{:S(2)}, u32[]{:S(2)}) async-start(bf16[32,2,32,128]{3,2,1,0:T(8,128)(2,1)} %join.3), calls=%async_computation.5 | async-start | bytes 1048576 | tf_op jit(solution)/shard_map/all_to_all | solution.py:595
  225.3 0.8 copy-start.3

commit v5 on v4

--- a/solution.py
+++ b/solution.py
@@ -113,30 +113,66 @@
         out_ref[:, cut] = x_ref[cut, :].T
 
 
-def weight_kernel(me_ref, xt_ref, *rest, shards, steps, halves):
-    span = xt_ref.shape[0] // steps
-    xt = xt_ref[pl.ds(pl.multiple_of(pl.program_id(0) * span, span), span), :]
-    core = me_ref[0] % 2
-    shape = (span // KEY_BLOCK, KEY_BLOCK, HEAD_DIM)
-    sums = []
-    for at in range(0, shards, 2):
-        g = jnp.concatenate([rest[at][...], rest[at + 1][...]], axis=1)
-        got = jnp.dot(xt, g, preferred_element_type=jnp.float32).astype(jnp.bfloat16)
-        sums += [got[:, :HEAD_DIM].reshape(shape), got[:, HEAD_DIM:].reshape(shape)]
-    if halves:
-        keep_ref, give_ref = rest[-2:]
-        for p in range(2):
-            keep_ref[:, p] = jnp.where(core == 0, sums[p], sums[2 + p])
-            give_ref[:, p] = jnp.where(core == 0, sums[2 + p], sums[p])
-    else:
-        for p in range(shards):
-            rest[-1][:, p] = sums[p]
-
-
-def join_kernel(keep_ref, got_ref, *rest):
-    out_ref = rest[-1]
-    both = keep_ref[...].astype(jnp.float32) + got_ref[...].astype(jnp.float32)
-    out_ref[...] = both.astype(jnp.bfloat16)
+def weight_kernel(me_ref, xt_ref, *rest, extra, slot, halves):
+    shards = rest[:4]
+    outs = rest[4 + extra : -4]
+    g_s, o_s, in_sem, out_sem = rest[-4:]
+    copies = []
+    for n, shard in enumerate(shards):
+        lanes = pl.ds((n % 2) * HEAD_DIM, HEAD_DIM)
+        copy = pltpu.make_async_copy(shard, g_s.at[n // 2, :, lanes], in_sem.at[n])
+        copy.start()
+        copies.append(copy)
+    rows = xt_ref.shape[0]
+    shape = (WEIGH_ROWS // KEY_BLOCK, KEY_BLOCK, HEAD_DIM)
+    ends = []
+    for pair in range(2):
+        copies[2 * pair].wait()
+        copies[2 * pair + 1].wait()
+        g = g_s[pair]
+
+        def some(b, carry, pair=pair, g=g):
+            first = pl.multiple_of(b * WEIGH_ROWS, WEIGH_ROWS)
+            xt = xt_ref[pl.ds(first, WEIGH_ROWS), :]
+            got = jnp.dot(xt, g, preferred_element_type=jnp.float32).astype(jnp.bfloat16)
+            owners = pl.ds(b * shape[0], shape[0])
+            o_s[pair, owners, 0] = got[:, :HEAD_DIM].reshape(shape)
+            o_s[pair, owners, 1] = got[:, HEAD_DIM:].reshape(shape)
+            return carry
+
+        lax.fori_loop(0, rows // WEIGH_ROWS, some, 0)
+        if halves:
+            core = me_ref[0] % 2
+            for out, mine in ((outs[0], core == pair), (outs[1], core != pair)):
+                copy = pltpu.make_async_copy(o_s.at[pair], out, out_sem.at[pair])
+                pl.when(mine)(copy.start)
+                ends.append((copy, mine))
+        else:
+            target = outs[0].at[:, slot, pl.ds(2 * pair, 2)]
+            copy = pltpu.make_async_copy(o_s.at[pair], target, out_sem.at[pair])
+            copy.start()
+            ends.append((copy, None))
+    for copy, mine in ends:
+        if mine is None:
+            copy.wait()
+        else:
+            pl.when(mine)(copy.wait)
+
+
+def join_kernel(keep_ref, got_ref, *rest, at):
+    out_ref, keep_s, got_s, sem = rest[-4:]
+    one = pltpu.make_async_copy(keep_ref, keep_s, sem.at[0])
+    two = pltpu.make_async_copy(got_ref, got_s, sem.at[1])
+    one.start()
+    two.start()
+    one.wait()
+    two.wait()
+    both = keep_s[...].astype(jnp.float32) + got_s[...].astype(jnp.float32)
+    got_s[...] = both.astype(jnp.bfloat16)
+    count = keep_ref.shape[1]
+    back = pltpu.make_async_copy(got_s, out_ref.at[:, pl.ds(at * count, count)], sem.at[2])
+    back.start()
+    back.wait()
 
 
 def put_sum(out_ref, got_ref, sources, column, first):
@@ -155,13 +191,27 @@
         put_sum(out_ref, got_ref, sources, p, (place * heads + head) * HEAD_DIM)
 
 
-def pair_total_kernel(at_ref, got_ref, before_ref, out_ref, *, head, heads, order):
+def pair_total_kernel(at_ref, got_ref, before_ref, out_ref, got_s, sum_s, got_sem, sem,
+                      *, at, head, heads, order):
     tp = len(order)
-    out_ref[...] = before_ref[...]
+    got = pltpu.make_async_copy(got_ref.at[:, pl.ds(at * tp // 2, tp // 2)], got_s, got_sem)
+    got.start()
+    got.wait()
+    copies = []
     for p in range(tp):
         place = (at_ref[0] + order[p]) % tp
-        sources = range(p // 2, got_ref.shape[0], 2)
-        put_sum(out_ref, got_ref, sources, p % 2, (place * heads + head) * HEAD_DIM)
+        acc = got_s[p // 2, p % 2].astype(jnp.float32)
+        for i in range(p // 2 + 2, got_s.shape[0], 2):
+            acc = acc + got_s[i, p % 2].astype(jnp.float32)
+        sum_s[p] = acc
+        first = pl.multiple_of((place * heads + head) * HEAD_DIM, HEAD_DIM)
+        copy = pltpu.make_async_copy(
+            sum_s.at[p], out_ref.at[:, pl.ds(first, HEAD_DIM)], sem.at[p]
+        )
+        copy.start()
+        copies.append(copy)
+    for copy in copies:
+        copy.wait()
 
 
 def attend_kernel(me_ref, *refs, head, extra, merge, tiles, far):
@@ -302,13 +352,11 @@
         at = head * half + n // 2
         odd = n % 2
         for c in range(CAP):
-
-            @pl.when(tab_ref[4 + 2 * c + odd, at] > 0)
-            def _(c=c):
-                first = tab_ref[2 * c + odd, at] * KEY_BLOCK
-                rows = pl.ds(pl.multiple_of(first, KEY_BLOCK), KEY_BLOCK)
-                gk_ref[rows, :] += back_ref[n, c].astype(jnp.float32)
-                gv_ref[rows, :] += back_ref[n, CAP + c].astype(jnp.float32)
+            named = tab_ref[4 + 2 * c + odd, at] > 0
+            first = tab_ref[2 * c + odd, at] * KEY_BLOCK
+            rows = pl.ds(pl.multiple_of(first, KEY_BLOCK), KEY_BLOCK)
+            gk_ref[rows, :] += jnp.where(named, back_ref[n, c].astype(jnp.float32), 0.0)
+            gv_ref[rows, :] += jnp.where(named, back_ref[n, CAP + c].astype(jnp.float32), 0.0)
 
         return carry
 
@@ -478,34 +526,31 @@
 
 def weigh(me, xt, shards, buffer, spans, slot, slots, halves=False):
     cols, rows = xt.shape
-    tall = pl.BlockSpec((rows, HEAD_DIM), lambda i: (0, 0))
-    in_specs = [SMEM, VMEM] + [tall] * len(shards)
+    in_specs = [SMEM, VMEM] + [ANY] * len(shards)
     args = [me, pltpu.with_memory_space_constraint(xt, pltpu.VMEM), *shards]
     aliases = {}
     if buffer is not None:
         aliases[len(args)] = 0
         in_specs.append(ANY)
         args.append(buffer)
-    owned = cols // spans
-    per = WEIGH_ROWS // owned
+    half = (spans, len(shards) // 2, cols // spans, HEAD_DIM)
     if halves:
-        shape = (spans, len(shards) // 2, owned, HEAD_DIM)
-        out_spec = pl.BlockSpec((per,) + shape[1:], lambda i: (i, 0, 0, 0))
-        out_specs = [out_spec] * 2
-        out_shape = [jax.ShapeDtypeStruct(shape, jnp.bfloat16)] * 2
+        out_specs = [ANY, ANY]
+        out_shape = [jax.ShapeDtypeStruct(half, jnp.bfloat16)] * 2
     else:
-        out_specs = pl.BlockSpec(
-            (per, None, len(shards), owned, HEAD_DIM), lambda i: (i, slot, 0, 0, 0)
-        )
+        out_specs = ANY
         out_shape = jax.ShapeDtypeStruct(five(spans, slots), jnp.bfloat16)
     return pl.pallas_call(
-        functools.partial(
-            weight_kernel, shards=len(shards), steps=cols // WEIGH_ROWS, halves=halves
-        ),
-        grid=(cols // WEIGH_ROWS,),
+        functools.partial(weight_kernel, extra=len(aliases), slot=slot, halves=halves),
         in_specs=in_specs,
         out_specs=out_specs,
         out_shape=out_shape,
+        scratch_shapes=[
+            pltpu.VMEM((2, rows, 2 * HEAD_DIM), jnp.bfloat16),
+            pltpu.VMEM((2,) + half, jnp.bfloat16),
+            pltpu.SemaphoreType.DMA((4,)),
+            pltpu.SemaphoreType.DMA((2,)),
+        ],
         input_output_aliases=aliases,
         compiler_params=params(),
         cost_estimate=cost(2 * cols * rows * len(shards) * HEAD_DIM, 8 << 20),
@@ -518,20 +563,22 @@
 
 
 def join(keep, got, buffer, at):
-    spans, count = keep.shape[:2]
-    args, in_specs, aliases = [keep, got], [tiles_of(spans, count, 0)] * 2, {}
+    args, aliases = [keep, got], {}
     out_shape = jax.ShapeDtypeStruct(keep.shape, keep.dtype)
     if buffer is not None:
         aliases = {2: 0}
         args.append(buffer)
-        in_specs.append(ANY)
         out_shape = jax.ShapeDtypeStruct(buffer.shape, buffer.dtype)
     return pl.pallas_call(
-        join_kernel,
-        grid=(1,),
-        in_specs=in_specs,
-        out_specs=tiles_of(spans, count, at),
+        functools.partial(join_kernel, at=at),
+        in_specs=[ANY] * len(args),
+        out_specs=ANY,
         out_shape=out_shape,
+        scratch_shapes=[
+            pltpu.VMEM(keep.shape, keep.dtype),
+            pltpu.VMEM(keep.shape, keep.dtype),
+            pltpu.SemaphoreType.DMA((3,)),
+        ],
         input_output_aliases=aliases,
         compiler_params=params(),
         cost_estimate=cost(1 << 24),
@@ -555,12 +602,18 @@
 
 
 def pair_total(place, got, at, buffer, head, heads, order):
-    return pl.pallas_call(
-        functools.partial(pair_total_kernel, head=head, heads=heads, order=order),
-        grid=(1,),
-        in_specs=[SMEM, tiles_of(got.shape[0], len(order) // 2, at), VMEM],
-        out_specs=VMEM,
+    half = (got.shape[0], len(order) // 2, KEY_BLOCK, HEAD_DIM)
+    return pl.pallas_call(
+        functools.partial(pair_total_kernel, at=at, head=head, heads=heads, order=order),
+        in_specs=[SMEM, ANY, ANY],
+        out_specs=ANY,
         out_shape=jax.ShapeDtypeStruct(buffer.shape, buffer.dtype),
+        scratch_shapes=[
+            pltpu.VMEM(half, got.dtype),
+            pltpu.VMEM((len(order), KEY_BLOCK, HEAD_DIM), jnp.float32),
+            pltpu.SemaphoreType.DMA,
+            pltpu.SemaphoreType.DMA((len(order),)),
+        ],
         input_output_aliases={2: 0},
         compiler_params=params(),
         cost_estimate=cost(1 << 24),
@@ -586,7 +639,7 @@
         out_specs=[column, column],
         out_shape=[jax.ShapeDtypeStruct((rows, width), jnp.float32)] * 2,
         input_output_aliases=aliases,
-        compiler_params=params(),
+        compiler_params=pltpu.CompilerParams(vmem_limit_bytes=32 * 1024 * 1024),
         cost_estimate=cost(1 << 24),
     )(*args)
 

time: 235 us -> 232 us (0.987)
  Pallas kernels: 104 us -> 101 us
    pallas_call x3, Pallas kernels: 14 us -> 10.3 us  [land(): pl.pallas_call(functools.partial(land_kernel, head=head, spans=spans), gr...]
    unnamed x28 -> x40, local copies, waits for them, and re-layouts: 8.41 us -> 7.63 us
  transfers between devices with their start and end apart: 17 -> 17, of which waited for: 7 -> 8; matrix products, arithmetic and copies ran while one was open for 0% -> 0% of each run, Pallas kernels for 41% -> 40%
where the time goes in v5:
time: 232 us; the launch traced here: 230 us
  Pallas kernels  101 us (44%)
  waiting for transfers between devices  66.2 us (29%)
  starting transfers between devices  53.9 us (23%)
  local copies, waits for them, and re-layouts  7.63 us (3%)
    pallas_call x3, Pallas kernels, attend(): pl.pallas_call(functools.partial(attend_kernel, head=head, extra=len(alia...  51.6 us
    ppermute x9, waiting for transfers between devices, shift(): return lax.ppermute(x, 'tp', [(i, (i + by) % tp) for i in range(tp)])  50.1 us
    all_to_all x6, starting transfers between devices, exchange(): return lax.all_to_all(x, 'kv', split_axis=0, concat_axis=0, tiled=True)  42.4 us
    pallas_call x3, Pallas kernels, weigh(): pl.pallas_call(functools.partial(weight_kernel, extra=len(aliases), slot=...  14.8 us
    all_to_all x6, waiting for transfers between devices, exchange(): return lax.all_to_all(x, 'kv', split_axis=0, concat_axis=0, tiled=True)  14 us
    ppermute x9, starting transfers between devices, shift(): return lax.ppermute(x, 'tp', [(i, (i + by) % tp) for i in range(tp)])  11.2 us
    pallas_call x3, Pallas kernels, land(): pl.pallas_call(functools.partial(land_kernel, head=head, spans=spans), gr...  10.3 us
    unnamed x40, local copies, waits for them, and re-layouts  7.63 us
  transfers between devices with their start and end apart: 17, of which 8 were waited for; matrix products, arithmetic and copies ran while one was open for 0% of the time, Pallas kernels for 40%

profile of v5, /device:TPU:0, one launch (start us, length us, event | category | flops | bytes accessed | tf_op | source)
XLA Modules:
  0.0 229.6 jit_solution(17513162687349860580)
XLA Ops:
  0.6 3.6 %first.1 = (bf16[32,1,4,32,128]{4,3,2,1,0:T(8,128)(2,1)}, s32[8,128]{1,0:T(8,128)}) custom-call(s32[1]{0:T(128)} %bitcast.me_ref, s32[3,12,2048]{2,1,0:T(8,128)} %bitcast.9, bf16[64,32,384]{2,1,0:T(8,128)(2,1)} %bitcast.5, bf16[64,32,384]{2,1,0:T(8,128)(2,1)} %bitcast.7), custom_call_target="tpu_custom_call" | custom-call | flops 67108864 | bytes 1048576 | tf_op jit(solution)/shard_map/first/pallas_call | solution.py:396
  4.2 8.5 %all-to-all-start = ((bf16[32,1,4,32,128]{4,3,2,1,0:T(8,128)(2,1)}), bf16[32,1,4,32,128]{4,3,2,1,0:T(8,128)(2,1)S(1)}, u32[]{:S(2)}, u32[]{:S(2)}) async-start(bf16[32,1,4,32,128]{4,3,2,1,0:T(8,128)(2,1)} %get-tuple-element.33), calls=%async_computation | async-start | bytes 2097152 | tf_op jit(solution)/shard_map/all_to_all | solution.py:648
  12.7 3.9 %pack.1 = (bf16[32,1,4,32,128]{4,3,2,1,0:T(8,128)(2,1)}, bf16[32,1,4,32,128]{4,3,2,1,0:T(8,128)(2,1)}) custom-call(s32[8,128]{1,0:T(8,128)} %get-tuple-element.34.tab_ref, bf16[64,32,384]{2,1,0:T(8,128)(2,1)} %bitcast.6, bf16[64,32,384]{2,1,0:T(8,128)(2,1)} %bitcast.8), custom_call_target="tpu_custom_call" | custom-call | flops 67108864 | bytes 1048576 | tf_op jit(solution)/shard_map/pack/pallas_call | solution.py:419
  16.6 13.3 %all-to-all-done.refs_6_ = bf16[32,1,4,32,128]{4,3,2,1,0:T(8,128)(2,1)S(1)} async-done(((bf16[32,1,4,32,128]{4,3,2,1,0:T(8,128)(2,1)}), bf16[32,1,4,32,128]{4,3,2,1,0:T(8,128)(2,1)S(1)}, u32[]{:S(2)}, u32[]{:S(2)}) %all-to-all-start) | async-done | bytes 1048608 | tf_op jit(solution)/shard_map/all_to_all | solution.py:648
  29.9 3.9 %all-to-all-start.2 = ((bf16[32,1,4,32,128]{4,3,2,1,0:T(8,128)(2,1)}), bf16[32,1,4,32,128]{4,3,2,1,0:T(8,128)(2,1)S(1)}, u32[]{:S(2)}, u32[]{:S(2)}) async-start(bf16[32,1,4,32,128]{4,3,2,1,0:T(8,128)(2,1)} %get-tuple-element.37), calls=%async_computation.2 | async-start | bytes 2097152 | tf_op jit(solution)/shard_map/all_to_all | solution.py:648
  33.8 3.1 %mask.1.refs_5_ = f32[3,64,2048]{2,1,0:T(8,128)} custom-call(s32[1]{0:T(128)} %bitcast.me_ref, s32[3,12,2048]{2,1,0:T(8,128)} %bitcast.10), custom_call_target="tpu_custom_call" | custom-call | flops 67108864 | bytes 1048576 | tf_op jit(solution)/shard_map/mask/pallas_call | solution.py:433
  36.9 17.1 %shard_map.102 = (bf16[2048,384]{1,0:T(8,128)(2,1)}, bf16[2048,128]{1,0:T(8,128)(2,1)}, f32[2048,128]{1,0:T(8,128)}, f32[2048,128]{1,0:T(8,128)}, bf16[32,1,4,32,128]{4,3,2,1,0:T(8,128)(2,1)}) custom-call(s32[1]{0:T(128)} %bitcast.me_ref, bf16[2048,384]{1,0:T(8,128)(2,1)} %refs_0_.5, bf16[2048,384]{1,0:T(8,128)(2,1)} %refs_1_.5, bf16[2048,384]{1,0:T(8,128)(2,1)} %refs_2_.5, ...), custom_call_target="tpu_custom_call" | custom-call | flops 5368709120 | bytes 8388608 | tf_op jit(solution)/shard_map/pallas_call | solution.py:495
  54.0 7.6 %all-to-all-start.1 = ((bf16[32,1,4,32,128]{4,3,2,1,0:T(8,128)(2,1)}), bf16[32,1,4,32,128]{4,3,2,1,0:T(8,128)(2,1)}, u32[]{:S(2)}, u32[]{:S(2)}) async-start(bf16[32,1,4,32,128]{4,3,2,1,0:T(8,128)(2,1)} %get-tuple-element.36), calls=%async_computation.1 | async-start | bytes 2097152 | tf_op jit(solution)/shard_map/all_to_all | solution.py:648
  61.6 2.8 %collective-permute-start.4 = (bf16[2048,128]{1,0:T(8,128)(2,1)}, bf16[2048,128]{1,0:T(8,128)(2,1)}, u32[]{:S(2)}, u32[]{:S(2)}) collective-permute-start(bf16[2048,128]{1,0:T(8,128)(2,1)} %get-tuple-element.47.rest_0_), channel_id=1, source_target_pairs={{0,3},{1,0},{2,1},{3,2},{4,7},{5,4},{6,5},{7,6},{8,11},{9,8},{10,9... | collective-permute-start | bytes 1572872 | tf_op jit(solution)/shard_map/ppermute | solution.py:652
  64.4 2.3 %collective-permute-start.6 = (bf16[2048,128]{1,0:T(8,128)(2,1)}, bf16[2048,128]{1,0:T(8,128)(2,1)}, u32[]{:S(2)}, u32[]{:S(2)}) collective-permute-start(bf16[2048,128]{1,0:T(8,128)(2,1)} %get-tuple-element.47.rest_0_), channel_id=1, source_target_pairs={{0,2},{1,3},{2,0},{3,1},{4,6},{5,7},{6,4},{7,5},{8,10},{9,11},{10,... | collective-permute-start | bytes 1572872 | tf_op jit(solution)/shard_map/ppermute | solution.py:652
  66.7 3.6 %turn.1.xt_ref = bf16[1024,2048]{1,0:T(8,128)(2,1)S(1)} custom-call(bf16[2048,1024]{1,0:T(8,128)(2,1)} %x_ref.1), custom_call_target="tpu_custom_call" | custom-call | flops 67108864 | bytes 1048576 | tf_op jit(solution)/shard_map/turn/pallas_call | solution.py:446
  70.3 18.0 %shard_map.103 = (bf16[2048,384]{1,0:T(8,128)(2,1)}, bf16[2048,128]{1,0:T(8,128)(2,1)}, f32[2048,128]{1,0:T(8,128)}, f32[2048,128]{1,0:T(8,128)}, bf16[32,2,4,32,128]{4,3,2,1,0:T(8,128)(2,1)}) custom-call(s32[1]{0:T(128)} %bitcast.me_ref, bf16[2048,384]{1,0:T(8,128)(2,1)} %refs_0_.5, bf16[2048,384]{1,0:T(8,128)(2,1)} %refs_1_.5, ...), custom_call_target="tpu_custom_call", output_to_operand_aliasing={{0}: (8, {})} | custom-call | flops 5368709120 | bytes 8388608 | tf_op jit(solution)/shard_map/pallas_call | solution.py:495
  88.3 2.6 %collective-permute-done.5.rest_2_ = bf16[2048,128]{1,0:T(8,128)(2,1)} collective-permute-done((bf16[2048,128]{1,0:T(8,128)(2,1)}, bf16[2048,128]{1,0:T(8,128)(2,1)}, u32[]{:S(2)}, u32[]{:S(2)}) %collective-permute-start.5) | collective-permute-done | bytes 524320 | tf_op jit(solution)/shard_map/ppermute | solution.py:652
  90.9 4.9 %weigh.4 = bf16[32,2,4,32,128]{4,3,2,1,0:T(8,128)(2,1)} custom-call(s32[1]{0:T(128)} %bitcast.me_ref, bf16[1024,2048]{1,0:T(8,128)(2,1)S(1)} %turn.1.xt_ref, bf16[2048,128]{1,0:T(8,128)(2,1)} %get-tuple-element.47.rest_0_, bf16[2048,128]{1,0:T(8,128)(2,1)} %collective-permute-done.4.rest_1_, ...), custom_call_target="tpu_custom_call", output_to_operand_aliasing={{}: (6, {})} | custom-call | flops 2147483648 | bytes 8388608 | tf_op jit(solution)/shard_map/weigh/pallas_call | solution.py:543
  95.8 7.5 %all-to-all-start.4 = ((bf16[32,2,4,32,128]{4,3,2,1,0:T(8,128)(2,1)}), bf16[32,2,4,32,128]{4,3,2,1,0:T(8,128)(2,1)}, u32[]{:S(2)}, u32[]{:S(2)}) async-start(bf16[32,2,4,32,128]{4,3,2,1,0:T(8,128)(2,1)} %weigh.4), calls=%async_computation.4 | async-start | bytes 4194304 | tf_op jit(solution)/shard_map/all_to_all | solution.py:648
  103.4 0.4 collective-permute-start
  103.7 1.7 collective-permute-start.1
  105.5 0.6 collective-permute-start.2
  106.1 12.2 %collective-permute-done.rest_1_ = bf16[2048,128]{1,0:T(8,128)(2,1)S(1)} collective-permute-done((bf16[2048,128]{1,0:T(8,128)(2,1)S(1)}, bf16[2048,128]{1,0:T(8,128)(2,1)S(1)}, u32[]{:S(2)}, u32[]{:S(2)}) %collective-permute-start) | collective-permute-done | bytes 524320 | tf_op jit(solution)/shard_map/ppermute | solution.py:652
  118.2 11.8 %collective-permute-done.1.rest_2_ = bf16[2048,128]{1,0:T(8,128)(2,1)S(1)} collective-permute-done((bf16[2048,128]{1,0:T(8,128)(2,1)S(1)}, bf16[2048,128]{1,0:T(8,128)(2,1)S(1)}, u32[]{:S(2)}, u32[]{:S(2)}) %collective-permute-start.1) | collective-permute-done | bytes 524320 | tf_op jit(solution)/shard_map/ppermute | solution.py:652
  130.0 0.8 copy-done.19
  130.8 2.2 copy-done.1
  133.0 4.9 %weigh.3 = (bf16[32,2,32,128]{3,2,1,0:T(8,128)(2,1)}, bf16[32,2,32,128]{3,2,1,0:T(8,128)(2,1)}) custom-call(s32[1]{0:T(128)} %bitcast.me_ref, bf16[1024,2048]{1,0:T(8,128)(2,1)S(1)} %copy-done.1, bf16[2048,128]{1,0:T(8,128)(2,1)} %get-tuple-element.41.rest_0_, bf16[2048,128]{1,0:T(8,128)(2,1)} %copy-done.17, bf16[2048,128]{1,0:T(8,128)(2,1)} %copy-done.19, ...), custom_call_target="tpu_custom_call" | custom-call | flops 2147483648 | bytes 8388608 | tf_op jit(solution)/shard_map/weigh/pallas_call | solution.py:543
  138.0 0.3 collective-permute-start.3
  138.3 16.6 %shard_map.104 = (bf16[2048,384]{1,0:T(8,128)(2,1)}, bf16[2048,128]{1,0:T(8,128)(2,1)}, f32[2048,128]{1,0:T(8,128)}, f32[2048,128]{1,0:T(8,128)}, bf16[32,6,32,128]{3,2,1,0:T(8,128)(2,1)}) custom-call(s32[1]{0:T(128)} %bitcast.me_ref, bf16[2048,384]{1,0:T(8,128)(2,1)} %refs_0_.5, bf16[2048,384]{1,0:T(8,128)(2,1)} %refs_1_.5, ...), custom_call_target="tpu_custom_call", output_to_operand_aliasing={{0}: (8, {})} | custom-call | flops 5368709120 | bytes 8388608 | tf_op jit(solution)/shard_map/pallas_call | solution.py:495
  154.9 0.8 copy-done.13
  155.6 2.2 join.2
  157.9 7.6 %all-to-all-start.3 = ((bf16[32,6,32,128]{3,2,1,0:T(8,128)(2,1)}), bf16[32,6,32,128]{3,2,1,0:T(8,128)(2,1)}, u32[]{:S(2)}, u32[]{:S(2)}) async-start(bf16[32,6,32,128]{3,2,1,0:T(8,128)(2,1)} %join.2), calls=%async_computation.3 | async-start | bytes 3145728 | tf_op jit(solution)/shard_map/all_to_all | solution.py:648
  165.5 0.7 collective-permute-start.7
  166.2 1.4 collective-permute-start.8
  167.6 1.2 collective-permute-start.9
  168.8 11.5 %collective-permute-done.7.rest_1_ = bf16[2048,128]{1,0:T(8,128)(2,1)S(1)} collective-permute-done((bf16[2048,128]{1,0:T(8,128)(2,1)S(1)}, bf16[2048,128]{1,0:T(8,128)(2,1)S(1)}, u32[]{:S(2)}, u32[]{:S(2)}) %collective-permute-start.7) | collective-permute-done | bytes 524320 | tf_op jit(solution)/shard_map/ppermute | solution.py:652
  180.4 12.1 %collective-permute-done.8.rest_2_ = bf16[2048,128]{1,0:T(8,128)(2,1)S(1)} collective-permute-done((bf16[2048,128]{1,0:T(8,128)(2,1)S(1)}, bf16[2048,128]{1,0:T(8,128)(2,1)S(1)}, u32[]{:S(2)}, u32[]{:S(2)}) %collective-permute-start.8) | collective-permute-done | bytes 524320 | tf_op jit(solution)/shard_map/ppermute | solution.py:652
  192.4 0.8 copy-done.18
  193.2 2.2 copy-done.2
  195.4 4.9 %weigh.5 = (bf16[32,2,32,128]{3,2,1,0:T(8,128)(2,1)}, bf16[32,2,32,128]{3,2,1,0:T(8,128)(2,1)}) custom-call(s32[1]{0:T(128)} %bitcast.me_ref, bf16[1024,2048]{1,0:T(8,128)(2,1)S(1)} %copy-done.2, bf16[2048,128]{1,0:T(8,128)(2,1)} %get-tuple-element.59.rest_0_, bf16[2048,128]{1,0:T(8,128)(2,1)} %copy-done.16, bf16[2048,128]{1,0:T(8,128)(2,1)} %copy-done.18, ...), custom_call_target="tpu_custom_call" | custom-call | flops 2147483648 | bytes 8388608 | tf_op jit(solution)/shard_map/weigh/pallas_call | solution.py:543
  200.4 0.1 collective-permute-start.10
  200.5 2.1 collective-permute-done.10.got_ref
  202.6 0.8 copy-done.12
  203.4 2.1 join.3
  205.5 7.4 %all-to-all-start.5 = ((bf16[32,2,32,128]{3,2,1,0:T(8,128)(2,1)}), bf16[32,2,32,128]{3,2,1,0:T(8,128)(2,1)}, u32[]{:S(2)}, u32[]{:S(2)}) async-start(bf16[32,2,32,128]{3,2,1,0:T(8,128)(2,1)} %join.3), calls=%async_computation.5 | async-start | bytes 1048576 | tf_op jit(solution)/shard_map/all_to_all | solution.py:648
  212.9 3.5 %shard_map.105 = (f32[2048,384]{1,0:T(8,128)}, f32[2048,384]{1,0:T(8,128)}) custom-call(s32[1]{0:T(128)} %bitcast.me_ref, s32[8,128]{1,0:T(8,128)S(1)} %copy-done.9, bf16[32,1,4,32,128]{4,3,2,1,0:T(8,128)(2,1)} %all-to-all-done.1.refs_6_.back_ref, f32[2048,128]{1,0:T(8,128)S(1)} %copy-done.7, f32[2048,128]{1,0:T(8,128)S(1)} %copy-done.8), custom_call_target="tpu_custom_call" | custom-call | flops 16777216 | bytes 1048576 | tf_op jit(solution)/shard_map/pallas_call | solution.py:635
  216.5 2.1 total.1.before_ref
  218.5 3.4 %shard_map.106 = (f32[2048,384]{1,0:T(8,128)}, f32[2048,384]{1,0:T(8,128)}) custom-call(s32[1]{0:T(128)} %bitcast.me_ref, s32[8,128]{1,0:T(8,128)S(1)} %copy-done.9, bf16[32,2,4,32,128]{4,3,2,1,0:T(8,128)(2,1)} %all-to-all-done.4.back_ref.got_ref, f32[2048,128]{1,0:T(8,128)S(1)} %copy-done.3, ...), custom_call_target="tpu_custom_call", output_to_operand_aliasing={{0}: (5, {}), {1}: (6, {})} | custom-call | flops 16777216 | bytes 1048576 | tf_op jit(solution)/shard_map/pallas_call | solution.py:635
  221.9 1.9 pairtotal.2.before_ref
  223.8 0.6 all-to-all-done.5.got_ref
  224.5 1.8 pairtotal.3
  226.2 3.4 %shard_map.107 = (f32[2048,384]{1,0:T(8,128)}, f32[2048,384]{1,0:T(8,128)}) custom-call(s32[1]{0:T(128)} %bitcast.me_ref, s32[8,128]{1,0:T(8,128)S(1)} %copy-done.9, bf16[32,6,32,128]{3,2,1,0:T(8,128)(2,1)} %all-to-all-done.3.back_ref.got_ref, f32[2048,128]{1,0:T(8,128)S(1)} %copy-done.5, ...), custom_call_target="tpu_custom_call", output_to_operand_aliasing={{0}: (5, {}), {1}: (6, {})} | custom-call | flops 16777216 | bytes 1048576 | tf_op jit(solution)/shard_map/pallas_call | solution.py:635
  (44 shorter events, 0.1 us)
Async XLA Ops:
  4.2 25.7 %all-to-all-start = ((bf16[32,1,4,32,128]{4,3,2,1,0:T(8,128)(2,1)}), bf16[32,1,4,32,128]{4,3,2,1,0:T(8,128)(2,1)S(1)}, u32[]{:S(2)}, u32[]{:S(2)}) async-start(bf16[32,1,4,32,128]{4,3,2,1,0:T(8,128)(2,1)} %get-tuple-element.33), calls=%async_computation | async-start | bytes 2097152 | tf_op jit(solution)/shard_map/all_to_all | solution.py:648
  29.9 7.0 %copy-start.11 = (bf16[32,1,4,32,128]{4,3,2,1,0:T(8,128)(2,1)}, bf16[32,1,4,32,128]{4,3,2,1,0:T(8,128)(2,1)S(1)}, u32[]{:S(2)}) copy-start(bf16[32,1,4,32,128]{4,3,2,1,0:T(8,128)(2,1)S(1)} %all-to-all-done.refs_6_) | copy-start | bytes 3145732
  29.9 24.1 %all-to-all-start.2 = ((bf16[32,1,4,32,128]{4,3,2,1,0:T(8,128)(2,1)}), bf16[32,1,4,32,128]{4,3,2,1,0:T(8,128)(2,1)S(1)}, u32[]{:S(2)}, u32[]{:S(2)}) async-start(bf16[32,1,4,32,128]{4,3,2,1,0:T(8,128)(2,1)} %get-tuple-element.37), calls=%async_computation.2 | async-start | bytes 2097152 | tf_op jit(solution)/shard_map/all_to_all | solution.py:648
  54.0 10.4 %copy-start.10 = (bf16[32,1,4,32,128]{4,3,2,1,0:T(8,128)(2,1)}, bf16[32,1,4,32,128]{4,3,2,1,0:T(8,128)(2,1)S(1)}, u32[]{:S(2)}) copy-start(bf16[32,1,4,32,128]{4,3,2,1,0:T(8,128)(2,1)S(1)} %all-to-all-done.2.refs_6_) | copy-start | bytes 3145732
  54.0 41.8 %all-to-all-start.1 = ((bf16[32,1,4,32,128]{4,3,2,1,0:T(8,128)(2,1)}), bf16[32,1,4,32,128]{4,3,2,1,0:T(8,128)(2,1)}, u32[]{:S(2)}, u32[]{:S(2)}) async-start(bf16[32,1,4,32,128]{4,3,2,1,0:T(8,128)(2,1)} %get-tuple-element.36), calls=%async_computation.1 | async-start | bytes 2097152 | tf_op jit(solution)/shard_map/all_to_all | solution.py:648
  61.6 26.7 %collective-permute-start.4 = (bf16[2048,128]{1,0:T(8,128)(2,1)}, bf16[2048,128]{1,0:T(8,128)(2,1)}, u32[]{:S(2)}, u32[]{:S(2)}) collective-permute-start(bf16[2048,128]{1,0:T(8,128)(2,1)} %get-tuple-element.47.rest_0_), channel_id=1, source_target_pairs={{0,3},{1,0},{2,1},{3,2},{4,7},{5,4},{6,5},{7,6},{8,11},{9,8},{10,9... | collective-permute-start | bytes 1572872 | tf_op jit(solution)/shard_map/ppermute | solution.py:652
  64.4 26.5 %collective-permute-start.5 = (bf16[2048,128]{1,0:T(8,128)(2,1)}, bf16[2048,128]{1,0:T(8,128)(2,1)}, u32[]{:S(2)}, u32[]{:S(2)}) collective-permute-start(bf16[2048,128]{1,0:T(8,128)(2,1)} %get-tuple-element.47.rest_0_), channel_id=1, source_target_pairs={{0,1},{1,2},{2,3},{3,0},{4,5},{5,6},{6,7},{7,4},{8,9},{9,10},{10,1... | collective-permute-start | bytes 1572872 | tf_op jit(solution)/shard_map/ppermute | solution.py:652
  64.4 26.5 %collective-permute-start.6 = (bf16[2048,128]{1,0:T(8,128)(2,1)}, bf16[2048,128]{1,0:T(8,128)(2,1)}, u32[]{:S(2)}, u32[]{:S(2)}) collective-permute-start(bf16[2048,128]{1,0:T(8,128)(2,1)} %get-tuple-element.47.rest_0_), channel_id=1, source_target_pairs={{0,2},{1,3},{2,0},{3,1},{4,6},{5,7},{6,4},{7,5},{8,10},{9,11},{10,... | collective-permute-start | bytes 1572872 | tf_op jit(solution)/shard_map/ppermute | solution.py:652
  70.3 20.6 %copy-start = (bf16[1024,2048]{1,0:T(8,128)(2,1)}, bf16[1024,2048]{1,0:T(8,128)(2,1)S(1)}, u32[]{:S(2)}) copy-start(bf16[1024,2048]{1,0:T(8,128)(2,1)S(1)} %turn.1.xt_ref) | copy-start | bytes 12582916
  95.8 7.5 %copy-start.14 = (bf16[2048,128]{1,0:T(8,128)(2,1)S(1)}, bf16[2048,128]{1,0:T(8,128)(2,1)}, u32[]{:S(2)}) copy-start(bf16[2048,128]{1,0:T(8,128)(2,1)} %get-tuple-element.41.rest_0_) | copy-start | bytes 1572868
  95.8 62.0 %all-to-all-start.4 = ((bf16[32,2,4,32,128]{4,3,2,1,0:T(8,128)(2,1)}), bf16[32,2,4,32,128]{4,3,2,1,0:T(8,128)(2,1)}, u32[]{:S(2)}, u32[]{:S(2)}) async-start(bf16[32,2,4,32,128]{4,3,2,1,0:T(8,128)(2,1)} %weigh.4), calls=%async_computation.4 | async-start | bytes 4194304 | tf_op jit(solution)/shard_map/all_to_all | solution.py:648
  103.4 14.9 %collective-permute-start = (bf16[2048,128]{1,0:T(8,128)(2,1)S(1)}, bf16[2048,128]{1,0:T(8,128)(2,1)S(1)}, u32[]{:S(2)}, u32[]{:S(2)}) collective-permute-start(bf16[2048,128]{1,0:T(8,128)(2,1)S(1)} %copy-done.14), channel_id=1, source_target_pairs={{0,3},{1,0},{2,1},{3,2},{4,7},{5,4},{6,5},{7,6},{8,11},{9,8},{10,9... | collective-permute-start | bytes 1572872 | tf_op jit(solution)/shard_map/ppermute | solution.py:652
  103.7 26.3 %collective-permute-start.1 = (bf16[2048,128]{1,0:T(8,128)(2,1)S(1)}, bf16[2048,128]{1,0:T(8,128)(2,1)S(1)}, u32[]{:S(2)}, u32[]{:S(2)}) collective-permute-start(bf16[2048,128]{1,0:T(8,128)(2,1)S(1)} %copy-done.14), channel_id=1, source_target_pairs={{0,1},{1,2},{2,3},{3,0},{4,5},{5,6},{6,7},{7,4},{8,9},{9,10},{10,1... | collective-permute-start | bytes 1572872 | tf_op jit(solution)/shard_map/ppermute | solution.py:652
  105.5 25.4 %collective-permute-start.2 = (bf16[2048,128]{1,0:T(8,128)(2,1)S(1)}, bf16[2048,128]{1,0:T(8,128)(2,1)}, u32[]{:S(2)}, u32[]{:S(2)}) collective-permute-start(bf16[2048,128]{1,0:T(8,128)(2,1)S(1)} %copy-done.14), channel_id=1, source_target_pairs={{0,2},{1,3},{2,0},{3,1},{4,6},{5,7},{6,4},{7,5},{8,10},{9,11},{10,... | collective-permute-start | bytes 1572872 | tf_op jit(solution)/shard_map/ppermute | solution.py:652
  118.2 11.8 %copy-start.17 = (bf16[2048,128]{1,0:T(8,128)(2,1)}, bf16[2048,128]{1,0:T(8,128)(2,1)S(1)}, u32[]{:S(2)}) copy-start(bf16[2048,128]{1,0:T(8,128)(2,1)S(1)} %collective-permute-done.rest_1_) | copy-start | bytes 1572868
  130.0 0.8 copy-start.19
  130.8 2.2 copy-start.1
  138.0 16.9 %collective-permute-start.3 = (bf16[32,2,32,128]{3,2,1,0:T(8,128)(2,1)}, bf16[32,2,32,128]{3,2,1,0:T(8,128)(2,1)S(1)}, u32[]{:S(2)}, u32[]{:S(2)}) collective-permute-start(bf16[32,2,32,128]{3,2,1,0:T(8,128)(2,1)} %get-tuple-element.43), channel_id=1, source_target_pairs={{0,4},{4,0},{8,12},{12,8},{16,20},{20,16},{24,28},{28,24},{32,36},... | collective-permute-start | bytes 1572872 | tf_op jit(solution)/shard_map/ppermute | solution.py:687
  154.9 0.8 copy-start.13
  157.9 7.6 %copy-start.15 = (bf16[2048,128]{1,0:T(8,128)(2,1)S(1)}, bf16[2048,128]{1,0:T(8,128)(2,1)}, u32[]{:S(2)}) copy-start(bf16[2048,128]{1,0:T(8,128)(2,1)} %get-tuple-element.59.rest_0_) | copy-start | bytes 1572868
  157.9 47.6 %all-to-all-start.3 = ((bf16[32,6,32,128]{3,2,1,0:T(8,128)(2,1)}), bf16[32,6,32,128]{3,2,1,0:T(8,128)(2,1)}, u32[]{:S(2)}, u32[]{:S(2)}) async-start(bf16[32,6,32,128]{3,2,1,0:T(8,128)(2,1)} %join.2), calls=%async_computation.3 | async-start | bytes 3145728 | tf_op jit(solution)/shard_map/all_to_all | solution.py:648
  165.5 14.9 %collective-permute-start.7 = (bf16[2048,128]{1,0:T(8,128)(2,1)S(1)}, bf16[2048,128]{1,0:T(8,128)(2,1)S(1)}, u32[]{:S(2)}, u32[]{:S(2)}) collective-permute-start(bf16[2048,128]{1,0:T(8,128)(2,1)S(1)} %copy-done.15), channel_id=1, source_target_pairs={{0,3},{1,0},{2,1},{3,2},{4,7},{5,4},{6,5},{7,6},{8,11},{9,8},{10,9... | collective-permute-start | bytes 1572872 | tf_op jit(solution)/shard_map/ppermute | solution.py:652
  166.2 26.2 %collective-permute-start.8 = (bf16[2048,128]{1,0:T(8,128)(2,1)S(1)}, bf16[2048,128]{1,0:T(8,128)(2,1)S(1)}, u32[]{:S(2)}, u32[]{:S(2)}) collective-permute-start(bf16[2048,128]{1,0:T(8,128)(2,1)S(1)} %copy-done.15), channel_id=1, source_target_pairs={{0,1},{1,2},{2,3},{3,0},{4,5},{5,6},{6,7},{7,4},{8,9},{9,10},{10,1... | collective-permute-start | bytes 1572872 | tf_op jit(solution)/shard_map/ppermute | solution.py:652
  167.6 25.6 %collective-permute-start.9 = (bf16[2048,128]{1,0:T(8,128)(2,1)S(1)}, bf16[2048,128]{1,0:T(8,128)(2,1)}, u32[]{:S(2)}, u32[]{:S(2)}) collective-permute-start(bf16[2048,128]{1,0:T(8,128)(2,1)S(1)} %copy-done.15), channel_id=1, source_target_pairs={{0,2},{1,3},{2,0},{3,1},{4,6},{5,7},{6,4},{7,5},{8,10},{9,11},{10,... | collective-permute-start | bytes 1572872 | tf_op jit(solution)/shard_map/ppermute | solution.py:652
  180.4 12.1 %copy-start.16 = (bf16[2048,128]{1,0:T(8,128)(2,1)}, bf16[2048,128]{1,0:T(8,128)(2,1)S(1)}, u32[]{:S(2)}) copy-start(bf16[2048,128]{1,0:T(8,128)(2,1)S(1)} %collective-permute-done.7.rest_1_) | copy-start | bytes 1572868
  192.4 0.8 copy-start.18
  193.2 2.2 copy-start.2
  200.3 12.6 %copy-start.7 = (f32[2048,128]{1,0:T(8,128)S(1)}, f32[2048,128]{1,0:T(8,128)}, u32[]{:S(2)}) copy-start(f32[2048,128]{1,0:T(8,128)} %get-tuple-element.51.dko_ref) | copy-start | bytes 3145732
  200.3 12.6 %copy-start.8 = (f32[2048,128]{1,0:T(8,128)S(1)}, f32[2048,128]{1,0:T(8,128)}, u32[]{:S(2)}) copy-start(f32[2048,128]{1,0:T(8,128)} %get-tuple-element.52.dvo_ref) | copy-start | bytes 3145732
  200.3 12.6 %copy-start.9 = (s32[8,128]{1,0:T(8,128)S(1)}, s32[8,128]{1,0:T(8,128)}, u32[]{:S(2)}) copy-start(s32[8,128]{1,0:T(8,128)} %get-tuple-element.34.tab_ref) | copy-start | bytes 12292
  200.4 2.2 collective-permute-start.10
  202.6 0.8 copy-start.12
  205.5 18.9 %all-to-all-start.5 = ((bf16[32,2,32,128]{3,2,1,0:T(8,128)(2,1)}), bf16[32,2,32,128]{3,2,1,0:T(8,128)(2,1)}, u32[]{:S(2)}, u32[]{:S(2)}) async-start(bf16[32,2,32,128]{3,2,1,0:T(8,128)(2,1)} %join.3), calls=%async_computation.5 | async-start | bytes 1048576 | tf_op jit(solution)/shard_map/all_to_all | solution.py:648
  212.9 5.6 %copy-start.3 = (f32[2048,128]{1,0:T(8,128)S(1)}, f32[2048,128]{1,0:T(8,128)}, u32[]{:S(2)}) copy-start(f32[2048,128]{1,0:T(8,128)} %get-tuple-element.49.dko_ref) | copy-start | bytes 3145732
  212.9 5.6 %copy-start.4 = (f32[2048,128]{1,0:T(8,128)S(1)}, f32[2048,128]{1,0:T(8,128)}, u32[]{:S(2)}) copy-start(f32[2048,128]{1,0:T(8,128)} %get-tuple-element.50.dvo_ref) | copy-start | bytes 3145732
  221.9 4.3 %copy-start.5 = (f32[2048,128]{1,0:T(8,128)S(1)}, f32[2048,128]{1,0:T(8,128)}, u32[]{:S(2)}) copy-start(f32[2048,128]{1,0:T(8,128)} %get-tuple-element.45.dko_ref) | copy-start | bytes 3145732
  221.9 4.3 %copy-start.6 = (f32[2048,128]{1,0:T(8,128)S(1)}, f32[2048,128]{1,0:T(8,128)}, u32[]{:S(2)}) copy-start(f32[2048,128]{1,0:T(8,128)} %get-tuple-element.46.dvo_ref) | copy-start | bytes 3145732

commit v6 on v5

--- a/solution.py
+++ b/solution.py
@@ -35,7 +35,7 @@
                 send[2 * m + odd, CAP + c] = v_ref[b, :, lanes]
         return carry
 
-    lax.fori_loop(0, half, fill, 0, unroll=2)
+    lax.fori_loop(0, half, fill, 0)
 
 
 def first_kernel(me_ref, chosen_ref, k_ref, v_ref, send, tab_ref, lo_s, hi_s, tab_v, tab_s, sem,
@@ -84,7 +84,8 @@
     row = lax.broadcasted_iota(jnp.int32, (128, blocks * KEY_BLOCK), 0)
     expand = ((place + (me % 2) * blocks) == row).astype(jnp.bfloat16)
     start = pl.multiple_of((me // 2) * 128, 128)
-    for h in range(heads):
+
+    def one(h, carry):
         ids = chosen_ref[h, :, pl.ds(start, 128)]
         cols = [jnp.broadcast_to(ids[c : c + 1, :], (slots, 128)) for c in range(picks)]
         least = jnp.full((slots, 128), BIG, jnp.int32)
@@ -104,6 +105,9 @@
         hot = jnp.where(named, 1.0, 0.0).astype(jnp.bfloat16)
         full = jnp.dot(hot, expand, preferred_element_type=jnp.float32)
         bias_ref[h] = jnp.where(full > 0.5, 0.0, NEG)
+        return carry
+
+    lax.fori_loop(0, heads, one, 0)
 
 
 def turn_kernel(x_ref, out_ref):
@@ -140,7 +144,7 @@
             o_s[pair, owners, 1] = got[:, HEAD_DIM:].reshape(shape)
             return carry
 
-        lax.fori_loop(0, rows // WEIGH_ROWS, some, 0)
+        lax.fori_loop(0, rows // WEIGH_ROWS, some, 0, unroll=not halves)
         if halves:
             core = me_ref[0] % 2
             for out, mine in ((outs[0], core == pair), (outs[1], core != pair)):
@@ -327,15 +331,10 @@
         if merge:
             me = me_ref[0]
             for n in range(shape[0]):
-
-                @pl.when(n < me)
-                def _(n=n):
-                    back_ref[n, 0:CAP] = dk[n]
-                    back_ref[n, CAP : 2 * CAP] = dv[n]
-
-                @pl.when(n >= me)
-                def _(n=n):
-                    back_ref[n] = ahead_ref[n]
+                back_ref[n, 0:CAP] = jnp.where(n < me, dk[n], ahead_ref[n, 0:CAP])
+                back_ref[n, CAP : 2 * CAP] = jnp.where(
+                    n < me, dv[n], ahead_ref[n, CAP : 2 * CAP]
+                )
         else:
             back_ref[:, 0:CAP] = dk
             back_ref[:, CAP : 2 * CAP] = dv

time: 232 us -> 232 us (level)
  no operation moved by 1% of the time
where the time goes in v6:
time: 232 us; the launch traced here: 230 us
  Pallas kernels  101 us (44%)
  waiting for transfers between devices  66.1 us (28%)
  starting transfers between devices  53.9 us (23%)
  local copies, waits for them, and re-layouts  7.63 us (3%)
    pallas_call x3, Pallas kernels, attend(): pl.pallas_call(functools.partial(attend_kernel, head=head, extra=len(alia...  51.4 us
    ppermute x9, waiting for transfers between devices, shift(): return lax.ppermute(x, 'tp', [(i, (i + by) % tp) for i in range(tp)])  50.1 us
    all_to_all x6, starting transfers between devices, exchange(): return lax.all_to_all(x, 'kv', split_axis=0, concat_axis=0, tiled=True)  42.3 us
    pallas_call x3, Pallas kernels, weigh(): pl.pallas_call(functools.partial(weight_kernel, extra=len(aliases), slot=...  14.4 us
    all_to_all x6, waiting for transfers between devices, exchange(): return lax.all_to_all(x, 'kv', split_axis=0, concat_axis=0, tiled=True)  13.9 us
    ppermute x9, starting transfers between devices, shift(): return lax.ppermute(x, 'tp', [(i, (i + by) % tp) for i in range(tp)])  11.2 us
    pallas_call x3, Pallas kernels, land(): pl.pallas_call(functools.partial(land_kernel, head=head, spans=spans), gr...  10.3 us
    unnamed x40, local copies, waits for them, and re-layouts  7.63 us
  transfers between devices with their start and end apart: 17, of which 8 were waited for; matrix products, arithmetic and copies ran while one was open for 0% of the time, Pallas kernels for 40%

profile of v6, /device:TPU:0, one launch (start us, length us, event | category | flops | bytes accessed | tf_op | source)
XLA Modules:
  0.0 229.6 jit_solution(2060929565502525269)
XLA Ops:
  0.6 3.6 %first.1 = (bf16[32,1,4,32,128]{4,3,2,1,0:T(8,128)(2,1)}, s32[8,128]{1,0:T(8,128)}) custom-call(s32[1]{0:T(128)} %bitcast.me_ref, s32[3,12,2048]{2,1,0:T(8,128)} %bitcast.9, bf16[64,32,384]{2,1,0:T(8,128)(2,1)} %bitcast.5, bf16[64,32,384]{2,1,0:T(8,128)(2,1)} %bitcast.7), custom_call_target="tpu_custom_call" | custom-call | flops 67108864 | bytes 1048576 | tf_op jit(solution)/shard_map/first/pallas_call | solution.py:395
  4.2 8.5 %all-to-all-start = ((bf16[32,1,4,32,128]{4,3,2,1,0:T(8,128)(2,1)}), bf16[32,1,4,32,128]{4,3,2,1,0:T(8,128)(2,1)S(1)}, u32[]{:S(2)}, u32[]{:S(2)}) async-start(bf16[32,1,4,32,128]{4,3,2,1,0:T(8,128)(2,1)} %get-tuple-element.33), calls=%async_computation | async-start | bytes 2097152 | tf_op jit(solution)/shard_map/all_to_all | solution.py:647
  12.7 3.9 %pack.1 = (bf16[32,1,4,32,128]{4,3,2,1,0:T(8,128)(2,1)}, bf16[32,1,4,32,128]{4,3,2,1,0:T(8,128)(2,1)}) custom-call(s32[8,128]{1,0:T(8,128)} %get-tuple-element.34.tab_ref, bf16[64,32,384]{2,1,0:T(8,128)(2,1)} %bitcast.6, bf16[64,32,384]{2,1,0:T(8,128)(2,1)} %bitcast.8), custom_call_target="tpu_custom_call" | custom-call | flops 67108864 | bytes 1048576 | tf_op jit(solution)/shard_map/pack/pallas_call | solution.py:418
  16.7 13.3 %all-to-all-done.refs_6_ = bf16[32,1,4,32,128]{4,3,2,1,0:T(8,128)(2,1)S(1)} async-done(((bf16[32,1,4,32,128]{4,3,2,1,0:T(8,128)(2,1)}), bf16[32,1,4,32,128]{4,3,2,1,0:T(8,128)(2,1)S(1)}, u32[]{:S(2)}, u32[]{:S(2)}) %all-to-all-start) | async-done | bytes 1048608 | tf_op jit(solution)/shard_map/all_to_all | solution.py:647
  29.9 3.9 %all-to-all-start.2 = ((bf16[32,1,4,32,128]{4,3,2,1,0:T(8,128)(2,1)}), bf16[32,1,4,32,128]{4,3,2,1,0:T(8,128)(2,1)S(1)}, u32[]{:S(2)}, u32[]{:S(2)}) async-start(bf16[32,1,4,32,128]{4,3,2,1,0:T(8,128)(2,1)} %get-tuple-element.37), calls=%async_computation.2 | async-start | bytes 2097152 | tf_op jit(solution)/shard_map/all_to_all | solution.py:647
  33.9 3.7 %mask.1.refs_5_ = f32[3,64,2048]{2,1,0:T(8,128)} custom-call(s32[1]{0:T(128)} %bitcast.me_ref, s32[3,12,2048]{2,1,0:T(8,128)} %bitcast.10), custom_call_target="tpu_custom_call" | custom-call | flops 67108864 | bytes 1048576 | tf_op jit(solution)/shard_map/mask/pallas_call | solution.py:432
  37.5 16.8 %shard_map.102 = (bf16[2048,384]{1,0:T(8,128)(2,1)}, bf16[2048,128]{1,0:T(8,128)(2,1)}, f32[2048,128]{1,0:T(8,128)}, f32[2048,128]{1,0:T(8,128)}, bf16[32,1,4,32,128]{4,3,2,1,0:T(8,128)(2,1)}) custom-call(s32[1]{0:T(128)} %bitcast.me_ref, bf16[2048,384]{1,0:T(8,128)(2,1)} %refs_0_.5, bf16[2048,384]{1,0:T(8,128)(2,1)} %refs_1_.5, bf16[2048,384]{1,0:T(8,128)(2,1)} %refs_2_.5, ...), custom_call_target="tpu_custom_call" | custom-call | flops 5368709120 | bytes 8388608 | tf_op jit(solution)/shard_map/pallas_call | solution.py:494
  54.4 7.5 %all-to-all-start.1 = ((bf16[32,1,4,32,128]{4,3,2,1,0:T(8,128)(2,1)}), bf16[32,1,4,32,128]{4,3,2,1,0:T(8,128)(2,1)}, u32[]{:S(2)}, u32[]{:S(2)}) async-start(bf16[32,1,4,32,128]{4,3,2,1,0:T(8,128)(2,1)} %get-tuple-element.36), calls=%async_computation.1 | async-start | bytes 2097152 | tf_op jit(solution)/shard_map/all_to_all | solution.py:647
  61.9 2.8 %collective-permute-start.4 = (bf16[2048,128]{1,0:T(8,128)(2,1)}, bf16[2048,128]{1,0:T(8,128)(2,1)}, u32[]{:S(2)}, u32[]{:S(2)}) collective-permute-start(bf16[2048,128]{1,0:T(8,128)(2,1)} %get-tuple-element.47.rest_0_), channel_id=1, source_target_pairs={{0,3},{1,0},{2,1},{3,2},{4,7},{5,4},{6,5},{7,6},{8,11},{9,8},{10,9... | collective-permute-start | bytes 1572872 | tf_op jit(solution)/shard_map/ppermute | solution.py:651
  64.7 2.3 %collective-permute-start.6 = (bf16[2048,128]{1,0:T(8,128)(2,1)}, bf16[2048,128]{1,0:T(8,128)(2,1)}, u32[]{:S(2)}, u32[]{:S(2)}) collective-permute-start(bf16[2048,128]{1,0:T(8,128)(2,1)} %get-tuple-element.47.rest_0_), channel_id=1, source_target_pairs={{0,2},{1,3},{2,0},{3,1},{4,6},{5,7},{6,4},{7,5},{8,10},{9,11},{10,... | collective-permute-start | bytes 1572872 | tf_op jit(solution)/shard_map/ppermute | solution.py:651
  67.0 3.6 %turn.1.xt_ref = bf16[1024,2048]{1,0:T(8,128)(2,1)S(1)} custom-call(bf16[2048,1024]{1,0:T(8,128)(2,1)} %x_ref.1), custom_call_target="tpu_custom_call" | custom-call | flops 67108864 | bytes 1048576 | tf_op jit(solution)/shard_map/turn/pallas_call | solution.py:445
  70.6 18.0 %shard_map.103 = (bf16[2048,384]{1,0:T(8,128)(2,1)}, bf16[2048,128]{1,0:T(8,128)(2,1)}, f32[2048,128]{1,0:T(8,128)}, f32[2048,128]{1,0:T(8,128)}, bf16[32,2,4,32,128]{4,3,2,1,0:T(8,128)(2,1)}) custom-call(s32[1]{0:T(128)} %bitcast.me_ref, bf16[2048,384]{1,0:T(8,128)(2,1)} %refs_0_.5, bf16[2048,384]{1,0:T(8,128)(2,1)} %refs_1_.5, ...), custom_call_target="tpu_custom_call", output_to_operand_aliasing={{0}: (8, {})} | custom-call | flops 5368709120 | bytes 8388608 | tf_op jit(solution)/shard_map/pallas_call | solution.py:494
  88.7 2.6 %collective-permute-done.5.rest_2_ = bf16[2048,128]{1,0:T(8,128)(2,1)} collective-permute-done((bf16[2048,128]{1,0:T(8,128)(2,1)}, bf16[2048,128]{1,0:T(8,128)(2,1)}, u32[]{:S(2)}, u32[]{:S(2)}) %collective-permute-start.5) | collective-permute-done | bytes 524320 | tf_op jit(solution)/shard_map/ppermute | solution.py:651
  91.3 4.5 %weigh.4 = bf16[32,2,4,32,128]{4,3,2,1,0:T(8,128)(2,1)} custom-call(s32[1]{0:T(128)} %bitcast.me_ref, bf16[1024,2048]{1,0:T(8,128)(2,1)S(1)} %turn.1.xt_ref, bf16[2048,128]{1,0:T(8,128)(2,1)} %get-tuple-element.47.rest_0_, bf16[2048,128]{1,0:T(8,128)(2,1)} %collective-permute-done.4.rest_1_, ...), custom_call_target="tpu_custom_call", output_to_operand_aliasing={{}: (6, {})} | custom-call | flops 2147483648 | bytes 8388608 | tf_op jit(solution)/shard_map/weigh/pallas_call | solution.py:542
  95.8 7.5 %all-to-all-start.4 = ((bf16[32,2,4,32,128]{4,3,2,1,0:T(8,128)(2,1)}), bf16[32,2,4,32,128]{4,3,2,1,0:T(8,128)(2,1)}, u32[]{:S(2)}, u32[]{:S(2)}) async-start(bf16[32,2,4,32,128]{4,3,2,1,0:T(8,128)(2,1)} %weigh.4), calls=%async_computation.4 | async-start | bytes 4194304 | tf_op jit(solution)/shard_map/all_to_all | solution.py:647
  103.3 0.4 collective-permute-start
  103.7 1.7 collective-permute-start.1
  105.4 0.6 collective-permute-start.2
  106.0 12.2 %collective-permute-done.rest_1_ = bf16[2048,128]{1,0:T(8,128)(2,1)S(1)} collective-permute-done((bf16[2048,128]{1,0:T(8,128)(2,1)S(1)}, bf16[2048,128]{1,0:T(8,128)(2,1)S(1)}, u32[]{:S(2)}, u32[]{:S(2)}) %collective-permute-start) | collective-permute-done | bytes 524320 | tf_op jit(solution)/shard_map/ppermute | solution.py:651
  118.2 11.8 %collective-permute-done.1.rest_2_ = bf16[2048,128]{1,0:T(8,128)(2,1)S(1)} collective-permute-done((bf16[2048,128]{1,0:T(8,128)(2,1)S(1)}, bf16[2048,128]{1,0:T(8,128)(2,1)S(1)}, u32[]{:S(2)}, u32[]{:S(2)}) %collective-permute-start.1) | collective-permute-done | bytes 524320 | tf_op jit(solution)/shard_map/ppermute | solution.py:651
  130.0 0.8 copy-done.19
  130.8 2.2 copy-done.1
  133.0 4.9 %weigh.3 = (bf16[32,2,32,128]{3,2,1,0:T(8,128)(2,1)}, bf16[32,2,32,128]{3,2,1,0:T(8,128)(2,1)}) custom-call(s32[1]{0:T(128)} %bitcast.me_ref, bf16[1024,2048]{1,0:T(8,128)(2,1)S(1)} %copy-done.1, bf16[2048,128]{1,0:T(8,128)(2,1)} %get-tuple-element.41.rest_0_, bf16[2048,128]{1,0:T(8,128)(2,1)} %copy-done.17, bf16[2048,128]{1,0:T(8,128)(2,1)} %copy-done.19, ...), custom_call_target="tpu_custom_call" | custom-call | flops 2147483648 | bytes 8388608 | tf_op jit(solution)/shard_map/weigh/pallas_call | solution.py:542
  137.9 0.3 collective-permute-start.3
  138.3 16.6 %shard_map.104 = (bf16[2048,384]{1,0:T(8,128)(2,1)}, bf16[2048,128]{1,0:T(8,128)(2,1)}, f32[2048,128]{1,0:T(8,128)}, f32[2048,128]{1,0:T(8,128)}, bf16[32,6,32,128]{3,2,1,0:T(8,128)(2,1)}) custom-call(s32[1]{0:T(128)} %bitcast.me_ref, bf16[2048,384]{1,0:T(8,128)(2,1)} %refs_0_.5, bf16[2048,384]{1,0:T(8,128)(2,1)} %refs_1_.5, ...), custom_call_target="tpu_custom_call", output_to_operand_aliasing={{0}: (8, {})} | custom-call | flops 5368709120 | bytes 8388608 | tf_op jit(solution)/shard_map/pallas_call | solution.py:494
  154.8 0.8 copy-done.13
  155.6 2.2 join.2
  157.9 7.6 %all-to-all-start.3 = ((bf16[32,6,32,128]{3,2,1,0:T(8,128)(2,1)}), bf16[32,6,32,128]{3,2,1,0:T(8,128)(2,1)}, u32[]{:S(2)}, u32[]{:S(2)}) async-start(bf16[32,6,32,128]{3,2,1,0:T(8,128)(2,1)} %join.2), calls=%async_computation.3 | async-start | bytes 3145728 | tf_op jit(solution)/shard_map/all_to_all | solution.py:647
  165.5 0.7 collective-permute-start.7
  166.2 1.4 collective-permute-start.8
  167.6 1.2 collective-permute-start.9
  168.8 11.5 %collective-permute-done.7.rest_1_ = bf16[2048,128]{1,0:T(8,128)(2,1)S(1)} collective-permute-done((bf16[2048,128]{1,0:T(8,128)(2,1)S(1)}, bf16[2048,128]{1,0:T(8,128)(2,1)S(1)}, u32[]{:S(2)}, u32[]{:S(2)}) %collective-permute-start.7) | collective-permute-done | bytes 524320 | tf_op jit(solution)/shard_map/ppermute | solution.py:651
  180.3 12.1 %collective-permute-done.8.rest_2_ = bf16[2048,128]{1,0:T(8,128)(2,1)S(1)} collective-permute-done((bf16[2048,128]{1,0:T(8,128)(2,1)S(1)}, bf16[2048,128]{1,0:T(8,128)(2,1)S(1)}, u32[]{:S(2)}, u32[]{:S(2)}) %collective-permute-start.8) | collective-permute-done | bytes 524320 | tf_op jit(solution)/shard_map/ppermute | solution.py:651
  192.4 0.8 copy-done.18
  193.2 2.2 copy-done.2
  195.4 4.9 %weigh.5 = (bf16[32,2,32,128]{3,2,1,0:T(8,128)(2,1)}, bf16[32,2,32,128]{3,2,1,0:T(8,128)(2,1)}) custom-call(s32[1]{0:T(128)} %bitcast.me_ref, bf16[1024,2048]{1,0:T(8,128)(2,1)S(1)} %copy-done.2, bf16[2048,128]{1,0:T(8,128)(2,1)} %get-tuple-element.59.rest_0_, bf16[2048,128]{1,0:T(8,128)(2,1)} %copy-done.16, bf16[2048,128]{1,0:T(8,128)(2,1)} %copy-done.18, ...), custom_call_target="tpu_custom_call" | custom-call | flops 2147483648 | bytes 8388608 | tf_op jit(solution)/shard_map/weigh/pallas_call | solution.py:542
  200.3 0.1 collective-permute-start.10
  200.4 2.1 collective-permute-done.10.got_ref
  202.5 0.8 copy-done.12
  203.3 2.1 join.3
  205.5 7.4 %all-to-all-start.5 = ((bf16[32,2,32,128]{3,2,1,0:T(8,128)(2,1)}), bf16[32,2,32,128]{3,2,1,0:T(8,128)(2,1)}, u32[]{:S(2)}, u32[]{:S(2)}) async-start(bf16[32,2,32,128]{3,2,1,0:T(8,128)(2,1)} %join.3), calls=%async_computation.5 | async-start | bytes 1048576 | tf_op jit(solution)/shard_map/all_to_all | solution.py:647
  212.9 3.5 %shard_map.105 = (f32[2048,384]{1,0:T(8,128)}, f32[2048,384]{1,0:T(8,128)}) custom-call(s32[1]{0:T(128)} %bitcast.me_ref, s32[8,128]{1,0:T(8,128)S(1)} %copy-done.9, bf16[32,1,4,32,128]{4,3,2,1,0:T(8,128)(2,1)} %all-to-all-done.1.refs_6_.back_ref, f32[2048,128]{1,0:T(8,128)S(1)} %copy-done.7, f32[2048,128]{1,0:T(8,128)S(1)} %copy-done.8), custom_call_target="tpu_custom_call" | custom-call | flops 16777216 | bytes 1048576 | tf_op jit(solution)/shard_map/pallas_call | solution.py:634
  216.4 2.1 total.1.before_ref
  218.5 3.4 %shard_map.106 = (f32[2048,384]{1,0:T(8,128)}, f32[2048,384]{1,0:T(8,128)}) custom-call(s32[1]{0:T(128)} %bitcast.me_ref, s32[8,128]{1,0:T(8,128)S(1)} %copy-done.9, bf16[32,2,4,32,128]{4,3,2,1,0:T(8,128)(2,1)} %all-to-all-done.4.back_ref.got_ref, f32[2048,128]{1,0:T(8,128)S(1)} %copy-done.3, ...), custom_call_target="tpu_custom_call", output_to_operand_aliasing={{0}: (5, {}), {1}: (6, {})} | custom-call | flops 16777216 | bytes 1048576 | tf_op jit(solution)/shard_map/pallas_call | solution.py:634
  221.9 1.9 pairtotal.2.before_ref
  223.8 0.6 all-to-all-done.5.got_ref
  224.4 1.8 pairtotal.3
  226.2 3.4 %shard_map.107 = (f32[2048,384]{1,0:T(8,128)}, f32[2048,384]{1,0:T(8,128)}) custom-call(s32[1]{0:T(128)} %bitcast.me_ref, s32[8,128]{1,0:T(8,128)S(1)} %copy-done.9, bf16[32,6,32,128]{3,2,1,0:T(8,128)(2,1)} %all-to-all-done.3.back_ref.got_ref, f32[2048,128]{1,0:T(8,128)S(1)} %copy-done.5, ...), custom_call_target="tpu_custom_call", output_to_operand_aliasing={{0}: (5, {}), {1}: (6, {})} | custom-call | flops 16777216 | bytes 1048576 | tf_op jit(solution)/shard_map/pallas_call | solution.py:634
  (44 shorter events, 0.1 us)
Async XLA Ops:
  4.2 25.7 %all-to-all-start = ((bf16[32,1,4,32,128]{4,3,2,1,0:T(8,128)(2,1)}), bf16[32,1,4,32,128]{4,3,2,1,0:T(8,128)(2,1)S(1)}, u32[]{:S(2)}, u32[]{:S(2)}) async-start(bf16[32,1,4,32,128]{4,3,2,1,0:T(8,128)(2,1)} %get-tuple-element.33), calls=%async_computation | async-start | bytes 2097152 | tf_op jit(solution)/shard_map/all_to_all | solution.py:647
  29.9 7.6 %copy-start.11 = (bf16[32,1,4,32,128]{4,3,2,1,0:T(8,128)(2,1)}, bf16[32,1,4,32,128]{4,3,2,1,0:T(8,128)(2,1)S(1)}, u32[]{:S(2)}) copy-start(bf16[32,1,4,32,128]{4,3,2,1,0:T(8,128)(2,1)S(1)} %all-to-all-done.refs_6_) | copy-start | bytes 3145732
  29.9 24.5 %all-to-all-start.2 = ((bf16[32,1,4,32,128]{4,3,2,1,0:T(8,128)(2,1)}), bf16[32,1,4,32,128]{4,3,2,1,0:T(8,128)(2,1)S(1)}, u32[]{:S(2)}, u32[]{:S(2)}) async-start(bf16[32,1,4,32,128]{4,3,2,1,0:T(8,128)(2,1)} %get-tuple-element.37), calls=%async_computation.2 | async-start | bytes 2097152 | tf_op jit(solution)/shard_map/all_to_all | solution.py:647
  54.4 10.4 %copy-start.10 = (bf16[32,1,4,32,128]{4,3,2,1,0:T(8,128)(2,1)}, bf16[32,1,4,32,128]{4,3,2,1,0:T(8,128)(2,1)S(1)}, u32[]{:S(2)}) copy-start(bf16[32,1,4,32,128]{4,3,2,1,0:T(8,128)(2,1)S(1)} %all-to-all-done.2.refs_6_) | copy-start | bytes 3145732
  54.4 41.4 %all-to-all-start.1 = ((bf16[32,1,4,32,128]{4,3,2,1,0:T(8,128)(2,1)}), bf16[32,1,4,32,128]{4,3,2,1,0:T(8,128)(2,1)}, u32[]{:S(2)}, u32[]{:S(2)}) async-start(bf16[32,1,4,32,128]{4,3,2,1,0:T(8,128)(2,1)} %get-tuple-element.36), calls=%async_computation.1 | async-start | bytes 2097152 | tf_op jit(solution)/shard_map/all_to_all | solution.py:647
  61.9 26.7 %collective-permute-start.4 = (bf16[2048,128]{1,0:T(8,128)(2,1)}, bf16[2048,128]{1,0:T(8,128)(2,1)}, u32[]{:S(2)}, u32[]{:S(2)}) collective-permute-start(bf16[2048,128]{1,0:T(8,128)(2,1)} %get-tuple-element.47.rest_0_), channel_id=1, source_target_pairs={{0,3},{1,0},{2,1},{3,2},{4,7},{5,4},{6,5},{7,6},{8,11},{9,8},{10,9... | collective-permute-start | bytes 1572872 | tf_op jit(solution)/shard_map/ppermute | solution.py:651
  64.7 26.5 %collective-permute-start.5 = (bf16[2048,128]{1,0:T(8,128)(2,1)}, bf16[2048,128]{1,0:T(8,128)(2,1)}, u32[]{:S(2)}, u32[]{:S(2)}) collective-permute-start(bf16[2048,128]{1,0:T(8,128)(2,1)} %get-tuple-element.47.rest_0_), channel_id=1, source_target_pairs={{0,1},{1,2},{2,3},{3,0},{4,5},{5,6},{6,7},{7,4},{8,9},{9,10},{10,1... | collective-permute-start | bytes 1572872 | tf_op jit(solution)/shard_map/ppermute | solution.py:651
  64.7 26.5 %collective-permute-start.6 = (bf16[2048,128]{1,0:T(8,128)(2,1)}, bf16[2048,128]{1,0:T(8,128)(2,1)}, u32[]{:S(2)}, u32[]{:S(2)}) collective-permute-start(bf16[2048,128]{1,0:T(8,128)(2,1)} %get-tuple-element.47.rest_0_), channel_id=1, source_target_pairs={{0,2},{1,3},{2,0},{3,1},{4,6},{5,7},{6,4},{7,5},{8,10},{9,11},{10,... | collective-permute-start | bytes 1572872 | tf_op jit(solution)/shard_map/ppermute | solution.py:651
  70.6 20.6 %copy-start = (bf16[1024,2048]{1,0:T(8,128)(2,1)}, bf16[1024,2048]{1,0:T(8,128)(2,1)S(1)}, u32[]{:S(2)}) copy-start(bf16[1024,2048]{1,0:T(8,128)(2,1)S(1)} %turn.1.xt_ref) | copy-start | bytes 12582916
  95.8 7.5 %copy-start.14 = (bf16[2048,128]{1,0:T(8,128)(2,1)S(1)}, bf16[2048,128]{1,0:T(8,128)(2,1)}, u32[]{:S(2)}) copy-start(bf16[2048,128]{1,0:T(8,128)(2,1)} %get-tuple-element.41.rest_0_) | copy-start | bytes 1572868
  95.8 62.0 %all-to-all-start.4 = ((bf16[32,2,4,32,128]{4,3,2,1,0:T(8,128)(2,1)}), bf16[32,2,4,32,128]{4,3,2,1,0:T(8,128)(2,1)}, u32[]{:S(2)}, u32[]{:S(2)}) async-start(bf16[32,2,4,32,128]{4,3,2,1,0:T(8,128)(2,1)} %weigh.4), calls=%async_computation.4 | async-start | bytes 4194304 | tf_op jit(solution)/shard_map/all_to_all | solution.py:647
  103.3 14.9 %collective-permute-start = (bf16[2048,128]{1,0:T(8,128)(2,1)S(1)}, bf16[2048,128]{1,0:T(8,128)(2,1)S(1)}, u32[]{:S(2)}, u32[]{:S(2)}) collective-permute-start(bf16[2048,128]{1,0:T(8,128)(2,1)S(1)} %copy-done.14), channel_id=1, source_target_pairs={{0,3},{1,0},{2,1},{3,2},{4,7},{5,4},{6,5},{7,6},{8,11},{9,8},{10,9... | collective-permute-start | bytes 1572872 | tf_op jit(solution)/shard_map/ppermute | solution.py:651
  103.7 26.3 %collective-permute-start.1 = (bf16[2048,128]{1,0:T(8,128)(2,1)S(1)}, bf16[2048,128]{1,0:T(8,128)(2,1)S(1)}, u32[]{:S(2)}, u32[]{:S(2)}) collective-permute-start(bf16[2048,128]{1,0:T(8,128)(2,1)S(1)} %copy-done.14), channel_id=1, source_target_pairs={{0,1},{1,2},{2,3},{3,0},{4,5},{5,6},{6,7},{7,4},{8,9},{9,10},{10,1... | collective-permute-start | bytes 1572872 | tf_op jit(solution)/shard_map/ppermute | solution.py:651
  105.4 25.4 %collective-permute-start.2 = (bf16[2048,128]{1,0:T(8,128)(2,1)S(1)}, bf16[2048,128]{1,0:T(8,128)(2,1)}, u32[]{:S(2)}, u32[]{:S(2)}) collective-permute-start(bf16[2048,128]{1,0:T(8,128)(2,1)S(1)} %copy-done.14), channel_id=1, source_target_pairs={{0,2},{1,3},{2,0},{3,1},{4,6},{5,7},{6,4},{7,5},{8,10},{9,11},{10,... | collective-permute-start | bytes 1572872 | tf_op jit(solution)/shard_map/ppermute | solution.py:651
  118.2 11.8 %copy-start.17 = (bf16[2048,128]{1,0:T(8,128)(2,1)}, bf16[2048,128]{1,0:T(8,128)(2,1)S(1)}, u32[]{:S(2)}) copy-start(bf16[2048,128]{1,0:T(8,128)(2,1)S(1)} %collective-permute-done.rest_1_) | copy-start | bytes 1572868
  130.0 0.8 copy-start.19
  130.8 2.2 copy-start.1
  137.9 16.9 %collective-permute-start.3 = (bf16[32,2,32,128]{3,2,1,0:T(8,128)(2,1)}, bf16[32,2,32,128]{3,2,1,0:T(8,128)(2,1)S(1)}, u32[]{:S(2)}, u32[]{:S(2)}) collective-permute-start(bf16[32,2,32,128]{3,2,1,0:T(8,128)(2,1)} %get-tuple-element.43), channel_id=1, source_target_pairs={{0,4},{4,0},{8,12},{12,8},{16,20},{20,16},{24,28},{28,24},{32,36},... | collective-permute-start | bytes 1572872 | tf_op jit(solution)/shard_map/ppermute | solution.py:686
  154.8 0.8 copy-start.13
  157.9 7.6 %copy-start.15 = (bf16[2048,128]{1,0:T(8,128)(2,1)S(1)}, bf16[2048,128]{1,0:T(8,128)(2,1)}, u32[]{:S(2)}) copy-start(bf16[2048,128]{1,0:T(8,128)(2,1)} %get-tuple-element.59.rest_0_) | copy-start | bytes 1572868
  157.9 47.6 %all-to-all-start.3 = ((bf16[32,6,32,128]{3,2,1,0:T(8,128)(2,1)}), bf16[32,6,32,128]{3,2,1,0:T(8,128)(2,1)}, u32[]{:S(2)}, u32[]{:S(2)}) async-start(bf16[32,6,32,128]{3,2,1,0:T(8,128)(2,1)} %join.2), calls=%async_computation.3 | async-start | bytes 3145728 | tf_op jit(solution)/shard_map/all_to_all | solution.py:647
  165.5 14.9 %collective-permute-start.7 = (bf16[2048,128]{1,0:T(8,128)(2,1)S(1)}, bf16[2048,128]{1,0:T(8,128)(2,1)S(1)}, u32[]{:S(2)}, u32[]{:S(2)}) collective-permute-start(bf16[2048,128]{1,0:T(8,128)(2,1)S(1)} %copy-done.15), channel_id=1, source_target_pairs={{0,3},{1,0},{2,1},{3,2},{4,7},{5,4},{6,5},{7,6},{8,11},{9,8},{10,9... | collective-permute-start | bytes 1572872 | tf_op jit(solution)/shard_map/ppermute | solution.py:651
  166.2 26.2 %collective-permute-start.8 = (bf16[2048,128]{1,0:T(8,128)(2,1)S(1)}, bf16[2048,128]{1,0:T(8,128)(2,1)S(1)}, u32[]{:S(2)}, u32[]{:S(2)}) collective-permute-start(bf16[2048,128]{1,0:T(8,128)(2,1)S(1)} %copy-done.15), channel_id=1, source_target_pairs={{0,1},{1,2},{2,3},{3,0},{4,5},{5,6},{6,7},{7,4},{8,9},{9,10},{10,1... | collective-permute-start | bytes 1572872 | tf_op jit(solution)/shard_map/ppermute | solution.py:651
  167.6 25.6 %collective-permute-start.9 = (bf16[2048,128]{1,0:T(8,128)(2,1)S(1)}, bf16[2048,128]{1,0:T(8,128)(2,1)}, u32[]{:S(2)}, u32[]{:S(2)}) collective-permute-start(bf16[2048,128]{1,0:T(8,128)(2,1)S(1)} %copy-done.15), channel_id=1, source_target_pairs={{0,2},{1,3},{2,0},{3,1},{4,6},{5,7},{6,4},{7,5},{8,10},{9,11},{10,... | collective-permute-start | bytes 1572872 | tf_op jit(solution)/shard_map/ppermute | solution.py:651
  180.3 12.1 %copy-start.16 = (bf16[2048,128]{1,0:T(8,128)(2,1)}, bf16[2048,128]{1,0:T(8,128)(2,1)S(1)}, u32[]{:S(2)}) copy-start(bf16[2048,128]{1,0:T(8,128)(2,1)S(1)} %collective-permute-done.7.rest_1_) | copy-start | bytes 1572868
  192.4 0.8 copy-start.18
  193.2 2.2 copy-start.2
  200.3 12.6 %copy-start.7 = (f32[2048,128]{1,0:T(8,128)S(1)}, f32[2048,128]{1,0:T(8,128)}, u32[]{:S(2)}) copy-start(f32[2048,128]{1,0:T(8,128)} %get-tuple-element.51.dko_ref) | copy-start | bytes 3145732
  200.3 12.6 %copy-start.8 = (f32[2048,128]{1,0:T(8,128)S(1)}, f32[2048,128]{1,0:T(8,128)}, u32[]{:S(2)}) copy-start(f32[2048,128]{1,0:T(8,128)} %get-tuple-element.52.dvo_ref) | copy-start | bytes 3145732
  200.3 12.6 %copy-start.9 = (s32[8,128]{1,0:T(8,128)S(1)}, s32[8,128]{1,0:T(8,128)}, u32[]{:S(2)}) copy-start(s32[8,128]{1,0:T(8,128)} %get-tuple-element.34.tab_ref) | copy-start | bytes 12292
  200.3 2.2 collective-permute-start.10
  202.5 0.8 copy-start.12
  205.5 18.9 %all-to-all-start.5 = ((bf16[32,2,32,128]{3,2,1,0:T(8,128)(2,1)}), bf16[32,2,32,128]{3,2,1,0:T(8,128)(2,1)}, u32[]{:S(2)}, u32[]{:S(2)}) async-start(bf16[32,2,32,128]{3,2,1,0:T(8,128)(2,1)} %join.3), calls=%async_computation.5 | async-start | bytes 1048576 | tf_op jit(solution)/shard_map/all_to_all | solution.py:647
  212.9 5.6 %copy-start.3 = (f32[2048,128]{1,0:T(8,128)S(1)}, f32[2048,128]{1,0:T(8,128)}, u32[]{:S(2)}) copy-start(f32[2048,128]{1,0:T(8,128)} %get-tuple-element.49.dko_ref) | copy-start | bytes 3145732
  212.9 5.6 %copy-start.4 = (f32[2048,128]{1,0:T(8,128)S(1)}, f32[2048,128]{1,0:T(8,128)}, u32[]{:S(2)}) copy-start(f32[2048,128]{1,0:T(8,128)} %get-tuple-element.50.dvo_ref) | copy-start | bytes 3145732
  221.9 4.3 %copy-start.5 = (f32[2048,128]{1,0:T(8,128)S(1)}, f32[2048,128]{1,0:T(8,128)}, u32[]{:S(2)}) copy-start(f32[2048,128]{1,0:T(8,128)} %get-tuple-element.45.dko_ref) | copy-start | bytes 3145732
  221.9 4.3 %copy-start.6 = (f32[2048,128]{1,0:T(8,128)S(1)}, f32[2048,128]{1,0:T(8,128)}, u32[]{:S(2)}) copy-start(f32[2048,128]{1,0:T(8,128)} %get-tuple-element.46.dvo_ref) | copy-start | bytes 3145732

commit v7 on v6

--- a/solution.py
+++ b/solution.py
@@ -111,10 +111,12 @@
 
 
 def turn_kernel(x_ref, out_ref):
-    rows = x_ref.shape[0]
-    for i in range(rows // 256):
-        cut = slice(i * 256, (i + 1) * 256)
+    def some(i, carry):
+        cut = pl.ds(pl.multiple_of(i * 512, 512), 512)
         out_ref[:, cut] = x_ref[cut, :].T
+        return carry
+
+    lax.fori_loop(0, x_ref.shape[0] // 512, some, 0)
 
 
 def weight_kernel(me_ref, xt_ref, *rest, extra, slot, halves):
@@ -144,7 +146,7 @@
             o_s[pair, owners, 1] = got[:, HEAD_DIM:].reshape(shape)
             return carry
 
-        lax.fori_loop(0, rows // WEIGH_ROWS, some, 0, unroll=not halves)
+        lax.fori_loop(0, rows // WEIGH_ROWS, some, 0, unroll=halves)
         if halves:
             core = me_ref[0] % 2
             for out, mine in ((outs[0], core == pair), (outs[1], core != pair)):

time: 232 us -> 232 us (level)
  no operation moved by 1% of the time
where the time goes in v7:
time: 232 us; the launch traced here: 229 us
  Pallas kernels  101 us (44%)
  waiting for transfers between devices  65.7 us (28%)
  starting transfers between devices  53.9 us (23%)
  local copies, waits for them, and re-layouts  7.63 us (3%)
    pallas_call x3, Pallas kernels, attend(): pl.pallas_call(functools.partial(attend_kernel, head=head, extra=len(alia...  51.4 us
    ppermute x9, waiting for transfers between devices, shift(): return lax.ppermute(x, 'tp', [(i, (i + by) % tp) for i in range(tp)])  49.7 us
    all_to_all x6, starting transfers between devices, exchange(): return lax.all_to_all(x, 'kv', split_axis=0, concat_axis=0, tiled=True)  42.3 us
    pallas_call x3, Pallas kernels, weigh(): pl.pallas_call(functools.partial(weight_kernel, extra=len(aliases), slot=...  14 us
    all_to_all x6, waiting for transfers between devices, exchange(): return lax.all_to_all(x, 'kv', split_axis=0, concat_axis=0, tiled=True)  13.9 us
    ppermute x9, starting transfers between devices, shift(): return lax.ppermute(x, 'tp', [(i, (i + by) % tp) for i in range(tp)])  11.2 us
    pallas_call x3, Pallas kernels, land(): pl.pallas_call(functools.partial(land_kernel, head=head, spans=spans), gr...  10.3 us
    unnamed x40, local copies, waits for them, and re-layouts  7.63 us
  transfers between devices with their start and end apart: 17, of which 8 were waited for; matrix products, arithmetic and copies ran while one was open for 0% of the time, Pallas kernels for 40%

profile of v7, /device:TPU:0, one launch (start us, length us, event | category | flops | bytes accessed | tf_op | source)
XLA Modules:
  0.0 229.3 jit_solution(1018883325336019918)
XLA Ops:
  0.6 3.6 %first.1 = (bf16[32,1,4,32,128]{4,3,2,1,0:T(8,128)(2,1)}, s32[8,128]{1,0:T(8,128)}) custom-call(s32[1]{0:T(128)} %bitcast.me_ref, s32[3,12,2048]{2,1,0:T(8,128)} %bitcast.9, bf16[64,32,384]{2,1,0:T(8,128)(2,1)} %bitcast.5, bf16[64,32,384]{2,1,0:T(8,128)(2,1)} %bitcast.7), custom_call_target="tpu_custom_call" | custom-call | flops 67108864 | bytes 1048576 | tf_op jit(solution)/shard_map/first/pallas_call | solution.py:397
  4.2 8.5 %all-to-all-start = ((bf16[32,1,4,32,128]{4,3,2,1,0:T(8,128)(2,1)}), bf16[32,1,4,32,128]{4,3,2,1,0:T(8,128)(2,1)S(1)}, u32[]{:S(2)}, u32[]{:S(2)}) async-start(bf16[32,1,4,32,128]{4,3,2,1,0:T(8,128)(2,1)} %get-tuple-element.33), calls=%async_computation | async-start | bytes 2097152 | tf_op jit(solution)/shard_map/all_to_all | solution.py:649
  12.7 3.9 %pack.1 = (bf16[32,1,4,32,128]{4,3,2,1,0:T(8,128)(2,1)}, bf16[32,1,4,32,128]{4,3,2,1,0:T(8,128)(2,1)}) custom-call(s32[8,128]{1,0:T(8,128)} %get-tuple-element.34.tab_ref, bf16[64,32,384]{2,1,0:T(8,128)(2,1)} %bitcast.6, bf16[64,32,384]{2,1,0:T(8,128)(2,1)} %bitcast.8), custom_call_target="tpu_custom_call" | custom-call | flops 67108864 | bytes 1048576 | tf_op jit(solution)/shard_map/pack/pallas_call | solution.py:420
  16.7 13.3 %all-to-all-done.refs_6_ = bf16[32,1,4,32,128]{4,3,2,1,0:T(8,128)(2,1)S(1)} async-done(((bf16[32,1,4,32,128]{4,3,2,1,0:T(8,128)(2,1)}), bf16[32,1,4,32,128]{4,3,2,1,0:T(8,128)(2,1)S(1)}, u32[]{:S(2)}, u32[]{:S(2)}) %all-to-all-start) | async-done | bytes 1048608 | tf_op jit(solution)/shard_map/all_to_all | solution.py:649
  29.9 3.9 %all-to-all-start.2 = ((bf16[32,1,4,32,128]{4,3,2,1,0:T(8,128)(2,1)}), bf16[32,1,4,32,128]{4,3,2,1,0:T(8,128)(2,1)S(1)}, u32[]{:S(2)}, u32[]{:S(2)}) async-start(bf16[32,1,4,32,128]{4,3,2,1,0:T(8,128)(2,1)} %get-tuple-element.37), calls=%async_computation.2 | async-start | bytes 2097152 | tf_op jit(solution)/shard_map/all_to_all | solution.py:649
  33.9 3.7 %mask.1.refs_5_ = f32[3,64,2048]{2,1,0:T(8,128)} custom-call(s32[1]{0:T(128)} %bitcast.me_ref, s32[3,12,2048]{2,1,0:T(8,128)} %bitcast.10), custom_call_target="tpu_custom_call" | custom-call | flops 67108864 | bytes 1048576 | tf_op jit(solution)/shard_map/mask/pallas_call | solution.py:434
  37.5 16.8 %shard_map.102 = (bf16[2048,384]{1,0:T(8,128)(2,1)}, bf16[2048,128]{1,0:T(8,128)(2,1)}, f32[2048,128]{1,0:T(8,128)}, f32[2048,128]{1,0:T(8,128)}, bf16[32,1,4,32,128]{4,3,2,1,0:T(8,128)(2,1)}) custom-call(s32[1]{0:T(128)} %bitcast.me_ref, bf16[2048,384]{1,0:T(8,128)(2,1)} %refs_0_.5, bf16[2048,384]{1,0:T(8,128)(2,1)} %refs_1_.5, bf16[2048,384]{1,0:T(8,128)(2,1)} %refs_2_.5, ...), custom_call_target="tpu_custom_call" | custom-call | flops 5368709120 | bytes 8388608 | tf_op jit(solution)/shard_map/pallas_call | solution.py:496
  54.4 7.5 %all-to-all-start.1 = ((bf16[32,1,4,32,128]{4,3,2,1,0:T(8,128)(2,1)}), bf16[32,1,4,32,128]{4,3,2,1,0:T(8,128)(2,1)}, u32[]{:S(2)}, u32[]{:S(2)}) async-start(bf16[32,1,4,32,128]{4,3,2,1,0:T(8,128)(2,1)} %get-tuple-element.36), calls=%async_computation.1 | async-start | bytes 2097152 | tf_op jit(solution)/shard_map/all_to_all | solution.py:649
  61.9 2.8 %collective-permute-start.4 = (bf16[2048,128]{1,0:T(8,128)(2,1)}, bf16[2048,128]{1,0:T(8,128)(2,1)}, u32[]{:S(2)}, u32[]{:S(2)}) collective-permute-start(bf16[2048,128]{1,0:T(8,128)(2,1)} %get-tuple-element.47.rest_0_), channel_id=1, source_target_pairs={{0,3},{1,0},{2,1},{3,2},{4,7},{5,4},{6,5},{7,6},{8,11},{9,8},{10,9... | collective-permute-start | bytes 1572872 | tf_op jit(solution)/shard_map/ppermute | solution.py:653
  64.7 2.3 %collective-permute-start.6 = (bf16[2048,128]{1,0:T(8,128)(2,1)}, bf16[2048,128]{1,0:T(8,128)(2,1)}, u32[]{:S(2)}, u32[]{:S(2)}) collective-permute-start(bf16[2048,128]{1,0:T(8,128)(2,1)} %get-tuple-element.47.rest_0_), channel_id=1, source_target_pairs={{0,2},{1,3},{2,0},{3,1},{4,6},{5,7},{6,4},{7,5},{8,10},{9,11},{10,... | collective-permute-start | bytes 1572872 | tf_op jit(solution)/shard_map/ppermute | solution.py:653
  67.0 4.1 %turn.1.xt_ref = bf16[1024,2048]{1,0:T(8,128)(2,1)S(1)} custom-call(bf16[2048,1024]{1,0:T(8,128)(2,1)} %x_ref.1), custom_call_target="tpu_custom_call" | custom-call | flops 67108864 | bytes 1048576 | tf_op jit(solution)/shard_map/turn/pallas_call | solution.py:447
  71.1 18.0 %shard_map.103 = (bf16[2048,384]{1,0:T(8,128)(2,1)}, bf16[2048,128]{1,0:T(8,128)(2,1)}, f32[2048,128]{1,0:T(8,128)}, f32[2048,128]{1,0:T(8,128)}, bf16[32,2,4,32,128]{4,3,2,1,0:T(8,128)(2,1)}) custom-call(s32[1]{0:T(128)} %bitcast.me_ref, bf16[2048,384]{1,0:T(8,128)(2,1)} %refs_0_.5, bf16[2048,384]{1,0:T(8,128)(2,1)} %refs_1_.5, ...), custom_call_target="tpu_custom_call", output_to_operand_aliasing={{0}: (8, {})} | custom-call | flops 5368709120 | bytes 8388608 | tf_op jit(solution)/shard_map/pallas_call | solution.py:496
  89.1 2.1 collective-permute-done.5.rest_2_
  91.3 4.9 %weigh.4 = bf16[32,2,4,32,128]{4,3,2,1,0:T(8,128)(2,1)} custom-call(s32[1]{0:T(128)} %bitcast.me_ref, bf16[1024,2048]{1,0:T(8,128)(2,1)S(1)} %turn.1.xt_ref, bf16[2048,128]{1,0:T(8,128)(2,1)} %get-tuple-element.47.rest_0_, bf16[2048,128]{1,0:T(8,128)(2,1)} %collective-permute-done.4.rest_1_, ...), custom_call_target="tpu_custom_call", output_to_operand_aliasing={{}: (6, {})} | custom-call | flops 2147483648 | bytes 8388608 | tf_op jit(solution)/shard_map/weigh/pallas_call | solution.py:544
  96.2 7.5 %all-to-all-start.4 = ((bf16[32,2,4,32,128]{4,3,2,1,0:T(8,128)(2,1)}), bf16[32,2,4,32,128]{4,3,2,1,0:T(8,128)(2,1)}, u32[]{:S(2)}, u32[]{:S(2)}) async-start(bf16[32,2,4,32,128]{4,3,2,1,0:T(8,128)(2,1)} %weigh.4), calls=%async_computation.4 | async-start | bytes 4194304 | tf_op jit(solution)/shard_map/all_to_all | solution.py:649
  103.7 0.4 collective-permute-start
  104.1 1.7 collective-permute-start.1
  105.8 0.6 collective-permute-start.2
  106.4 12.2 %collective-permute-done.rest_1_ = bf16[2048,128]{1,0:T(8,128)(2,1)S(1)} collective-permute-done((bf16[2048,128]{1,0:T(8,128)(2,1)S(1)}, bf16[2048,128]{1,0:T(8,128)(2,1)S(1)}, u32[]{:S(2)}, u32[]{:S(2)}) %collective-permute-start) | collective-permute-done | bytes 524320 | tf_op jit(solution)/shard_map/ppermute | solution.py:653
  118.6 11.8 %collective-permute-done.1.rest_2_ = bf16[2048,128]{1,0:T(8,128)(2,1)S(1)} collective-permute-done((bf16[2048,128]{1,0:T(8,128)(2,1)S(1)}, bf16[2048,128]{1,0:T(8,128)(2,1)S(1)}, u32[]{:S(2)}, u32[]{:S(2)}) %collective-permute-start.1) | collective-permute-done | bytes 524320 | tf_op jit(solution)/shard_map/ppermute | solution.py:653
  130.3 0.8 copy-done.19
  131.2 2.2 copy-done.1
  133.4 4.6 %weigh.3 = (bf16[32,2,32,128]{3,2,1,0:T(8,128)(2,1)}, bf16[32,2,32,128]{3,2,1,0:T(8,128)(2,1)}) custom-call(s32[1]{0:T(128)} %bitcast.me_ref, bf16[1024,2048]{1,0:T(8,128)(2,1)S(1)} %copy-done.1, bf16[2048,128]{1,0:T(8,128)(2,1)} %get-tuple-element.41.rest_0_, bf16[2048,128]{1,0:T(8,128)(2,1)} %copy-done.17, bf16[2048,128]{1,0:T(8,128)(2,1)} %copy-done.19, ...), custom_call_target="tpu_custom_call" | custom-call | flops 2147483648 | bytes 8388608 | tf_op jit(solution)/shard_map/weigh/pallas_call | solution.py:544
  137.9 0.3 collective-permute-start.3
  138.3 16.6 %shard_map.104 = (bf16[2048,384]{1,0:T(8,128)(2,1)}, bf16[2048,128]{1,0:T(8,128)(2,1)}, f32[2048,128]{1,0:T(8,128)}, f32[2048,128]{1,0:T(8,128)}, bf16[32,6,32,128]{3,2,1,0:T(8,128)(2,1)}) custom-call(s32[1]{0:T(128)} %bitcast.me_ref, bf16[2048,384]{1,0:T(8,128)(2,1)} %refs_0_.5, bf16[2048,384]{1,0:T(8,128)(2,1)} %refs_1_.5, ...), custom_call_target="tpu_custom_call", output_to_operand_aliasing={{0}: (8, {})} | custom-call | flops 5368709120 | bytes 8388608 | tf_op jit(solution)/shard_map/pallas_call | solution.py:496
  154.9 0.8 copy-done.13
  155.6 2.2 join.2
  157.9 7.6 %all-to-all-start.3 = ((bf16[32,6,32,128]{3,2,1,0:T(8,128)(2,1)}), bf16[32,6,32,128]{3,2,1,0:T(8,128)(2,1)}, u32[]{:S(2)}, u32[]{:S(2)}) async-start(bf16[32,6,32,128]{3,2,1,0:T(8,128)(2,1)} %join.2), calls=%async_computation.3 | async-start | bytes 3145728 | tf_op jit(solution)/shard_map/all_to_all | solution.py:649
  165.5 0.7 collective-permute-start.7
  166.2 1.4 collective-permute-start.8
  167.6 1.2 collective-permute-start.9
  168.8 11.5 %collective-permute-done.7.rest_1_ = bf16[2048,128]{1,0:T(8,128)(2,1)S(1)} collective-permute-done((bf16[2048,128]{1,0:T(8,128)(2,1)S(1)}, bf16[2048,128]{1,0:T(8,128)(2,1)S(1)}, u32[]{:S(2)}, u32[]{:S(2)}) %collective-permute-start.7) | collective-permute-done | bytes 524320 | tf_op jit(solution)/shard_map/ppermute | solution.py:653
  180.3 12.1 %collective-permute-done.8.rest_2_ = bf16[2048,128]{1,0:T(8,128)(2,1)S(1)} collective-permute-done((bf16[2048,128]{1,0:T(8,128)(2,1)S(1)}, bf16[2048,128]{1,0:T(8,128)(2,1)S(1)}, u32[]{:S(2)}, u32[]{:S(2)}) %collective-permute-start.8) | collective-permute-done | bytes 524320 | tf_op jit(solution)/shard_map/ppermute | solution.py:653
  192.4 0.8 copy-done.18
  193.2 2.2 copy-done.2
  195.4 4.5 %weigh.5 = (bf16[32,2,32,128]{3,2,1,0:T(8,128)(2,1)}, bf16[32,2,32,128]{3,2,1,0:T(8,128)(2,1)}) custom-call(s32[1]{0:T(128)} %bitcast.me_ref, bf16[1024,2048]{1,0:T(8,128)(2,1)S(1)} %copy-done.2, bf16[2048,128]{1,0:T(8,128)(2,1)} %get-tuple-element.59.rest_0_, bf16[2048,128]{1,0:T(8,128)(2,1)} %copy-done.16, bf16[2048,128]{1,0:T(8,128)(2,1)} %copy-done.18, ...), custom_call_target="tpu_custom_call" | custom-call | flops 2147483648 | bytes 8388608 | tf_op jit(solution)/shard_map/weigh/pallas_call | solution.py:544
  200.0 0.1 collective-permute-start.10
  200.1 2.1 collective-permute-done.10.got_ref
  202.2 0.8 copy-done.12
  203.0 2.1 join.3
  205.1 7.4 %all-to-all-start.5 = ((bf16[32,2,32,128]{3,2,1,0:T(8,128)(2,1)}), bf16[32,2,32,128]{3,2,1,0:T(8,128)(2,1)}, u32[]{:S(2)}, u32[]{:S(2)}) async-start(bf16[32,2,32,128]{3,2,1,0:T(8,128)(2,1)} %join.3), calls=%async_computation.5 | async-start | bytes 1048576 | tf_op jit(solution)/shard_map/all_to_all | solution.py:649
  212.6 3.5 %shard_map.105 = (f32[2048,384]{1,0:T(8,128)}, f32[2048,384]{1,0:T(8,128)}) custom-call(s32[1]{0:T(128)} %bitcast.me_ref, s32[8,128]{1,0:T(8,128)S(1)} %copy-done.9, bf16[32,1,4,32,128]{4,3,2,1,0:T(8,128)(2,1)} %all-to-all-done.1.refs_6_.back_ref, f32[2048,128]{1,0:T(8,128)S(1)} %copy-done.7, f32[2048,128]{1,0:T(8,128)S(1)} %copy-done.8), custom_call_target="tpu_custom_call" | custom-call | flops 16777216 | bytes 1048576 | tf_op jit(solution)/shard_map/pallas_call | solution.py:636
  216.1 2.1 total.1.before_ref
  218.1 3.4 %shard_map.106 = (f32[2048,384]{1,0:T(8,128)}, f32[2048,384]{1,0:T(8,128)}) custom-call(s32[1]{0:T(128)} %bitcast.me_ref, s32[8,128]{1,0:T(8,128)S(1)} %copy-done.9, bf16[32,2,4,32,128]{4,3,2,1,0:T(8,128)(2,1)} %all-to-all-done.4.back_ref.got_ref, f32[2048,128]{1,0:T(8,128)S(1)} %copy-done.3, ...), custom_call_target="tpu_custom_call", output_to_operand_aliasing={{0}: (5, {}), {1}: (6, {})} | custom-call | flops 16777216 | bytes 1048576 | tf_op jit(solution)/shard_map/pallas_call | solution.py:636
  221.5 1.9 pairtotal.2.before_ref
  223.5 0.6 all-to-all-done.5.got_ref
  224.1 1.8 pairtotal.3
  225.9 3.4 %shard_map.107 = (f32[2048,384]{1,0:T(8,128)}, f32[2048,384]{1,0:T(8,128)}) custom-call(s32[1]{0:T(128)} %bitcast.me_ref, s32[8,128]{1,0:T(8,128)S(1)} %copy-done.9, bf16[32,6,32,128]{3,2,1,0:T(8,128)(2,1)} %all-to-all-done.3.back_ref.got_ref, f32[2048,128]{1,0:T(8,128)S(1)} %copy-done.5, ...), custom_call_target="tpu_custom_call", output_to_operand_aliasing={{0}: (5, {}), {1}: (6, {})} | custom-call | flops 16777216 | bytes 1048576 | tf_op jit(solution)/shard_map/pallas_call | solution.py:636
  (44 shorter events, 0.1 us)
Async XLA Ops:
  4.2 25.7 %all-to-all-start = ((bf16[32,1,4,32,128]{4,3,2,1,0:T(8,128)(2,1)}), bf16[32,1,4,32,128]{4,3,2,1,0:T(8,128)(2,1)S(1)}, u32[]{:S(2)}, u32[]{:S(2)}) async-start(bf16[32,1,4,32,128]{4,3,2,1,0:T(8,128)(2,1)} %get-tuple-element.33), calls=%async_computation | async-start | bytes 2097152 | tf_op jit(solution)/shard_map/all_to_all | solution.py:649
  29.9 7.6 %copy-start.11 = (bf16[32,1,4,32,128]{4,3,2,1,0:T(8,128)(2,1)}, bf16[32,1,4,32,128]{4,3,2,1,0:T(8,128)(2,1)S(1)}, u32[]{:S(2)}) copy-start(bf16[32,1,4,32,128]{4,3,2,1,0:T(8,128)(2,1)S(1)} %all-to-all-done.refs_6_) | copy-start | bytes 3145732
  29.9 24.5 %all-to-all-start.2 = ((bf16[32,1,4,32,128]{4,3,2,1,0:T(8,128)(2,1)}), bf16[32,1,4,32,128]{4,3,2,1,0:T(8,128)(2,1)S(1)}, u32[]{:S(2)}, u32[]{:S(2)}) async-start(bf16[32,1,4,32,128]{4,3,2,1,0:T(8,128)(2,1)} %get-tuple-element.37), calls=%async_computation.2 | async-start | bytes 2097152 | tf_op jit(solution)/shard_map/all_to_all | solution.py:649
  54.4 10.4 %copy-start.10 = (bf16[32,1,4,32,128]{4,3,2,1,0:T(8,128)(2,1)}, bf16[32,1,4,32,128]{4,3,2,1,0:T(8,128)(2,1)S(1)}, u32[]{:S(2)}) copy-start(bf16[32,1,4,32,128]{4,3,2,1,0:T(8,128)(2,1)S(1)} %all-to-all-done.2.refs_6_) | copy-start | bytes 3145732
  54.4 41.8 %all-to-all-start.1 = ((bf16[32,1,4,32,128]{4,3,2,1,0:T(8,128)(2,1)}), bf16[32,1,4,32,128]{4,3,2,1,0:T(8,128)(2,1)}, u32[]{:S(2)}, u32[]{:S(2)}) async-start(bf16[32,1,4,32,128]{4,3,2,1,0:T(8,128)(2,1)} %get-tuple-element.36), calls=%async_computation.1 | async-start | bytes 2097152 | tf_op jit(solution)/shard_map/all_to_all | solution.py:649
  61.9 27.2 %collective-permute-start.4 = (bf16[2048,128]{1,0:T(8,128)(2,1)}, bf16[2048,128]{1,0:T(8,128)(2,1)}, u32[]{:S(2)}, u32[]{:S(2)}) collective-permute-start(bf16[2048,128]{1,0:T(8,128)(2,1)} %get-tuple-element.47.rest_0_), channel_id=1, source_target_pairs={{0,3},{1,0},{2,1},{3,2},{4,7},{5,4},{6,5},{7,6},{8,11},{9,8},{10,9... | collective-permute-start | bytes 1572872 | tf_op jit(solution)/shard_map/ppermute | solution.py:653
  64.7 26.5 %collective-permute-start.5 = (bf16[2048,128]{1,0:T(8,128)(2,1)}, bf16[2048,128]{1,0:T(8,128)(2,1)}, u32[]{:S(2)}, u32[]{:S(2)}) collective-permute-start(bf16[2048,128]{1,0:T(8,128)(2,1)} %get-tuple-element.47.rest_0_), channel_id=1, source_target_pairs={{0,1},{1,2},{2,3},{3,0},{4,5},{5,6},{6,7},{7,4},{8,9},{9,10},{10,1... | collective-permute-start | bytes 1572872 | tf_op jit(solution)/shard_map/ppermute | solution.py:653
  64.7 26.5 %collective-permute-start.6 = (bf16[2048,128]{1,0:T(8,128)(2,1)}, bf16[2048,128]{1,0:T(8,128)(2,1)}, u32[]{:S(2)}, u32[]{:S(2)}) collective-permute-start(bf16[2048,128]{1,0:T(8,128)(2,1)} %get-tuple-element.47.rest_0_), channel_id=1, source_target_pairs={{0,2},{1,3},{2,0},{3,1},{4,6},{5,7},{6,4},{7,5},{8,10},{9,11},{10,... | collective-permute-start | bytes 1572872 | tf_op jit(solution)/shard_map/ppermute | solution.py:653
  71.1 20.1 %copy-start = (bf16[1024,2048]{1,0:T(8,128)(2,1)}, bf16[1024,2048]{1,0:T(8,128)(2,1)S(1)}, u32[]{:S(2)}) copy-start(bf16[1024,2048]{1,0:T(8,128)(2,1)S(1)} %turn.1.xt_ref) | copy-start | bytes 12582916
  96.2 7.5 %copy-start.14 = (bf16[2048,128]{1,0:T(8,128)(2,1)S(1)}, bf16[2048,128]{1,0:T(8,128)(2,1)}, u32[]{:S(2)}) copy-start(bf16[2048,128]{1,0:T(8,128)(2,1)} %get-tuple-element.41.rest_0_) | copy-start | bytes 1572868
  96.2 61.7 %all-to-all-start.4 = ((bf16[32,2,4,32,128]{4,3,2,1,0:T(8,128)(2,1)}), bf16[32,2,4,32,128]{4,3,2,1,0:T(8,128)(2,1)}, u32[]{:S(2)}, u32[]{:S(2)}) async-start(bf16[32,2,4,32,128]{4,3,2,1,0:T(8,128)(2,1)} %weigh.4), calls=%async_computation.4 | async-start | bytes 4194304 | tf_op jit(solution)/shard_map/all_to_all | solution.py:649
  103.7 14.9 %collective-permute-start = (bf16[2048,128]{1,0:T(8,128)(2,1)S(1)}, bf16[2048,128]{1,0:T(8,128)(2,1)S(1)}, u32[]{:S(2)}, u32[]{:S(2)}) collective-permute-start(bf16[2048,128]{1,0:T(8,128)(2,1)S(1)} %copy-done.14), channel_id=1, source_target_pairs={{0,3},{1,0},{2,1},{3,2},{4,7},{5,4},{6,5},{7,6},{8,11},{9,8},{10,9... | collective-permute-start | bytes 1572872 | tf_op jit(solution)/shard_map/ppermute | solution.py:653
  104.1 26.3 %collective-permute-start.1 = (bf16[2048,128]{1,0:T(8,128)(2,1)S(1)}, bf16[2048,128]{1,0:T(8,128)(2,1)S(1)}, u32[]{:S(2)}, u32[]{:S(2)}) collective-permute-start(bf16[2048,128]{1,0:T(8,128)(2,1)S(1)} %copy-done.14), channel_id=1, source_target_pairs={{0,1},{1,2},{2,3},{3,0},{4,5},{5,6},{6,7},{7,4},{8,9},{9,10},{10,1... | collective-permute-start | bytes 1572872 | tf_op jit(solution)/shard_map/ppermute | solution.py:653
  105.8 25.4 %collective-permute-start.2 = (bf16[2048,128]{1,0:T(8,128)(2,1)S(1)}, bf16[2048,128]{1,0:T(8,128)(2,1)}, u32[]{:S(2)}, u32[]{:S(2)}) collective-permute-start(bf16[2048,128]{1,0:T(8,128)(2,1)S(1)} %copy-done.14), channel_id=1, source_target_pairs={{0,2},{1,3},{2,0},{3,1},{4,6},{5,7},{6,4},{7,5},{8,10},{9,11},{10,... | collective-permute-start | bytes 1572872 | tf_op jit(solution)/shard_map/ppermute | solution.py:653
  118.6 11.8 %copy-start.17 = (bf16[2048,128]{1,0:T(8,128)(2,1)}, bf16[2048,128]{1,0:T(8,128)(2,1)S(1)}, u32[]{:S(2)}) copy-start(bf16[2048,128]{1,0:T(8,128)(2,1)S(1)} %collective-permute-done.rest_1_) | copy-start | bytes 1572868
  130.3 0.8 copy-start.19
  131.2 2.2 copy-start.1
  137.9 16.9 %collective-permute-start.3 = (bf16[32,2,32,128]{3,2,1,0:T(8,128)(2,1)}, bf16[32,2,32,128]{3,2,1,0:T(8,128)(2,1)S(1)}, u32[]{:S(2)}, u32[]{:S(2)}) collective-permute-start(bf16[32,2,32,128]{3,2,1,0:T(8,128)(2,1)} %get-tuple-element.43), channel_id=1, source_target_pairs={{0,4},{4,0},{8,12},{12,8},{16,20},{20,16},{24,28},{28,24},{32,36},... | collective-permute-start | bytes 1572872 | tf_op jit(solution)/shard_map/ppermute | solution.py:688
  154.9 0.8 copy-start.13
  157.9 7.6 %copy-start.15 = (bf16[2048,128]{1,0:T(8,128)(2,1)S(1)}, bf16[2048,128]{1,0:T(8,128)(2,1)}, u32[]{:S(2)}) copy-start(bf16[2048,128]{1,0:T(8,128)(2,1)} %get-tuple-element.59.rest_0_) | copy-start | bytes 1572868
  157.9 47.2 %all-to-all-start.3 = ((bf16[32,6,32,128]{3,2,1,0:T(8,128)(2,1)}), bf16[32,6,32,128]{3,2,1,0:T(8,128)(2,1)}, u32[]{:S(2)}, u32[]{:S(2)}) async-start(bf16[32,6,32,128]{3,2,1,0:T(8,128)(2,1)} %join.2), calls=%async_computation.3 | async-start | bytes 3145728 | tf_op jit(solution)/shard_map/all_to_all | solution.py:649
  165.5 14.9 %collective-permute-start.7 = (bf16[2048,128]{1,0:T(8,128)(2,1)S(1)}, bf16[2048,128]{1,0:T(8,128)(2,1)S(1)}, u32[]{:S(2)}, u32[]{:S(2)}) collective-permute-start(bf16[2048,128]{1,0:T(8,128)(2,1)S(1)} %copy-done.15), channel_id=1, source_target_pairs={{0,3},{1,0},{2,1},{3,2},{4,7},{5,4},{6,5},{7,6},{8,11},{9,8},{10,9... | collective-permute-start | bytes 1572872 | tf_op jit(solution)/shard_map/ppermute | solution.py:653
  166.2 26.2 %collective-permute-start.8 = (bf16[2048,128]{1,0:T(8,128)(2,1)S(1)}, bf16[2048,128]{1,0:T(8,128)(2,1)S(1)}, u32[]{:S(2)}, u32[]{:S(2)}) collective-permute-start(bf16[2048,128]{1,0:T(8,128)(2,1)S(1)} %copy-done.15), channel_id=1, source_target_pairs={{0,1},{1,2},{2,3},{3,0},{4,5},{5,6},{6,7},{7,4},{8,9},{9,10},{10,1... | collective-permute-start | bytes 1572872 | tf_op jit(solution)/shard_map/ppermute | solution.py:653
  167.6 25.6 %collective-permute-start.9 = (bf16[2048,128]{1,0:T(8,128)(2,1)S(1)}, bf16[2048,128]{1,0:T(8,128)(2,1)}, u32[]{:S(2)}, u32[]{:S(2)}) collective-permute-start(bf16[2048,128]{1,0:T(8,128)(2,1)S(1)} %copy-done.15), channel_id=1, source_target_pairs={{0,2},{1,3},{2,0},{3,1},{4,6},{5,7},{6,4},{7,5},{8,10},{9,11},{10,... | collective-permute-start | bytes 1572872 | tf_op jit(solution)/shard_map/ppermute | solution.py:653
  180.3 12.1 %copy-start.16 = (bf16[2048,128]{1,0:T(8,128)(2,1)}, bf16[2048,128]{1,0:T(8,128)(2,1)S(1)}, u32[]{:S(2)}) copy-start(bf16[2048,128]{1,0:T(8,128)(2,1)S(1)} %collective-permute-done.7.rest_1_) | copy-start | bytes 1572868
  192.4 0.8 copy-start.18
  193.2 2.2 copy-start.2
  199.9 12.6 %copy-start.7 = (f32[2048,128]{1,0:T(8,128)S(1)}, f32[2048,128]{1,0:T(8,128)}, u32[]{:S(2)}) copy-start(f32[2048,128]{1,0:T(8,128)} %get-tuple-element.51.dko_ref) | copy-start | bytes 3145732
  200.0 12.6 %copy-start.8 = (f32[2048,128]{1,0:T(8,128)S(1)}, f32[2048,128]{1,0:T(8,128)}, u32[]{:S(2)}) copy-start(f32[2048,128]{1,0:T(8,128)} %get-tuple-element.52.dvo_ref) | copy-start | bytes 3145732
  200.0 12.6 %copy-start.9 = (s32[8,128]{1,0:T(8,128)S(1)}, s32[8,128]{1,0:T(8,128)}, u32[]{:S(2)}) copy-start(s32[8,128]{1,0:T(8,128)} %get-tuple-element.34.tab_ref) | copy-start | bytes 12292
  200.0 2.2 collective-permute-start.10
  202.2 0.8 copy-start.12
  205.1 18.9 %all-to-all-start.5 = ((bf16[32,2,32,128]{3,2,1,0:T(8,128)(2,1)}), bf16[32,2,32,128]{3,2,1,0:T(8,128)(2,1)}, u32[]{:S(2)}, u32[]{:S(2)}) async-start(bf16[32,2,32,128]{3,2,1,0:T(8,128)(2,1)} %join.3), calls=%async_computation.5 | async-start | bytes 1048576 | tf_op jit(solution)/shard_map/all_to_all | solution.py:649
  212.5 5.6 %copy-start.3 = (f32[2048,128]{1,0:T(8,128)S(1)}, f32[2048,128]{1,0:T(8,128)}, u32[]{:S(2)}) copy-start(f32[2048,128]{1,0:T(8,128)} %get-tuple-element.49.dko_ref) | copy-start | bytes 3145732
  212.6 5.6 %copy-start.4 = (f32[2048,128]{1,0:T(8,128)S(1)}, f32[2048,128]{1,0:T(8,128)}, u32[]{:S(2)}) copy-start(f32[2048,128]{1,0:T(8,128)} %get-tuple-element.50.dvo_ref) | copy-start | bytes 3145732
  221.5 4.3 %copy-start.5 = (f32[2048,128]{1,0:T(8,128)S(1)}, f32[2048,128]{1,0:T(8,128)}, u32[]{:S(2)}) copy-start(f32[2048,128]{1,0:T(8,128)} %get-tuple-element.45.dko_ref) | copy-start | bytes 3145732
  221.5 4.3 %copy-start.6 = (f32[2048,128]{1,0:T(8,128)S(1)}, f32[2048,128]{1,0:T(8,128)}, u32[]{:S(2)}) copy-start(f32[2048,128]{1,0:T(8,128)} %get-tuple-element.46.dvo_ref) | copy-start | bytes 3145732
